TPU v7x, 512 devices: a whole 4x8x8 slice. The times are simulated.
512 devices in a mesh: ep: 32 (over z, x), tp: 16 (over y, core).
Axes of the slice: x: 4, y: 8, z: 8, core: 2. Of those that a mesh axis runs over, the one named last changes fastest.
Arguments:
- queries: bfloat16 [12288, 2048], P('ep', 'tp'), may hold values from -8 to 8
- keys: bfloat16 [12288, 2048], P('ep', 'tp'), may hold values from -8 to 8
- values: bfloat16 [12288, 2048], P('ep', 'tp'), may hold values from -6 to 6
- key_offset: bfloat16 [12288, 16], P('ep', 'tp'), may hold values from -15.25 to -0.4
- rows: bfloat16 [4096, 2048], P('ep'), may hold values from -6 to 6
- gain: float32 [2048], replicated, may hold values from 0.1 to 1.9
- gate_w: bfloat16 [32, 2048, 3584], P('ep', None, 'tp'), may hold values from -0.125 to 0.125
- up_w: bfloat16 [32, 2048, 3584], P('ep', None, 'tp'), may hold values from -0.125 to 0.125
- down_w: bfloat16 [32, 3584, 2048], P('ep', 'tp'), may hold values from -0.09375 to 0.09375
- expert_ids: int32 [4096, 2], P('ep'), may hold values from 0 to 31, all different within a row; in each aligned block of 128 rows (0 to 127, 128 to 255, ...) at most 16 rows name the same one
- route_weights: float32 [4096, 2], P('ep'), may hold values from 0.2 to 1
Outputs:
- attended: bfloat16 [12288, 2048], P('ep', 'tp')
- mixed: bfloat16 [4096, 2048], P('ep')
Inputs may be any that keep to these rules, and one draw needn't show every extreme that they name: `expert_ids`: each token names 2 different experts; among the 128 tokens of one ep index no expert is chosen more than 16 times, and in some such block an expert is chosen exactly 16 times.
All inputs are finite; a program needn't handle non-finite values.
Results may differ from a plain program's by a relative error of at most 0.019.
Values may be sent and summed in bfloat16 or wider, within the bound.
No kernel may reach another device: no remote copies, remote signals or barrier semaphores. Data moves between devices by JAX's collectives and lax.ppermute only.
A program may use at most 128 MiB of HBM per device.

v0:
```python
import jax
import jax.numpy as jnp
from jax import lax
from jax.sharding import PartitionSpec as P

EPSILON = 1e-06


def in_blocks(x, dim, peers):
    before, after = (x.shape[:dim], x.shape[dim + 1 :])
    return jnp.moveaxis(x.reshape(*before, peers, -1, *after), dim, 0)


def sent_and_summed(x, axis, dim):
    parts = in_blocks(x, dim, lax.axis_size(axis))
    arrived = lax.all_to_all(parts, axis, split_axis=0, concat_axis=0, tiled=True)
    return arrived.astype(jnp.float32).sum(axis=0)


def joined_along(parts, dim):
    shape = list(parts.shape[1:])
    shape[dim] *= parts.shape[0]
    return jnp.moveaxis(parts, 0, dim).reshape(shape)


def sent_to_all(x, axis):
    copies = jnp.broadcast_to(x, (lax.axis_size(axis), *x.shape))
    return lax.all_to_all(copies, axis, split_axis=0, concat_axis=0, tiled=True)


def collect(x, axis, dim):
    return joined_along(sent_to_all(x, axis), dim)


def stick_mixer(queries, keys, values, key_offset):
    position = lax.axis_index("ep")
    query_len = queries.shape[0]
    heads = key_offset.shape[1]
    head_dim = queries.shape[1] // heads
    scale = head_dim ** (-0.5)
    query_heads = queries.reshape(query_len, heads, head_dim)
    query_pos = position * query_len + jnp.arange(query_len, dtype=jnp.int32)
    last_row = (position + 1) * query_len
    key_piece = lax.all_gather(keys, "ep", axis=0, tiled=True)
    value_piece = lax.all_gather(values, "ep", axis=0, tiled=True)
    offset_piece = lax.all_gather(key_offset, "ep", axis=0, tiled=True)
    block_count = key_piece.shape[0] // query_len
    key_split = key_piece.reshape(block_count, query_len, heads, head_dim)
    value_split = value_piece.reshape(block_count, query_len, heads, head_dim)
    offset_split = offset_piece.reshape(block_count, query_len, heads)

    def compute_block(key_here, value_here, offset_here, key_start):
        key_pos = key_start + jnp.arange(query_len, dtype=jnp.int32)
        logits = (
            jnp.einsum("qhd,khd->hqk", query_heads, key_here, preferred_element_type=jnp.float32)
            * scale
        )
        logits = logits + offset_here.astype(jnp.float32).T[:, None, :]
        strict = key_pos[None, None, :] < query_pos[None, :, None]
        breaks = jnp.where(strict, jax.nn.log_sigmoid(-logits), 0.0)
        within = lax.cumsum(breaks, axis=2, reverse=True) - breaks
        local = jnp.where(strict, jnp.exp(jax.nn.log_sigmoid(logits) + within), 0.0).astype(
            jnp.bfloat16
        )
        summed = jnp.einsum("hqk,khd->hqd", local, value_here, preferred_element_type=jnp.float32)
        return (summed, jnp.sum(breaks, axis=2))

    def skip_block(key_here, value_here, offset_here, key_start):
        return (
            jnp.zeros((heads, query_len, head_dim), jnp.float32),
            jnp.zeros((heads, query_len), jnp.float32),
        )

    def one_block(args):
        key_here, value_here, offset_here, block_index = args
        key_start = block_index * query_len
        return lax.cond(
            key_start < last_row,
            compute_block,
            skip_block,
            key_here,
            value_here,
            offset_here,
            key_start,
        )

    sums, totals = lax.map(
        one_block, (key_split, value_split, offset_split, jnp.arange(block_count, dtype=jnp.int32))
    )
    sums, totals = (sums, totals)
    later = lax.cumsum(totals, axis=0, reverse=True) - totals
    combined = jnp.einsum("bhq,bhqd->qhd", jnp.exp(later), sums)
    return combined.reshape(query_len, heads * head_dim).astype(jnp.bfloat16)


def routed_experts(rows, gain, gate_w, up_w, down_w, expert_ids, route_weights):
    ep_count = lax.axis_size("ep")
    local_experts = gate_w.shape[0]
    experts_all = ep_count * local_experts
    token_count = rows.shape[0]
    choose_count = expert_ids.shape[1]
    width = rows.shape[1]
    capacity = 2 * choose_count * token_count // experts_all
    rows_float = rows.astype(jnp.float32)
    normed = rows_float * lax.rsqrt(
        jnp.mean(rows_float * rows_float, axis=1, keepdims=True) + EPSILON
    )
    normed = (normed * gain[None, :]).astype(jnp.bfloat16)
    flat_ids = expert_ids.reshape(-1)
    onehot = (flat_ids[:, None] == jnp.arange(experts_all, dtype=jnp.int32)[None, :]).astype(
        jnp.int32
    )
    ranked = jnp.sum((jnp.cumsum(onehot, axis=0) - onehot) * onehot, axis=1)
    token_of = jnp.arange(token_count * choose_count, dtype=jnp.int32) // choose_count
    source_rows = (
        jnp.zeros((experts_all * capacity,), jnp.int32)
        .at[flat_ids * capacity + ranked]
        .set(token_of)
    )
    outgoing = normed[source_rows].reshape(ep_count, local_experts, capacity, width)
    arrived = lax.all_to_all(outgoing, "ep", split_axis=0, concat_axis=0, tiled=True)
    gate_val = jnp.einsum("sxcd,xdf->csxf", arrived, gate_w, preferred_element_type=jnp.float32)
    up_val = jnp.einsum("sxcd,xdf->csxf", arrived, up_w, preferred_element_type=jnp.float32)
    hidden = (jax.nn.silu(gate_val) * up_val).astype(jnp.bfloat16)
    share = sent_and_summed(
        jnp.einsum("csxf,xfd->csxd", hidden, down_w, preferred_element_type=jnp.float32).astype(
            jnp.bfloat16
        ),
        "tp",
        0,
    ).astype(jnp.bfloat16)
    returned = lax.all_to_all(share, "ep", split_axis=1, concat_axis=1, tiled=True)
    whole_slots = collect(returned, "tp", 0)
    flat_out = whole_slots.reshape(capacity * experts_all, width)
    slot_index = ranked * experts_all + flat_ids
    picked = flat_out[slot_index].astype(jnp.float32).reshape(token_count, choose_count, width)
    return jnp.sum(picked * route_weights[:, :, None], axis=1).astype(jnp.bfloat16)


def body(
    queries, keys, values, key_offset, rows, gain, gate_w, up_w, down_w, expert_ids, route_weights
):
    attended = stick_mixer(queries, keys, values, key_offset)
    mixed = routed_experts(rows, gain, gate_w, up_w, down_w, expert_ids, route_weights)
    return (attended, mixed)


def solution(mesh):
    in_specs = (
        P("ep", "tp"),
        P("ep", "tp"),
        P("ep", "tp"),
        P("ep", "tp"),
        P("ep", None),
        P(),
        P("ep", None, "tp"),
        P("ep", None, "tp"),
        P("ep", "tp", None),
        P("ep", None),
        P("ep", None),
    )
    out_specs = (P("ep", "tp"), P("ep", None))
    return jax.shard_map(body, mesh=mesh, in_specs=in_specs, out_specs=out_specs, check_vma=False)
```

profile of v0, /device:TPU:463, one launch (start us, length us, event | category | flops | bytes accessed | tf_op | source)
XLA Modules:
  0.0 519.0 jit_solution(13295193791613204802)
XLA Ops:
  17.3 6.6 %all-to-all-start = ((bf16[32,1,16,2048]{3,2,1,0:T(8,128)(2,1)}), bf16[32,1,16,2048]{3,2,1,0:T(8,128)(2,1)S(1)}, u32[]{:S(2)}, u32[]{:S(2)}) async-start(bf16[32,1,16,2048]{3,2,1,0:T(8,128)(2,1)} %bitcast.23), calls=%async_computation | async-start | bytes 4194304 | tf_op jit(solution)/shard_map/all_to_all | solution.py:121
  24.6 48.0 %all-to-all-done = bf16[32,1,16,2048]{3,2,1,0:T(8,128)(2,1)S(1)} async-done(((bf16[32,1,16,2048]{3,2,1,0:T(8,128)(2,1)}), bf16[32,1,16,2048]{3,2,1,0:T(8,128)(2,1)S(1)}, u32[]{:S(2)}, u32[]{:S(2)}) %all-to-all-start) | async-done | bytes 2097184 | tf_op jit(solution)/shard_map/all_to_all | solution.py:121
  76.1 58.9 %all_to_all.23 = bf16[16,1,32,1,2048]{4,2,3,1,0:T(8,128)(2,1)S(1)} all-to-all(bf16[16,1,32,1,2048]{4,2,3,1,0:T(8,128)(2,1)S(1)} %fusion.22), channel_id=1, replica_groups=mesh['ep'=32,'tp'=16] {'tp'}, dimensions={0} | all-to-all | bytes 4194304 | tf_op jit(solution)/shard_map/all_to_all | solution.py:16
  138.3 9.8 %all-to-all-start.2 = ((bf16[32,2,1024]{2,1,0:T(2,128)(2,1)}), bf16[32,2,1024]{2,1,0:T(2,128)(2,1)S(1)}, u32[]{:S(2)}, u32[]{:S(2)}) async-start(bf16[32,2,1024]{2,1,0:T(2,128)(2,1)} %reshape.303), calls=%async_computation.2 | async-start | bytes 262144 | tf_op jit(solution)/shard_map/all_to_all | solution.py:132
  148.2 37.1 %all_gather.10 = bf16[12288,1]{0,1:T(2,128)(2,1)S(1)} all-gather(bf16[384,1]{0,1:T(2,128)(2,1)S(1)} %copy-done.1), channel_id=1, replica_groups=mesh['ep'=32,'tp'=16] {'ep'}, dimensions={0}, use_global_device_ids=true | all-gather | bytes 25344 | tf_op jit(solution)/shard_map/all_gather | solution.py:46
  187.4 16.1 %all-to-all-start.3 = ((bf16[16,1,32,1,2048]{4,2,3,1,0:T(8,128)(2,1)}), bf16[16,1,32,1,2048]{4,2,3,1,0:T(8,128)(2,1)}, u32[]{:S(2)}, u32[]{:S(2)}) async-start(bf16[16,1,32,1,2048]{4,2,3,1,0:T(8,128)(2,1)} %broadcast_in_dim.46), calls=%async_computation.3 | async-start | bytes 4194304 | tf_op jit(solution)/shard_map/all_to_all | solution.py:28
  203.7 291.9 %while.13 = (s32[]{:T(128)}, bf16[32,1,384,128]{3,2,1,0:T(8,128)(2,1)}, f32[32,1,384]{2,1,0:T(1,128)S(1)}, s32[32]{0:T(128)S(1)}, s32[]{:T(128)}, /*index=5*/bf1...) while((s32[]{:T(128)}, ...), condition=%wide.region_6.7_spmd.clone, body=%wide.region_0.6_spmd.clone.sunk | while | flops 99241728 | bytes 5957639 | solution.py:87
  204.9 7.2 %conditional.3 = (bf16[1,1,384,128]{3,2,1,0:T(8,128)(2,1)S(1)}, f32[1,1,384]{2,1,0:T(1,128)S(1)}) conditional(s32[]{:T(128)} %convert_element_type.99, () %tuple.52, (s32[]{:T(128)}, s32[]{:T(128)}, bf16[32,384,1,128]{3,1,2,0:T(8,128)(2,1)}, s32[]{:T(128)}, bf16[384,1,128]{2,0,1:T(8,128)(2,1)S(1)}, /*index=5*/bf16[32,384,1]{1,0,2:T(8,128)(2,1)S(1)}, ...), branch_computations={%region_1.1_spmd, %region_2.5_spmd} | conditional | flops 99241728 | bytes 5755680 | solution.py:77
  206.5 3.5 fusion.4
  214.1 7.2 %conditional.3 = (bf16[1,1,384,128]{3,2,1,0:T(8,128)(2,1)S(1)}, f32[1,1,384]{2,1,0:T(1,128)S(1)}) conditional(s32[]{:T(128)} %convert_element_type.99, () %tuple.52, (s32[]{:T(128)}, s32[]{:T(128)}, bf16[32,384,1,128]{3,1,2,0:T(8,128)(2,1)}, s32[]{:T(128)}, bf16[384,1,128]{2,0,1:T(8,128)(2,1)S(1)}, /*index=5*/bf16[32,384,1]{1,0,2:T(8,128)(2,1)S(1)}, ...), branch_computations={%region_1.1_spmd, %region_2.5_spmd} | conditional | flops 99241728 | bytes 5755680 | solution.py:77
  215.6 3.5 fusion.4
  223.2 7.2 %conditional.3 = (bf16[1,1,384,128]{3,2,1,0:T(8,128)(2,1)S(1)}, f32[1,1,384]{2,1,0:T(1,128)S(1)}) conditional(s32[]{:T(128)} %convert_element_type.99, () %tuple.52, (s32[]{:T(128)}, s32[]{:T(128)}, bf16[32,384,1,128]{3,1,2,0:T(8,128)(2,1)}, s32[]{:T(128)}, bf16[384,1,128]{2,0,1:T(8,128)(2,1)S(1)}, /*index=5*/bf16[32,384,1]{1,0,2:T(8,128)(2,1)S(1)}, ...), branch_computations={%region_1.1_spmd, %region_2.5_spmd} | conditional | flops 99241728 | bytes 5755680 | solution.py:77
  224.7 3.5 fusion.4
  232.3 7.2 %conditional.3 = (bf16[1,1,384,128]{3,2,1,0:T(8,128)(2,1)S(1)}, f32[1,1,384]{2,1,0:T(1,128)S(1)}) conditional(s32[]{:T(128)} %convert_element_type.99, () %tuple.52, (s32[]{:T(128)}, s32[]{:T(128)}, bf16[32,384,1,128]{3,1,2,0:T(8,128)(2,1)}, s32[]{:T(128)}, bf16[384,1,128]{2,0,1:T(8,128)(2,1)S(1)}, /*index=5*/bf16[32,384,1]{1,0,2:T(8,128)(2,1)S(1)}, ...), branch_computations={%region_1.1_spmd, %region_2.5_spmd} | conditional | flops 99241728 | bytes 5755680 | solution.py:77
  233.9 3.5 fusion.4
  241.4 7.2 %conditional.3 = (bf16[1,1,384,128]{3,2,1,0:T(8,128)(2,1)S(1)}, f32[1,1,384]{2,1,0:T(1,128)S(1)}) conditional(s32[]{:T(128)} %convert_element_type.99, () %tuple.52, (s32[]{:T(128)}, s32[]{:T(128)}, bf16[32,384,1,128]{3,1,2,0:T(8,128)(2,1)}, s32[]{:T(128)}, bf16[384,1,128]{2,0,1:T(8,128)(2,1)S(1)}, /*index=5*/bf16[32,384,1]{1,0,2:T(8,128)(2,1)S(1)}, ...), branch_computations={%region_1.1_spmd, %region_2.5_spmd} | conditional | flops 99241728 | bytes 5755680 | solution.py:77
  243.0 3.5 fusion.4
  250.6 7.2 %conditional.3 = (bf16[1,1,384,128]{3,2,1,0:T(8,128)(2,1)S(1)}, f32[1,1,384]{2,1,0:T(1,128)S(1)}) conditional(s32[]{:T(128)} %convert_element_type.99, () %tuple.52, (s32[]{:T(128)}, s32[]{:T(128)}, bf16[32,384,1,128]{3,1,2,0:T(8,128)(2,1)}, s32[]{:T(128)}, bf16[384,1,128]{2,0,1:T(8,128)(2,1)S(1)}, /*index=5*/bf16[32,384,1]{1,0,2:T(8,128)(2,1)S(1)}, ...), branch_computations={%region_1.1_spmd, %region_2.5_spmd} | conditional | flops 99241728 | bytes 5755680 | solution.py:77
  252.1 3.5 fusion.4
  259.7 7.2 %conditional.3 = (bf16[1,1,384,128]{3,2,1,0:T(8,128)(2,1)S(1)}, f32[1,1,384]{2,1,0:T(1,128)S(1)}) conditional(s32[]{:T(128)} %convert_element_type.99, () %tuple.52, (s32[]{:T(128)}, s32[]{:T(128)}, bf16[32,384,1,128]{3,1,2,0:T(8,128)(2,1)}, s32[]{:T(128)}, bf16[384,1,128]{2,0,1:T(8,128)(2,1)S(1)}, /*index=5*/bf16[32,384,1]{1,0,2:T(8,128)(2,1)S(1)}, ...), branch_computations={%region_1.1_spmd, %region_2.5_spmd} | conditional | flops 99241728 | bytes 5755680 | solution.py:77
  261.2 3.5 fusion.4
  268.8 7.2 %conditional.3 = (bf16[1,1,384,128]{3,2,1,0:T(8,128)(2,1)S(1)}, f32[1,1,384]{2,1,0:T(1,128)S(1)}) conditional(s32[]{:T(128)} %convert_element_type.99, () %tuple.52, (s32[]{:T(128)}, s32[]{:T(128)}, bf16[32,384,1,128]{3,1,2,0:T(8,128)(2,1)}, s32[]{:T(128)}, bf16[384,1,128]{2,0,1:T(8,128)(2,1)S(1)}, /*index=5*/bf16[32,384,1]{1,0,2:T(8,128)(2,1)S(1)}, ...), branch_computations={%region_1.1_spmd, %region_2.5_spmd} | conditional | flops 99241728 | bytes 5755680 | solution.py:77
  270.4 3.5 fusion.4
  277.9 7.2 %conditional.3 = (bf16[1,1,384,128]{3,2,1,0:T(8,128)(2,1)S(1)}, f32[1,1,384]{2,1,0:T(1,128)S(1)}) conditional(s32[]{:T(128)} %convert_element_type.99, () %tuple.52, (s32[]{:T(128)}, s32[]{:T(128)}, bf16[32,384,1,128]{3,1,2,0:T(8,128)(2,1)}, s32[]{:T(128)}, bf16[384,1,128]{2,0,1:T(8,128)(2,1)S(1)}, /*index=5*/bf16[32,384,1]{1,0,2:T(8,128)(2,1)S(1)}, ...), branch_computations={%region_1.1_spmd, %region_2.5_spmd} | conditional | flops 99241728 | bytes 5755680 | solution.py:77
  279.5 3.5 fusion.4
  287.0 7.2 %conditional.3 = (bf16[1,1,384,128]{3,2,1,0:T(8,128)(2,1)S(1)}, f32[1,1,384]{2,1,0:T(1,128)S(1)}) conditional(s32[]{:T(128)} %convert_element_type.99, () %tuple.52, (s32[]{:T(128)}, s32[]{:T(128)}, bf16[32,384,1,128]{3,1,2,0:T(8,128)(2,1)}, s32[]{:T(128)}, bf16[384,1,128]{2,0,1:T(8,128)(2,1)S(1)}, /*index=5*/bf16[32,384,1]{1,0,2:T(8,128)(2,1)S(1)}, ...), branch_computations={%region_1.1_spmd, %region_2.5_spmd} | conditional | flops 99241728 | bytes 5755680 | solution.py:77
  288.6 3.5 fusion.4
  296.1 7.2 %conditional.3 = (bf16[1,1,384,128]{3,2,1,0:T(8,128)(2,1)S(1)}, f32[1,1,384]{2,1,0:T(1,128)S(1)}) conditional(s32[]{:T(128)} %convert_element_type.99, () %tuple.52, (s32[]{:T(128)}, s32[]{:T(128)}, bf16[32,384,1,128]{3,1,2,0:T(8,128)(2,1)}, s32[]{:T(128)}, bf16[384,1,128]{2,0,1:T(8,128)(2,1)S(1)}, /*index=5*/bf16[32,384,1]{1,0,2:T(8,128)(2,1)S(1)}, ...), branch_computations={%region_1.1_spmd, %region_2.5_spmd} | conditional | flops 99241728 | bytes 5755680 | solution.py:77
  297.7 3.5 fusion.4
  305.3 7.2 %conditional.3 = (bf16[1,1,384,128]{3,2,1,0:T(8,128)(2,1)S(1)}, f32[1,1,384]{2,1,0:T(1,128)S(1)}) conditional(s32[]{:T(128)} %convert_element_type.99, () %tuple.52, (s32[]{:T(128)}, s32[]{:T(128)}, bf16[32,384,1,128]{3,1,2,0:T(8,128)(2,1)}, s32[]{:T(128)}, bf16[384,1,128]{2,0,1:T(8,128)(2,1)S(1)}, /*index=5*/bf16[32,384,1]{1,0,2:T(8,128)(2,1)S(1)}, ...), branch_computations={%region_1.1_spmd, %region_2.5_spmd} | conditional | flops 99241728 | bytes 5755680 | solution.py:77
  314.4 7.2 %conditional.3 = (bf16[1,1,384,128]{3,2,1,0:T(8,128)(2,1)S(1)}, f32[1,1,384]{2,1,0:T(1,128)S(1)}) conditional(s32[]{:T(128)} %convert_element_type.99, () %tuple.52, (s32[]{:T(128)}, s32[]{:T(128)}, bf16[32,384,1,128]{3,1,2,0:T(8,128)(2,1)}, s32[]{:T(128)}, bf16[384,1,128]{2,0,1:T(8,128)(2,1)S(1)}, /*index=5*/bf16[32,384,1]{1,0,2:T(8,128)(2,1)S(1)}, ...), branch_computations={%region_1.1_spmd, %region_2.5_spmd} | conditional | flops 99241728 | bytes 5755680 | solution.py:77
  316.0 3.5 fusion.4
  323.5 7.2 %conditional.3 = (bf16[1,1,384,128]{3,2,1,0:T(8,128)(2,1)S(1)}, f32[1,1,384]{2,1,0:T(1,128)S(1)}) conditional(s32[]{:T(128)} %convert_element_type.99, () %tuple.52, (s32[]{:T(128)}, s32[]{:T(128)}, bf16[32,384,1,128]{3,1,2,0:T(8,128)(2,1)}, s32[]{:T(128)}, bf16[384,1,128]{2,0,1:T(8,128)(2,1)S(1)}, /*index=5*/bf16[32,384,1]{1,0,2:T(8,128)(2,1)S(1)}, ...), branch_computations={%region_1.1_spmd, %region_2.5_spmd} | conditional | flops 99241728 | bytes 5755680 | solution.py:77
  325.1 3.5 fusion.4
  332.6 7.2 %conditional.3 = (bf16[1,1,384,128]{3,2,1,0:T(8,128)(2,1)S(1)}, f32[1,1,384]{2,1,0:T(1,128)S(1)}) conditional(s32[]{:T(128)} %convert_element_type.99, () %tuple.52, (s32[]{:T(128)}, s32[]{:T(128)}, bf16[32,384,1,128]{3,1,2,0:T(8,128)(2,1)}, s32[]{:T(128)}, bf16[384,1,128]{2,0,1:T(8,128)(2,1)S(1)}, /*index=5*/bf16[32,384,1]{1,0,2:T(8,128)(2,1)S(1)}, ...), branch_computations={%region_1.1_spmd, %region_2.5_spmd} | conditional | flops 99241728 | bytes 5755680 | solution.py:77
  334.2 3.5 fusion.4
  341.8 7.2 %conditional.3 = (bf16[1,1,384,128]{3,2,1,0:T(8,128)(2,1)S(1)}, f32[1,1,384]{2,1,0:T(1,128)S(1)}) conditional(s32[]{:T(128)} %convert_element_type.99, () %tuple.52, (s32[]{:T(128)}, s32[]{:T(128)}, bf16[32,384,1,128]{3,1,2,0:T(8,128)(2,1)}, s32[]{:T(128)}, bf16[384,1,128]{2,0,1:T(8,128)(2,1)S(1)}, /*index=5*/bf16[32,384,1]{1,0,2:T(8,128)(2,1)S(1)}, ...), branch_computations={%region_1.1_spmd, %region_2.5_spmd} | conditional | flops 99241728 | bytes 5755680 | solution.py:77
  343.3 3.5 fusion.4
  350.9 7.2 %conditional.3 = (bf16[1,1,384,128]{3,2,1,0:T(8,128)(2,1)S(1)}, f32[1,1,384]{2,1,0:T(1,128)S(1)}) conditional(s32[]{:T(128)} %convert_element_type.99, () %tuple.52, (s32[]{:T(128)}, s32[]{:T(128)}, bf16[32,384,1,128]{3,1,2,0:T(8,128)(2,1)}, s32[]{:T(128)}, bf16[384,1,128]{2,0,1:T(8,128)(2,1)S(1)}, /*index=5*/bf16[32,384,1]{1,0,2:T(8,128)(2,1)S(1)}, ...), branch_computations={%region_1.1_spmd, %region_2.5_spmd} | conditional | flops 99241728 | bytes 5755680 | solution.py:77
  352.4 3.5 fusion.4
  360.0 7.2 %conditional.3 = (bf16[1,1,384,128]{3,2,1,0:T(8,128)(2,1)S(1)}, f32[1,1,384]{2,1,0:T(1,128)S(1)}) conditional(s32[]{:T(128)} %convert_element_type.99, () %tuple.52, (s32[]{:T(128)}, s32[]{:T(128)}, bf16[32,384,1,128]{3,1,2,0:T(8,128)(2,1)}, s32[]{:T(128)}, bf16[384,1,128]{2,0,1:T(8,128)(2,1)S(1)}, /*index=5*/bf16[32,384,1]{1,0,2:T(8,128)(2,1)S(1)}, ...), branch_computations={%region_1.1_spmd, %region_2.5_spmd} | conditional | flops 99241728 | bytes 5755680 | solution.py:77
  361.6 3.5 fusion.4
  369.1 7.2 %conditional.3 = (bf16[1,1,384,128]{3,2,1,0:T(8,128)(2,1)S(1)}, f32[1,1,384]{2,1,0:T(1,128)S(1)}) conditional(s32[]{:T(128)} %convert_element_type.99, () %tuple.52, (s32[]{:T(128)}, s32[]{:T(128)}, bf16[32,384,1,128]{3,1,2,0:T(8,128)(2,1)}, s32[]{:T(128)}, bf16[384,1,128]{2,0,1:T(8,128)(2,1)S(1)}, /*index=5*/bf16[32,384,1]{1,0,2:T(8,128)(2,1)S(1)}, ...), branch_computations={%region_1.1_spmd, %region_2.5_spmd} | conditional | flops 99241728 | bytes 5755680 | solution.py:77
  370.7 3.5 fusion.4
  378.2 7.2 %conditional.3 = (bf16[1,1,384,128]{3,2,1,0:T(8,128)(2,1)S(1)}, f32[1,1,384]{2,1,0:T(1,128)S(1)}) conditional(s32[]{:T(128)} %convert_element_type.99, () %tuple.52, (s32[]{:T(128)}, s32[]{:T(128)}, bf16[32,384,1,128]{3,1,2,0:T(8,128)(2,1)}, s32[]{:T(128)}, bf16[384,1,128]{2,0,1:T(8,128)(2,1)S(1)}, /*index=5*/bf16[32,384,1]{1,0,2:T(8,128)(2,1)S(1)}, ...), branch_computations={%region_1.1_spmd, %region_2.5_spmd} | conditional | flops 99241728 | bytes 5755680 | solution.py:77
  379.8 3.5 fusion.4
  387.4 7.2 %conditional.3 = (bf16[1,1,384,128]{3,2,1,0:T(8,128)(2,1)S(1)}, f32[1,1,384]{2,1,0:T(1,128)S(1)}) conditional(s32[]{:T(128)} %convert_element_type.99, () %tuple.52, (s32[]{:T(128)}, s32[]{:T(128)}, bf16[32,384,1,128]{3,1,2,0:T(8,128)(2,1)}, s32[]{:T(128)}, bf16[384,1,128]{2,0,1:T(8,128)(2,1)S(1)}, /*index=5*/bf16[32,384,1]{1,0,2:T(8,128)(2,1)S(1)}, ...), branch_computations={%region_1.1_spmd, %region_2.5_spmd} | conditional | flops 99241728 | bytes 5755680 | solution.py:77
  388.9 3.5 fusion.4
  396.5 7.2 %conditional.3 = (bf16[1,1,384,128]{3,2,1,0:T(8,128)(2,1)S(1)}, f32[1,1,384]{2,1,0:T(1,128)S(1)}) conditional(s32[]{:T(128)} %convert_element_type.99, () %tuple.52, (s32[]{:T(128)}, s32[]{:T(128)}, bf16[32,384,1,128]{3,1,2,0:T(8,128)(2,1)}, s32[]{:T(128)}, bf16[384,1,128]{2,0,1:T(8,128)(2,1)S(1)}, /*index=5*/bf16[32,384,1]{1,0,2:T(8,128)(2,1)S(1)}, ...), branch_computations={%region_1.1_spmd, %region_2.5_spmd} | conditional | flops 99241728 | bytes 5755680 | solution.py:77
  398.1 3.5 fusion.4
  405.6 7.2 %conditional.3 = (bf16[1,1,384,128]{3,2,1,0:T(8,128)(2,1)S(1)}, f32[1,1,384]{2,1,0:T(1,128)S(1)}) conditional(s32[]{:T(128)} %convert_element_type.99, () %tuple.52, (s32[]{:T(128)}, s32[]{:T(128)}, bf16[32,384,1,128]{3,1,2,0:T(8,128)(2,1)}, s32[]{:T(128)}, bf16[384,1,128]{2,0,1:T(8,128)(2,1)S(1)}, /*index=5*/bf16[32,384,1]{1,0,2:T(8,128)(2,1)S(1)}, ...), branch_computations={%region_1.1_spmd, %region_2.5_spmd} | conditional | flops 99241728 | bytes 5755680 | solution.py:77
  407.2 3.5 fusion.4
  414.8 7.2 %conditional.3 = (bf16[1,1,384,128]{3,2,1,0:T(8,128)(2,1)S(1)}, f32[1,1,384]{2,1,0:T(1,128)S(1)}) conditional(s32[]{:T(128)} %convert_element_type.99, () %tuple.52, (s32[]{:T(128)}, s32[]{:T(128)}, bf16[32,384,1,128]{3,1,2,0:T(8,128)(2,1)}, s32[]{:T(128)}, bf16[384,1,128]{2,0,1:T(8,128)(2,1)S(1)}, /*index=5*/bf16[32,384,1]{1,0,2:T(8,128)(2,1)S(1)}, ...), branch_computations={%region_1.1_spmd, %region_2.5_spmd} | conditional | flops 99241728 | bytes 5755680 | solution.py:77
  423.9 7.2 %conditional.3 = (bf16[1,1,384,128]{3,2,1,0:T(8,128)(2,1)S(1)}, f32[1,1,384]{2,1,0:T(1,128)S(1)}) conditional(s32[]{:T(128)} %convert_element_type.99, () %tuple.52, (s32[]{:T(128)}, s32[]{:T(128)}, bf16[32,384,1,128]{3,1,2,0:T(8,128)(2,1)}, s32[]{:T(128)}, bf16[384,1,128]{2,0,1:T(8,128)(2,1)S(1)}, /*index=5*/bf16[32,384,1]{1,0,2:T(8,128)(2,1)S(1)}, ...), branch_computations={%region_1.1_spmd, %region_2.5_spmd} | conditional | flops 99241728 | bytes 5755680 | solution.py:77
  433.0 7.2 %conditional.3 = (bf16[1,1,384,128]{3,2,1,0:T(8,128)(2,1)S(1)}, f32[1,1,384]{2,1,0:T(1,128)S(1)}) conditional(s32[]{:T(128)} %convert_element_type.99, () %tuple.52, (s32[]{:T(128)}, s32[]{:T(128)}, bf16[32,384,1,128]{3,1,2,0:T(8,128)(2,1)}, s32[]{:T(128)}, bf16[384,1,128]{2,0,1:T(8,128)(2,1)S(1)}, /*index=5*/bf16[32,384,1]{1,0,2:T(8,128)(2,1)S(1)}, ...), branch_computations={%region_1.1_spmd, %region_2.5_spmd} | conditional | flops 99241728 | bytes 5755680 | solution.py:77
  442.1 7.2 %conditional.3 = (bf16[1,1,384,128]{3,2,1,0:T(8,128)(2,1)S(1)}, f32[1,1,384]{2,1,0:T(1,128)S(1)}) conditional(s32[]{:T(128)} %convert_element_type.99, () %tuple.52, (s32[]{:T(128)}, s32[]{:T(128)}, bf16[32,384,1,128]{3,1,2,0:T(8,128)(2,1)}, s32[]{:T(128)}, bf16[384,1,128]{2,0,1:T(8,128)(2,1)S(1)}, /*index=5*/bf16[32,384,1]{1,0,2:T(8,128)(2,1)S(1)}, ...), branch_computations={%region_1.1_spmd, %region_2.5_spmd} | conditional | flops 99241728 | bytes 5755680 | solution.py:77
  451.2 7.2 %conditional.3 = (bf16[1,1,384,128]{3,2,1,0:T(8,128)(2,1)S(1)}, f32[1,1,384]{2,1,0:T(1,128)S(1)}) conditional(s32[]{:T(128)} %convert_element_type.99, () %tuple.52, (s32[]{:T(128)}, s32[]{:T(128)}, bf16[32,384,1,128]{3,1,2,0:T(8,128)(2,1)}, s32[]{:T(128)}, bf16[384,1,128]{2,0,1:T(8,128)(2,1)S(1)}, /*index=5*/bf16[32,384,1]{1,0,2:T(8,128)(2,1)S(1)}, ...), branch_computations={%region_1.1_spmd, %region_2.5_spmd} | conditional | flops 99241728 | bytes 5755680 | solution.py:77
  460.4 7.2 %conditional.3 = (bf16[1,1,384,128]{3,2,1,0:T(8,128)(2,1)S(1)}, f32[1,1,384]{2,1,0:T(1,128)S(1)}) conditional(s32[]{:T(128)} %convert_element_type.99, () %tuple.52, (s32[]{:T(128)}, s32[]{:T(128)}, bf16[32,384,1,128]{3,1,2,0:T(8,128)(2,1)}, s32[]{:T(128)}, bf16[384,1,128]{2,0,1:T(8,128)(2,1)S(1)}, /*index=5*/bf16[32,384,1]{1,0,2:T(8,128)(2,1)S(1)}, ...), branch_computations={%region_1.1_spmd, %region_2.5_spmd} | conditional | flops 99241728 | bytes 5755680 | solution.py:77
  469.5 7.2 %conditional.3 = (bf16[1,1,384,128]{3,2,1,0:T(8,128)(2,1)S(1)}, f32[1,1,384]{2,1,0:T(1,128)S(1)}) conditional(s32[]{:T(128)} %convert_element_type.99, () %tuple.52, (s32[]{:T(128)}, s32[]{:T(128)}, bf16[32,384,1,128]{3,1,2,0:T(8,128)(2,1)}, s32[]{:T(128)}, bf16[384,1,128]{2,0,1:T(8,128)(2,1)S(1)}, /*index=5*/bf16[32,384,1]{1,0,2:T(8,128)(2,1)S(1)}, ...), branch_computations={%region_1.1_spmd, %region_2.5_spmd} | conditional | flops 99241728 | bytes 5755680 | solution.py:77
  478.6 7.2 %conditional.3 = (bf16[1,1,384,128]{3,2,1,0:T(8,128)(2,1)S(1)}, f32[1,1,384]{2,1,0:T(1,128)S(1)}) conditional(s32[]{:T(128)} %convert_element_type.99, () %tuple.52, (s32[]{:T(128)}, s32[]{:T(128)}, bf16[32,384,1,128]{3,1,2,0:T(8,128)(2,1)}, s32[]{:T(128)}, bf16[384,1,128]{2,0,1:T(8,128)(2,1)S(1)}, /*index=5*/bf16[32,384,1]{1,0,2:T(8,128)(2,1)S(1)}, ...), branch_computations={%region_1.1_spmd, %region_2.5_spmd} | conditional | flops 99241728 | bytes 5755680 | solution.py:77
  487.7 7.2 %conditional.3 = (bf16[1,1,384,128]{3,2,1,0:T(8,128)(2,1)S(1)}, f32[1,1,384]{2,1,0:T(1,128)S(1)}) conditional(s32[]{:T(128)} %convert_element_type.99, () %tuple.52, (s32[]{:T(128)}, s32[]{:T(128)}, bf16[32,384,1,128]{3,1,2,0:T(8,128)(2,1)}, s32[]{:T(128)}, bf16[384,1,128]{2,0,1:T(8,128)(2,1)S(1)}, /*index=5*/bf16[32,384,1]{1,0,2:T(8,128)(2,1)S(1)}, ...), branch_computations={%region_1.1_spmd, %region_2.5_spmd} | conditional | flops 99241728 | bytes 5755680 | solution.py:77
  496.0 3.8 fusion.20
  500.5 5.2 %gather_fusion.1 = bf16[256,2048]{1,0:T(8,128)(2,1)} fusion(bf16[512,2048]{1,0:T(8,128)(2,1)} %bitcast.46, s32[1024]{0:T(1024)S(1)} %pad_clamp_fusion), kind=kCustom, calls=%fused_computation.1 | custom fusion | bytes 2098176 | tf_op jit(solution)/shard_map/gather | solution.py:136
  508.3 3.9 multiply_reduce_fusion
  (517 shorter events, 215.4 us)
Async XLA Ops:
  7.2 68.2 %copy-start = (bf16[1,224,2048]{2,1,0:T(8,128)(2,1)S(1)}, bf16[1,224,2048]{2,1,0:T(8,128)(2,1)}, u32[]{:S(2)}) copy-start(bf16[1,224,2048]{2,1,0:T(8,128)(2,1)} %param.23) | copy-start | bytes 2752516
  7.2 196.4 %all-gather.3.cloned.1.call-start = ((), (), s32[]{:S(2)}) async-start(), calls=%async_computation.4 | async-start | bytes 3244032 | tf_op jit(solution)/shard_map/all_gather | solution.py:44
  17.3 55.3 %all-to-all-start = ((bf16[32,1,16,2048]{3,2,1,0:T(8,128)(2,1)}), bf16[32,1,16,2048]{3,2,1,0:T(8,128)(2,1)S(1)}, u32[]{:S(2)}, u32[]{:S(2)}) async-start(bf16[32,1,16,2048]{3,2,1,0:T(8,128)(2,1)} %bitcast.23), calls=%async_computation | async-start | bytes 4194304 | tf_op jit(solution)/shard_map/all_to_all | solution.py:121
  23.9 179.8 %all-gather.5.cloned.1.call-start = ((), (), s32[]{:S(2)}) async-start(), calls=%async_computation.5 | async-start | bytes 3244032 | tf_op jit(solution)/shard_map/all_gather | solution.py:45
  72.6 2.0 copy-start.3
  135.1 13.1 %copy-start.1 = (bf16[384,1]{0,1:T(2,128)(2,1)S(1)}, bf16[384,1]{0,1:T(2,128)(2,1)}, u32[]{:S(2)}) copy-start(bf16[384,1]{0,1:T(2,128)(2,1)} %param.18) | copy-start | bytes 2308
  135.1 50.4 %copy-start.2 = (f32[128,2]{0,1:T(2,128)S(1)}, f32[128,2]{0,1:T(2,128)}, u32[]{:S(2)}) copy-start(f32[128,2]{0,1:T(2,128)} %param.25) | copy-start | bytes 3076
  138.3 47.3 %all-to-all-start.2 = ((bf16[32,2,1024]{2,1,0:T(2,128)(2,1)}), bf16[32,2,1024]{2,1,0:T(2,128)(2,1)S(1)}, u32[]{:S(2)}, u32[]{:S(2)}) async-start(bf16[32,2,1024]{2,1,0:T(2,128)(2,1)} %reshape.303), calls=%async_computation.2 | async-start | bytes 262144 | tf_op jit(solution)/shard_map/all_to_all | solution.py:132
  187.4 16.2 %copy-start.4 = (bf16[384,128]{1,0:T(8,128)(2,1)S(1)}, bf16[384,128]{1,0:T(8,128)(2,1)}, u32[]{:S(2)}) copy-start(bf16[384,128]{1,0:T(8,128)(2,1)} %param.15) | copy-start | bytes 294916
  187.4 313.0 %all-to-all-start.3 = ((bf16[16,1,32,1,2048]{4,2,3,1,0:T(8,128)(2,1)}), bf16[16,1,32,1,2048]{4,2,3,1,0:T(8,128)(2,1)}, u32[]{:S(2)}, u32[]{:S(2)}) async-start(bf16[16,1,32,1,2048]{4,2,3,1,0:T(8,128)(2,1)} %broadcast_in_dim.46), calls=%async_computation.3 | async-start | bytes 4194304 | tf_op jit(solution)/shard_map/all_to_all | solution.py:28
Sparse Core Ops, SparseCore 0:
  11.1 85.3 all-gather.2
  99.7 81.6 all-gather.4
where the time goes:
time: 522 us; the launch traced here: 519 us
  other arithmetic  151 us (29%)
  blocking collectives  96.1 us (18%)
  matrix products  92.5 us (18%)
  local copies, waits for them, and re-layouts  59.5 us (11%)
  waiting for transfers between devices  49.4 us (9%)
  starting transfers between devices  32.6 us (6%)
  loops' own time  23.3 us (4%)
  between operations  14.3 us (3%)
    another operation x66, other arithmetic  113 us
    all_to_all x1, blocking collectives, sent_and_summed(): lax.all_to_all(parts, axis, split_axis=0, concat_axis=0, tiled=True)  58.9 us
    all_to_all x1, waiting for transfers between devices, routed_experts(): lax.all_to_all(outgoing, 'ep', split_axis=0, concat_axis=0, tiled=True)  48 us
    dot_general x32, matrix products, compute_block(): jnp.einsum('qhd,khd->hqk', query_heads, key_here, preferred_element_type=...  47.9 us
    dot_general x32, matrix products, compute_block(): jnp.einsum('hqk,khd->hqd', local, value_here, preferred_element_type=jnp....  37.3 us
    all_gather x1, blocking collectives, stick_mixer(): offset_piece = lax.all_gather(key_offset, 'ep', axis=0, tiled=True)  37.1 us
    convert_element_type x32, other arithmetic, compute_block(): jnp.where(strict, jnp.exp(jax.nn.log_sigmoid(logits) + within), 0.0)  27.7 us
    another operation x1, loops' own time, stick_mixer(): lax.map(one_block, (key_split, value_split, offset_split, jnp.arange(bloc...  21.2 us
  transfers between devices with their start and end apart: 5, of which 1 were waited for; matrix products, arithmetic and copies ran while one was open for 56% of the time, Pallas kernels for 0%

commit v1 on v0

v1 whole, which is shorter than its diff:
```python
import functools

import jax
import jax.numpy as jnp
from jax import lax
from jax.experimental import pallas as pl
from jax.experimental.pallas import tpu as pltpu
from jax.sharding import Mesh
from jax.sharding import PartitionSpec as P

EPSILON = 1e-06
LOG2E = 1.4426950408889634
F32 = jnp.float32
BF16 = jnp.bfloat16
Z, X, Y, CORE = 8, 4, 8, 2
EP = ("z", "x")
TP = ("y", "core")
LANES = 128


def dot(a, b, dims=((1,), (0,))):
    return lax.dot_general(a, b, (dims, ((), ())), preferred_element_type=F32)


def block_kernel(depth, width, len_, hd, at_ref, q_ref, kvo_ref, sums_ref, totals_ref, tri_ref, tot_ref):
    z, x = at_ref[0], at_ref[1]
    c = hd**-0.5 * LOG2E
    rows_i = lax.broadcasted_iota(jnp.int32, (len_, len_), 0)
    cols_i = lax.broadcasted_iota(jnp.int32, (len_, len_), 1)
    tri_ref[...] = jnp.where(rows_i > cols_i, -1.0, 0.0).astype(BF16)
    tot_ref[...] = jnp.zeros_like(tot_ref)
    lane = lax.broadcasted_iota(jnp.int32, (len_, LANES), 1)
    n_off = len_ // LANES

    def pair(at, a, masked):
        rows = pl.ds(pl.multiple_of(a * len_, len_), len_)
        q = q_ref[rows, :]
        k = kvo_ref[at, pl.ds(0, len_), :]
        v = kvo_ref[at, pl.ds(len_, len_), :]
        o = kvo_ref[at, pl.ds(2 * len_, 16), :].astype(F32)
        off = jnp.concatenate([o[i : i + 1, :] for i in range(n_off)], axis=1) * LOG2E
        u = dot(q, k, ((1,), (1,))) * c + off
        sp = kept = jnp.maximum(u, 0.0) + jnp.log2(1.0 + jnp.exp2(-jnp.abs(u)))
        if masked:
            strict = cols_i < rows_i
            kept = jnp.where(strict, sp, 0.0)
        w = dot(kept.astype(BF16), tri_ref[...])
        p = jnp.exp2(u - sp + w)
        if masked:
            p = jnp.where(strict, p, 0.0)
        sums_ref[at, rows, :] = dot(p.astype(BF16), v).astype(sums_ref.dtype)
        total = jnp.broadcast_to(w[:, 0:1] - kept[:, 0:1], (len_, LANES))
        tot_ref[rows, :] = jnp.where(lane == at, total, tot_ref[rows, :])

    def full(i, carry):
        early = i < width * z
        pair(
            jnp.where(early, i // width, z),
            jnp.where(early, i % width, x + 1 + i - width * z),
            False,
        )
        return carry

    lax.fori_loop(0, width * z + width - 1 - x, full, 0)
    pair(z, x, True)

    def clear(i, carry):
        early = i < x
        at = jnp.where(early, z, z + 1 + (i - x) // width)
        a = jnp.where(early, i, (i - x) % width)
        rows = pl.ds(pl.multiple_of(a * len_, len_), len_)
        sums_ref[at, rows, :] = jnp.zeros((len_, hd), sums_ref.dtype)
        return carry

    lax.fori_loop(0, x + width * (depth - 1 - z), clear, 0)
    for r in range(0, width * len_, LANES):
        totals_ref[:, r : r + LANES] = tot_ref[r : r + LANES, :].T[:depth, :]


def join_kernel(depth, width, at_ref, totals_ref, sums_ref, out_ref, scale_ref):
    z, x = at_ref[0], at_ref[1]
    later = jnp.zeros((1, totals_ref.shape[2]), F32)
    scale_ref[...] = jnp.zeros_like(scale_ref)
    for at in reversed(range(depth)):
        mine = later
        for other in range(width):
            t = totals_ref[other, at : at + 1, :]
            mine = mine + jnp.where(other > x, t, 0.0)
            later = later + t
        scale_ref[at : at + 1, :] = jnp.exp2(mine)
    for r in range(0, totals_ref.shape[2], LANES):
        cols = scale_ref[:, r : r + LANES].T
        acc = jnp.zeros((LANES, out_ref.shape[1]), F32)
        for at in range(depth):
            acc = acc + sums_ref[at, r : r + LANES, :].astype(F32) * cols[:, at : at + 1]
        out_ref[r : r + LANES, :] = acc.astype(out_ref.dtype)


def vmem(n):
    return [pl.BlockSpec(memory_space=pltpu.VMEM)] * n


SMEM = pl.BlockSpec(memory_space=pltpu.SMEM)


def stick_mixer(queries, keys, values, key_offset):
    depth, width = lax.axis_size("z"), lax.axis_size("x")
    len_, hd = queries.shape
    at = jnp.stack([lax.axis_index("z"), lax.axis_index("x")]).astype(jnp.int32)
    off = jnp.pad(key_offset.reshape(-1, LANES), ((0, 16 - len_ // LANES), (0, 0)))
    kvo = jnp.concatenate([keys, values, off], axis=0)
    kvo = lax.all_gather(kvo, "z")
    q = lax.all_gather(queries, "x", tiled=True)
    n = width * len_
    sums, totals = pl.pallas_call(
        functools.partial(block_kernel, depth, width, len_, hd),
        out_shape=(
            jax.ShapeDtypeStruct((depth, n, hd), BF16),
            jax.ShapeDtypeStruct((depth, n), F32),
        ),
        in_specs=[SMEM] + vmem(2),
        out_specs=tuple(vmem(2)),
        scratch_shapes=[pltpu.VMEM((len_, len_), BF16), pltpu.VMEM((n, LANES), F32)],
        compiler_params=pltpu.CompilerParams(vmem_limit_bytes=40 << 20),
        cost_estimate=pl.CostEstimate(
            flops=depth * n * len_ * (2 * hd + 2 * len_ + 2 * hd),
            transcendentals=3 * depth * n * len_,
            bytes_accessed=depth * n * hd * 2 + kvo.size * 2 + q.size * 2,
        ),
        name="stick_blocks",
    )(at, q, kvo)
    totals = lax.all_gather(totals, "x")
    part = pl.pallas_call(
        functools.partial(join_kernel, depth, width),
        out_shape=jax.ShapeDtypeStruct((n, hd), BF16),
        in_specs=[SMEM] + vmem(2),
        out_specs=vmem(1)[0],
        scratch_shapes=[pltpu.VMEM((LANES, n), F32)],
        cost_estimate=pl.CostEstimate(
            flops=2 * depth * n * hd, transcendentals=depth * n, bytes_accessed=depth * n * hd * 2
        ),
        name="stick_join",
    )(at, totals, sums)
    parts = lax.all_to_all(part.reshape(width, len_, hd), "x", 0, 0, tiled=True)
    return parts.astype(F32).sum(axis=0).astype(BF16)


def dispatch_kernel(cap, at_ref, rows_ref, gain_ref, ids_ref, wts_ref, out_ref, hi_ref, lo_ref):
    tok = rows_ref.shape[0]
    width = out_ref.shape[1]
    slots = out_ref.shape[0]
    rows = rows_ref[...].astype(F32)
    rms = lax.rsqrt(jnp.mean(rows * rows, axis=1, keepdims=True) + EPSILON)
    own = pl.ds(pl.multiple_of(at_ref[0] * width, width), width)
    normed = (rows_ref[:, own].astype(F32) * rms * gain_ref[:, own]).astype(BF16)
    first, second = ids_ref[:, 0:1], ids_ref[:, 1:2]
    lane = lax.broadcasted_iota(jnp.int32, (tok, LANES), 1)
    chosen = jnp.where((first == lane) | (second == lane), 1.0, 0.0).astype(BF16)
    before = lax.broadcasted_iota(jnp.int32, (tok, tok), 1) < lax.broadcasted_iota(
        jnp.int32, (tok, tok), 0
    )
    rank = dot(jnp.where(before, 1.0, 0.0).astype(BF16), chosen).astype(BF16)
    spread = (
        lax.broadcasted_iota(jnp.int32, (LANES, slots), 1) // cap
        == lax.broadcasted_iota(jnp.int32, (LANES, slots), 0)
    )
    spread = jnp.where(spread, 1.0, 0.0).astype(BF16)
    slot = lax.broadcasted_iota(jnp.int32, (tok, slots), 1)
    taken = (dot(chosen, spread) > 0.5) & (dot(rank, spread) == (slot % cap).astype(F32))
    pick = jnp.where(taken, 1.0, 0.0).astype(BF16)
    out_ref[...] = dot(pick, normed, ((0,), (0,))).astype(BF16)
    weight = jnp.where(slot // cap == first, wts_ref[:, 0:1], wts_ref[:, 1:2])
    weight = jnp.where(taken, weight, 0.0)
    hi = weight.astype(BF16)
    hi_ref[...] = hi
    lo_ref[...] = (weight - hi.astype(F32)).astype(BF16)


def routed_experts(rows, gain, gate_w, up_w, down_w, expert_ids, route_weights):
    experts = lax.axis_size(EP)
    groups = lax.axis_size(TP)
    tok, width = rows.shape
    own = width // groups
    cap = 2 * expert_ids.shape[1] * tok // experts
    slots = experts * cap
    at = jnp.stack([lax.axis_index(TP)]).astype(jnp.int32)
    outgoing, hi, lo = pl.pallas_call(
        functools.partial(dispatch_kernel, cap),
        out_shape=(
            jax.ShapeDtypeStruct((slots, own), BF16),
            jax.ShapeDtypeStruct((tok, slots), BF16),
            jax.ShapeDtypeStruct((tok, slots), BF16),
        ),
        in_specs=[SMEM] + vmem(4),
        out_specs=tuple(vmem(3)),
        name="dispatch",
    )(at, rows, gain.reshape(1, -1), expert_ids, route_weights)
    arrived = lax.all_to_all(outgoing.reshape(experts, cap, own), EP, 0, 0, tiled=True)
    arrived = lax.all_gather(arrived.reshape(slots, own), TP)
    gate = jnp.einsum(
        "jsc,jcf->sf", arrived, gate_w.reshape(groups, own, -1), preferred_element_type=F32
    )
    up = jnp.einsum(
        "jsc,jcf->sf", arrived, up_w.reshape(groups, own, -1), preferred_element_type=F32
    )
    hidden = (jax.nn.silu(gate) * up).astype(BF16)
    part = jnp.einsum(
        "sf,fjc->jsc", hidden, down_w.reshape(-1, groups, own), preferred_element_type=F32
    ).astype(BF16)
    share = lax.psum_scatter(part, TP, scatter_dimension=0, tiled=True)
    back = lax.all_to_all(share.reshape(experts, cap, own), EP, 0, 0, tiled=True)
    back = back.reshape(slots, own)
    mixed = (dot(hi, back) + dot(lo, back)).astype(BF16)
    return lax.all_gather(mixed, TP, axis=1, tiled=True)


def body(
    queries, keys, values, key_offset, rows, gain, gate_w, up_w, down_w, expert_ids, route_weights
):
    mixed = routed_experts(rows, gain, gate_w, up_w, down_w, expert_ids, route_weights)
    attended = stick_mixer(queries, keys, values, key_offset)
    return (attended, mixed)


def solution(mesh):
    fine = Mesh(mesh.devices.reshape(Z, X, Y, CORE), ("z", "x", "y", "core"))
    return jax.shard_map(
        body,
        mesh=fine,
        in_specs=(
            P(EP, TP),
            P(EP, TP),
            P(EP, TP),
            P(EP, TP),
            P(EP, None),
            P(),
            P(EP, None, TP),
            P(EP, None, TP),
            P(EP, TP, None),
            P(EP, None),
            P(EP, None),
        ),
        out_specs=(P(EP, TP), P(EP, None)),
        check_vma=False,
    )
```

time: 522 us -> 228 us (0.44)
  the two profiles are of different devices: /device:TPU:463 before, /device:TPU:1 now
where the time goes in v1:
time: 228 us; the launch traced here: 227 us
  waiting for transfers between devices  98.4 us (43%)
  blocking collectives  74.4 us (33%)
  between operations  13.9 us (6%)
  Pallas kernels  12.1 us (5%)
  local copies, waits for them, and re-layouts  9.09 us (4%)
  starting transfers between devices  8.92 us (4%)
  matrix products  7.43 us (3%)
  other arithmetic  3.19 us (1%)
    all_gather x1, waiting for transfers between devices, routed_experts(): arrived = lax.all_gather(arrived.reshape(slots, own), TP)  34.7 us
    reduce_scatter x1, waiting for transfers between devices, routed_experts(): share = lax.psum_scatter(part, TP, scatter_dimension=0, tiled=True)  33.3 us
    all_to_all x1, blocking collectives, routed_experts(): lax.all_to_all(outgoing.reshape(experts, cap, own), EP, 0, 0, tiled=True)  23.2 us
    all_gather x1, waiting for transfers between devices, stick_mixer(): kvo = lax.all_gather(kvo, 'z')  21.7 us
    all_gather x1, blocking collectives, routed_experts(): return lax.all_gather(mixed, TP, axis=1, tiled=True)  21 us
    all_gather x1, blocking collectives, stick_mixer(): q = lax.all_gather(queries, 'x', tiled=True)  10.7 us
    all_gather x1, blocking collectives, stick_mixer(): totals = lax.all_gather(totals, 'x')  9.96 us
    all_to_all x1, blocking collectives, stick_mixer(): parts = lax.all_to_all(part.reshape(width, len_, hd), 'x', 0, 0, tiled=True)  9.66 us
  transfers between devices with their start and end apart: 4, of which 4 were waited for; matrix products, arithmetic and copies ran while one was open for 5% of the time, Pallas kernels for 4%

profile of v1, /device:TPU:1, one launch (start us, length us, event | category | flops | bytes accessed | tf_op | source)
XLA Modules:
  0.0 227.4 jit_solution(17921809803237896378)
XLA Ops:
  7.2 0.0 copy-start.3
  7.2 0.0 copy-start.4
  7.2 0.0 all-gather.5.cloned.1.call-start
  7.2 1.5 copy.17.ids_ref
  8.8 1.4 copy.18.wts_ref
  10.2 2.4 %dispatch.1 = (bf16[512,128]{1,0:T(8,128)(2,1)}, bf16[128,512]{1,0:T(8,128)(2,1)}, bf16[128,512]{1,0:T(8,128)(2,1)}) custom-call(s32[1]{0:T(128)} %bitcast.5.at_ref, bf16[128,2048]{1,0:T(8,128)(2,1)} %rows_ref.1, f32[1,2048]{1,0:T(1,128)} %bitcast.63, s32[128,2]{1,0:T(8,128)} %copy.17.ids_ref, f32[128,2]{1,0:T(8,128)} %copy.18.wts_ref), custom_call_target="tpu_custom_call" | custom-call | tf_op jit(solution)/shard_map/dispatch/pallas_call | solution.py:187
  12.6 23.2 %all_to_all.15 = bf16[32,16,128]{2,1,0:T(8,128)(2,1)} all-to-all(bf16[32,16,128]{2,1,0:T(8,128)(2,1)} %bitcast.62), channel_id=1, replica_groups=mesh['z'=8,'x'=4,'y'=8,'core'=2] {'z','x'}, dimensions={0} | all-to-all | bytes 262144 | tf_op jit(solution)/shard_map/all_to_all | solution.py:198
  35.7 0.0 all-gather.5.cloned.1.call-update
  35.8 0.0 all-gather.7.cloned.1.call-start
  35.8 0.7 reduce.1
  36.5 0.0 copy-start.5
  36.5 1.7 fusion.15
  38.2 0.0 all-gather.7.cloned.1.call-update
  38.2 0.0 reduce-scatter.2.cloned.1.call-start
  38.3 0.0 copy-done.3
  38.3 1.1 copy.22
  39.4 0.0 copy-done.4
  39.4 0.2 copy.23
  39.6 0.0 copy-done.5
  39.6 0.2 copy.24
  39.8 34.7 %all-gather.5.cloned.1.call-done = bf16[16,512,128]{2,1,0:T(8,128)(2,1)} async-done(((bf16[1,512,128]{2,1,0:T(8,128)(2,1)}), bf16[16,512,128]{2,1,0:T(8,128)(2,1)}) %all-gather.5.cloned.1.call-update) | async-done | bytes 2097168 | tf_op jit(solution)/shard_map/all_gather | solution.py:199
  74.5 2.6 %convolution_bitcast_fusion.1 = f32[512,224]{0,1:T(8,128)S(1)} fusion(bf16[16,512,128]{2,1,0:T(8,128)(2,1)} %all-gather.5.cloned.1.call-done, bf16[16,128,224]{1,0,2:T(8,128)(2,1)} %bitcast.58), kind=kOutput, calls=%fused_computation.3 | convolution fusion | flops 469762048 | bytes 3473408 | tf_op jit(solution)/shard_map/jsc,jcf->sf/dot_general | solution.py:200
  77.1 4.5 %convert_bitcast_fusion = bf16[16,512,128]{2,1,0:T(8,128)(2,1)} fusion(bf16[16,512,128]{2,1,0:T(8,128)(2,1)} %all-gather.5.cloned.1.call-done, bf16[16,128,224]{1,0,2:T(8,128)(2,1)S(1)} %bitcast.56, bf16[224,16,128]{2,1,0:T(8,128)(2,1)S(1)} %bitcast.57, f32[512,224]{0,1:T(8,128)S(1)} %convolution_bitcast_fusion.1), kind=kOutput, calls=%fused_computation | convolution fusion | flops 941260800 | bytes 6488064 | tf_op jit(solution)/shard_map/sf,fjc->jsc/dot_general | solution.py:207
  81.6 0.0 copy-start.8
  81.6 0.0 reduce-scatter.2.cloned.1.call-update
  81.6 0.1 pad_add_fusion.at_ref
  81.7 0.8 copy-done.8
  82.5 0.0 copy-start.1
  82.5 10.7 %all_gather.21.q_ref = bf16[1536,128]{1,0:T(8,128)(2,1)S(1)} all-gather(bf16[384,128]{1,0:T(8,128)(2,1)S(1)} %copy-done.8), channel_id=1, replica_groups=mesh['z'=8,'x'=4,'y'=8,'core'=2] {'x'}, dimensions={0}, use_global_device_ids=true | all-gather | bytes 491520 | tf_op jit(solution)/shard_map/all_gather | solution.py:113
  93.1 21.7 %all-gather.7.cloned.1.call-done = bf16[6272,128]{1,0:T(8,128)(2,1)} async-done(((bf16[784,128]{1,0:T(8,128)(2,1)}), bf16[6272,128]{1,0:T(8,128)(2,1)}) %all-gather.7.cloned.1.call-update) | async-done | bytes 1605648 | tf_op jit(solution)/shard_map/all_gather | solution.py:112
  114.9 0.0 copy-start.2
  114.9 1.4 copy-done.2
  116.3 4.4 %stick_blocks.1 = (bf16[8,1536,128]{2,1,0:T(8,128)(2,1)S(1)}, f32[8,1536]{1,0:T(8,128)S(1)}) custom-call(s32[2]{0:T(128)S(1)} %pad_add_fusion.at_ref, bf16[1536,128]{1,0:T(8,128)(2,1)S(1)} %all_gather.21.q_ref, bf16[8,784,128]{2,1,0:T(8,128)(2,1)S(1)} %bitcast.49), custom_call_target="tpu_custom_call" | custom-call | flops 6039797760 | bytes 5144576 | tf_op jit(solution)/shard_map/stick_blocks/pallas_call | solution.py:115
  120.7 0.0 copy-done.1
  120.7 0.0 copy-start
  120.7 1.6 copy-done
  122.4 10.0 %all-gather.1 = f32[32,1536]{1,0:T(8,128)} all-gather(f32[8,1536]{1,0:T(8,128)S(1)} %get-tuple-element.7), channel_id=3, replica_groups=mesh['z'=8,'x'=4,'y'=8,'core'=2] {'x'}, dimensions={0}, use_global_device_ids=true | all-gather | bytes 245760 | tf_op jit(solution)/shard_map/all_gather | solution.py:132
  132.3 0.0 copy-start.6
  132.3 0.0 copy-start.7
  132.3 5.2 %stick_join.1 = bf16[1536,128]{1,0:T(8,128)(2,1)} custom-call(s32[2]{0:T(128)} %copy-done.1, f32[4,8,1536]{2,1,0:T(8,128)} %bitcast.59, bf16[8,1536,128]{2,1,0:T(8,128)(2,1)} %copy-done), custom_call_target="tpu_custom_call" | custom-call | flops 3145728 | bytes 3145728 | tf_op jit(solution)/shard_map/stick_join/pallas_call | solution.py:133
  137.6 9.7 %all_to_all.16 = bf16[4,384,128]{2,1,0:T(8,128)(2,1)S(1)} all-to-all(bf16[4,384,128]{2,1,0:T(8,128)(2,1)} %bitcast.50), channel_id=1, replica_groups=mesh['z'=8,'x'=4,'y'=8,'core'=2] {'x'}, dimensions={0} | all-to-all | bytes 786432 | tf_op jit(solution)/shard_map/all_to_all | solution.py:144
  147.2 33.3 %reduce-scatter.2.cloned.1.call-done = bf16[1,512,128]{2,1,0:T(8,128)(2,1)} async-done(((bf16[16,512,128]{2,1,0:T(8,128)(2,1)}), bf16[1,512,128]{2,1,0:T(8,128)(2,1)}) %reduce-scatter.2.cloned.1.call-update) | async-done | bytes 131088 | tf_op jit(solution)/shard_map/reduce_scatter | solution.py:210
  180.5 8.8 %all-to-all-start.2 = ((bf16[32,16,128]{2,1,0:T(8,128)(2,1)}), bf16[32,16,128]{2,1,0:T(8,128)(2,1)S(1)}, u32[]{:S(2)}, u32[]{:S(2)}) async-start(bf16[32,16,128]{2,1,0:T(8,128)(2,1)} %bitcast.61), calls=%async_computation.3 | async-start | bytes 262144 | tf_op jit(solution)/shard_map/all_to_all | solution.py:211
  189.3 0.7 reduce_sum.12
  190.1 8.6 %all-to-all-done.2 = bf16[32,16,128]{2,1,0:T(8,128)(2,1)S(1)} async-done(((bf16[32,16,128]{2,1,0:T(8,128)(2,1)}), bf16[32,16,128]{2,1,0:T(8,128)(2,1)S(1)}, u32[]{:S(2)}, u32[]{:S(2)}) %all-to-all-start.2) | async-done | bytes 131104 | tf_op jit(solution)/shard_map/all_to_all | solution.py:211
  198.7 0.0 copy-done.6
  198.7 0.2 fusion.17
  198.9 0.0 copy-done.7
  198.9 0.2 fusion.3
  199.1 21.0 %all_gather.27 = bf16[128,2048]{1,0:T(8,128)(2,1)S(1)} all-gather(bf16[128,128]{1,0:T(8,128)(2,1)S(1)} %fusion.3), channel_id=1, replica_groups=mesh['z'=8,'x'=4,'y'=8,'core'=2] {'y','core'}, dimensions={1}, use_global_device_ids=true | all-gather | bytes 557056 | tf_op jit(solution)/shard_map/all_gather | solution.py:214
  220.0 0.8 copy.33
Async XLA Ops:
  7.2 31.1 %copy-start.3 = (bf16[1,2048,224]{1,2,0:T(8,128)(2,1)S(1)}, bf16[1,2048,224]{1,2,0:T(8,128)(2,1)}, u32[]{:S(2)}) copy-start(bf16[1,2048,224]{1,2,0:T(8,128)(2,1)} %param.17) | copy-start | bytes 2752516
  7.2 32.2 %copy-start.4 = (bf16[1,2048,224]{1,2,0:T(8,128)(2,1)S(1)}, bf16[1,2048,224]{1,2,0:T(8,128)(2,1)}, u32[]{:S(2)}) copy-start(bf16[1,2048,224]{1,2,0:T(8,128)(2,1)} %param.18) | copy-start | bytes 2752516
  7.2 67.3 %all-gather.5.cloned.1.call-start = ((), (), s32[]{:S(2)}) async-start(), calls=%async_computation.4 | async-start | bytes 2228224 | tf_op jit(solution)/shard_map/all_gather | solution.py:199
  35.8 79.1 %all-gather.7.cloned.1.call-start = ((), (), s32[]{:S(2)}) async-start(), calls=%async_computation.6 | async-start | bytes 1806336 | tf_op jit(solution)/shard_map/all_gather | solution.py:112
  36.5 3.1 %copy-start.5 = (bf16[1,224,2048]{2,1,0:T(8,128)(2,1)S(1)}, bf16[1,224,2048]{2,1,0:T(8,128)(2,1)}, u32[]{:S(2)}) copy-start(bf16[1,224,2048]{2,1,0:T(8,128)(2,1)} %param.19) | copy-start | bytes 2752516
  38.2 142.3 %reduce-scatter.2.cloned.1.call-start = ((), (), s32[]{:S(2)}) async-start(), calls=%async_computation.5 | async-start | bytes 2228224 | tf_op jit(solution)/shard_map/reduce_scatter | solution.py:210
  81.6 0.9 copy-start.8
  82.5 38.2 %copy-start.1 = (s32[2]{0:T(128)}, s32[2]{0:T(128)S(1)}, u32[]{:S(2)}) copy-start(s32[2]{0:T(128)S(1)} %pad_add_fusion.at_ref) | copy-start | bytes 28
  114.9 1.4 copy-start.2
  120.7 1.6 copy-start
  132.3 66.4 %copy-start.6 = (bf16[128,512]{1,0:T(8,128)(2,1)S(1)}, bf16[128,512]{1,0:T(8,128)(2,1)}, u32[]{:S(2)}) copy-start(bf16[128,512]{1,0:T(8,128)(2,1)} %get-tuple-element.9) | copy-start | bytes 393220
  132.3 66.5 %copy-start.7 = (bf16[128,512]{1,0:T(8,128)(2,1)S(1)}, bf16[128,512]{1,0:T(8,128)(2,1)}, u32[]{:S(2)}) copy-start(bf16[128,512]{1,0:T(8,128)(2,1)} %get-tuple-element.11) | copy-start | bytes 393220
  180.5 18.2 %all-to-all-start.2 = ((bf16[32,16,128]{2,1,0:T(8,128)(2,1)}), bf16[32,16,128]{2,1,0:T(8,128)(2,1)S(1)}, u32[]{:S(2)}, u32[]{:S(2)}) async-start(bf16[32,16,128]{2,1,0:T(8,128)(2,1)} %bitcast.61), calls=%async_computation.3 | async-start | bytes 262144 | tf_op jit(solution)/shard_map/all_to_all | solution.py:211
Sparse Core Ops, SparseCore 0:
  35.9 38.5 all-gather.4
  77.1 37.6 all-gather.6
  117.7 62.8 reduce-scatter.1

commit v2 on v1

v2 whole, which is shorter than its diff:
```python
import functools

import jax
import jax.numpy as jnp
from jax import lax
from jax.experimental import pallas as pl
from jax.experimental.pallas import tpu as pltpu
from jax.sharding import Mesh
from jax.sharding import PartitionSpec as P

EPSILON = 1e-06
LOG2E = 1.4426950408889634
F32 = jnp.float32
BF16 = jnp.bfloat16
Z, X, Y, CORE = 8, 4, 8, 2
EP = ("z", "x")
TP = ("y", "core")
LANES = 128


def dot(a, b, dims=((1,), (0,))):
    return lax.dot_general(a, b, (dims, ((), ())), preferred_element_type=F32)


def block_kernel(depth, width, len_, hd, at_ref, q_ref, kvo_ref, out_ref, tri_ref, tot_ref, acc_ref, carry_ref):
    z, x = at_ref[0], at_ref[1]
    c = hd**-0.5 * LOG2E
    rows_i = lax.broadcasted_iota(jnp.int32, (len_, len_), 0)
    cols_i = lax.broadcasted_iota(jnp.int32, (len_, len_), 1)
    tri_ref[...] = jnp.where(rows_i > cols_i, -1.0, 0.0).astype(BF16)
    tot_ref[...] = jnp.zeros_like(tot_ref)
    lane = lax.broadcasted_iota(jnp.int32, (len_, LANES), 1)
    n_off = len_ // LANES

    def pair(to, k_at, old, masked):
        q = q_ref[to]
        k = kvo_ref[k_at, pl.ds(0, len_), :]
        v = kvo_ref[k_at, pl.ds(len_, len_), :]
        o = kvo_ref[k_at, pl.ds(2 * len_, 16), :].astype(F32)
        off = jnp.concatenate([o[i : i + 1, :] for i in range(n_off)], axis=1) * LOG2E
        u = dot(q, k, ((1,), (1,))) * c + off
        sp = kept = jnp.maximum(u, 0.0) + jnp.log2(1.0 + jnp.exp2(-jnp.abs(u)))
        if masked:
            strict = cols_i < rows_i
            kept = jnp.where(strict, sp, 0.0)
        w = dot(kept.astype(BF16), tri_ref[...])
        p = jnp.exp2(u - sp + w)
        if masked:
            p = jnp.where(strict, p, 0.0)
        total = jnp.broadcast_to(w[:, 0:1] - kept[:, 0:1], (len_, LANES))
        summed = dot(p.astype(BF16), v)
        if masked:
            acc, carry = summed, total
        else:
            carry = carry_ref[...] * old
            acc = acc_ref[...] * old + jnp.exp2(carry) * summed
            carry = carry + total
        carry_ref[...] = carry
        acc_ref[...] = acc
        out_ref[to, pl.ds(0, len_), :] = acc.astype(BF16)
        tot_ref[...] = jnp.where(lane == to, carry, tot_ref[...])

    pair(z, x, None, True)

    def full(i, done):
        own = i < x
        j = i - x
        fresh = jnp.logical_and(jnp.logical_not(own), j % width == 0)
        pair(
            jnp.where(own, z, z + 1 + j // width),
            jnp.where(own, x - 1 - i, width - 1 - j % width),
            jnp.where(fresh, 0.0, 1.0),
            False,
        )
        return done

    lax.fori_loop(0, x + width * (depth - 1 - z), full, 0)

    def clear(i, done):
        out_ref[i, pl.ds(0, len_), :] = jnp.zeros((len_, hd), BF16)
        return done

    lax.fori_loop(0, z, clear, 0)
    cols = [tot_ref[r * LANES : (r + 1) * LANES, :].T for r in range(n_off)]
    for to in range(depth):
        rest = [col[to : to + 1, :] for col in cols]
        terms = []
        for _ in range(3):
            term = [r.astype(BF16).astype(F32) for r in rest]
            rest = [r - t for r, t in zip(rest, term)]
            terms += term
        terms.append(jnp.zeros((16 - len(terms), LANES), F32))
        out_ref[to, pl.ds(len_, 16), :] = jnp.concatenate(terms, axis=0).astype(BF16)


def join_kernel(depth, len_, in_ref, out_ref, scale_ref):
    n_off = len_ // LANES
    later = [jnp.zeros((1, LANES), F32)] * n_off
    scale_ref[...] = jnp.zeros_like(scale_ref)
    for at in reversed(range(depth)):
        t = in_ref[at, pl.ds(len_, 16), :].astype(F32)
        for r in range(n_off):
            scale_ref[at : at + 1, r * LANES : (r + 1) * LANES] = jnp.exp2(later[r])
            for term in range(3):
                i = term * n_off + r
                later[r] = later[r] + t[i : i + 1, :]
    for r in range(n_off):
        rows = slice(r * LANES, (r + 1) * LANES)
        cols = scale_ref[:, rows].T
        acc = jnp.zeros((LANES, out_ref.shape[1]), F32)
        for at in range(depth):
            acc = acc + in_ref[at, rows, :].astype(F32) * cols[:, at : at + 1]
        out_ref[rows, :] = acc.astype(out_ref.dtype)


def vmem(n):
    return [pl.BlockSpec(memory_space=pltpu.VMEM)] * n


SMEM = pl.BlockSpec(memory_space=pltpu.SMEM)


def stick_mixer(queries, keys, values, key_offset):
    depth, width = lax.axis_size("z"), lax.axis_size("x")
    len_, hd = queries.shape
    at = jnp.stack([lax.axis_index("z"), lax.axis_index("x")]).astype(jnp.int32)
    off = jnp.pad(key_offset.reshape(-1, LANES), ((0, 16 - len_ // LANES), (0, 0)))
    kvo = jnp.concatenate([keys, values, off], axis=0)
    kvo = lax.all_gather(kvo, "x")
    q = lax.all_gather(queries, "z")
    sums = pl.pallas_call(
        functools.partial(block_kernel, depth, width, len_, hd),
        out_shape=jax.ShapeDtypeStruct((depth, len_ + 16, hd), BF16),
        in_specs=[SMEM] + vmem(2),
        out_specs=vmem(1)[0],
        scratch_shapes=[
            pltpu.VMEM((len_, len_), BF16),
            pltpu.VMEM((len_, LANES), F32),
            pltpu.VMEM((len_, hd), F32),
            pltpu.VMEM((len_, LANES), F32),
        ],
        compiler_params=pltpu.CompilerParams(vmem_limit_bytes=32 << 20),
        cost_estimate=pl.CostEstimate(
            flops=depth * width * len_ * len_ * (4 * hd + 2 * len_),
            transcendentals=3 * depth * width * len_ * len_,
            bytes_accessed=2 * (2 * depth * len_ * hd + kvo.size),
        ),
        name="stick_blocks",
    )(at, q, kvo)
    sums = lax.all_to_all(sums, "z", 0, 0, tiled=True)
    return pl.pallas_call(
        functools.partial(join_kernel, depth, len_),
        out_shape=jax.ShapeDtypeStruct((len_, hd), BF16),
        in_specs=vmem(1),
        out_specs=vmem(1)[0],
        scratch_shapes=[pltpu.VMEM((LANES, len_), F32)],
        cost_estimate=pl.CostEstimate(
            flops=2 * depth * len_ * hd, transcendentals=depth * len_, bytes_accessed=2 * depth * len_ * hd
        ),
        name="stick_join",
    )(sums)


def dispatch_kernel(cap, at_ref, rows_ref, gain_ref, ids_ref, wts_ref, out_ref, hi_ref, lo_ref):
    tok, slots = rows_ref.shape[0], out_ref.shape[0]
    rows = rows_ref[...].astype(F32)
    rms = lax.rsqrt(jnp.mean(rows * rows, axis=1, keepdims=True) + EPSILON)
    first, second = ids_ref[:, 0:1], ids_ref[:, 1:2]
    lane = lax.broadcasted_iota(jnp.int32, (tok, LANES), 1)
    chosen = jnp.where((first == lane) | (second == lane), 1.0, 0.0).astype(BF16)
    before = lax.broadcasted_iota(jnp.int32, (tok, tok), 1) < lax.broadcasted_iota(
        jnp.int32, (tok, tok), 0
    )
    rank = dot(jnp.where(before, 1.0, 0.0).astype(BF16), chosen).astype(BF16)
    spread = (
        lax.broadcasted_iota(jnp.int32, (LANES, slots), 1) // cap
        == lax.broadcasted_iota(jnp.int32, (LANES, slots), 0)
    )
    spread = jnp.where(spread, 1.0, 0.0).astype(BF16)
    slot = lax.broadcasted_iota(jnp.int32, (tok, slots), 1)
    taken = (dot(chosen, spread) > 0.5) & (dot(rank, spread) == (slot % cap).astype(F32))
    pick = jnp.where(taken, 1.0, 0.0).astype(BF16)
    for i in range(out_ref.shape[1] // LANES):
        own = pl.ds(pl.multiple_of((2 * i + at_ref[0]) * LANES, LANES), LANES)
        normed = (rows_ref[:, own].astype(F32) * rms * gain_ref[:, own]).astype(BF16)
        out_ref[:, i * LANES : (i + 1) * LANES] = dot(pick, normed, ((0,), (0,))).astype(BF16)
    weight = jnp.where(slot // cap == first, wts_ref[:, 0:1], wts_ref[:, 1:2])
    weight = jnp.where(taken, weight, 0.0)
    hi = weight.astype(BF16)
    hi_ref[...] = hi
    lo_ref[...] = (weight - hi.astype(F32)).astype(BF16)


def expert_kernel(at_ref, mine_ref, other_ref, gate_ref, up_ref, down_ref, keep_ref, send_ref, all_ref):
    core = at_ref[0]
    chunks = mine_ref.shape[1] // LANES
    for i in range(chunks):
        here = slice(i * LANES, (i + 1) * LANES)
        all_ref[:, pl.ds(pl.multiple_of((2 * i + core) * LANES, LANES), LANES)] = mine_ref[:, here]
        all_ref[:, pl.ds(pl.multiple_of((2 * i + 1 - core) * LANES, LANES), LANES)] = other_ref[:, here]
    tokens = all_ref[...]
    gate = dot(tokens, gate_ref[...], ((1,), (1,)))
    up = dot(tokens, up_ref[...], ((1,), (1,)))
    hidden = (gate / (1.0 + jnp.exp(-gate)) * up).astype(BF16)
    all_ref[...] = dot(hidden, down_ref[...]).astype(BF16)
    for i in range(chunks):
        here = slice(i * LANES, (i + 1) * LANES)
        keep_ref[:, here] = all_ref[:, pl.ds(pl.multiple_of((2 * i + core) * LANES, LANES), LANES)]
        send_ref[:, here] = all_ref[:, pl.ds(pl.multiple_of((2 * i + 1 - core) * LANES, LANES), LANES)]


def swap(x):
    return lax.ppermute(x, "core", [(0, 1), (1, 0)])


def routed_experts(rows, gain, gate_w, up_w, down_w, expert_ids, route_weights):
    experts = lax.axis_size(EP)
    tok, width = rows.shape
    half = width // lax.axis_size("core")
    hosts = lax.axis_size("y")
    cap = 2 * expert_ids.shape[1] * tok // experts
    slots = experts * cap
    at = jnp.stack([lax.axis_index("core")]).astype(jnp.int32)
    outgoing, hi, lo = pl.pallas_call(
        functools.partial(dispatch_kernel, cap),
        out_shape=(
            jax.ShapeDtypeStruct((slots, half), BF16),
            jax.ShapeDtypeStruct((tok, slots), BF16),
            jax.ShapeDtypeStruct((tok, slots), BF16),
        ),
        in_specs=[SMEM] + vmem(4),
        out_specs=tuple(vmem(3)),
        name="dispatch",
    )(at, rows, gain.reshape(1, -1), expert_ids, route_weights)
    mine = lax.all_to_all(outgoing.reshape(experts, cap, half), EP, 0, 0, tiled=True)
    mine = mine.reshape(slots, half)
    hidden = gate_w.shape[2]
    keep, send = pl.pallas_call(
        expert_kernel,
        out_shape=(jax.ShapeDtypeStruct((slots, half), BF16),) * 2,
        in_specs=[SMEM] + vmem(5),
        out_specs=tuple(vmem(2)),
        scratch_shapes=[pltpu.VMEM((slots, width), BF16)],
        compiler_params=pltpu.CompilerParams(vmem_limit_bytes=32 << 20),
        cost_estimate=pl.CostEstimate(
            flops=6 * slots * width * hidden,
            transcendentals=slots * hidden,
            bytes_accessed=2 * (2 * slots * width + 3 * width * hidden),
        ),
        name="experts",
    )(at, mine, swap(mine), gate_w[0].T, up_w[0].T, down_w[0])
    share = (keep.astype(F32) + swap(send).astype(F32)).astype(BF16)
    back = lax.all_to_all(share.reshape(experts, cap, half), EP, 0, 0, tiled=True)
    back = back.reshape(slots, half)
    partial = (dot(hi, back) + dot(lo, back)).astype(BF16)
    partial = jnp.moveaxis(partial.reshape(tok, hosts, -1), 1, 0)
    partial = lax.all_to_all(partial, "y", 0, 0, tiled=True)
    mixed = partial.astype(F32).sum(axis=0).astype(BF16)
    return lax.all_gather(mixed, TP, axis=1, tiled=True)


def body(
    queries, keys, values, key_offset, rows, gain, gate_w, up_w, down_w, expert_ids, route_weights
):
    mixed = routed_experts(rows, gain, gate_w, up_w, down_w, expert_ids, route_weights)
    attended = stick_mixer(queries, keys, values, key_offset)
    return (attended, mixed)


def solution(mesh):
    fine = Mesh(mesh.devices.reshape(Z, X, Y, CORE), ("z", "x", "y", "core"))
    return jax.shard_map(
        body,
        mesh=fine,
        in_specs=(
            P(EP, TP),
            P(EP, TP),
            P(EP, TP),
            P(EP, TP),
            P(EP, None),
            P(),
            P(EP, None, TP),
            P(EP, None, TP),
            P(EP, TP, None),
            P(EP, None),
            P(EP, None),
        ),
        out_specs=(P(EP, TP), P(EP, None)),
        check_vma=False,
    )
```

time: 228 us -> 197 us (0.86)
  waiting for transfers between devices: 98.4 us -> 27.2 us
  blocking collectives: 74.4 us -> 106 us
  Pallas kernels: 12.1 us -> 31.7 us
  starting transfers between devices: 8.92 us -> 23 us
  between operations: 13.9 us -> 0.75 us
  matrix products: 7.43 us -> 0.62 us
  local copies, waits for them, and re-layouts: 9.09 us -> 4.97 us
    all_gather x2 -> x0, waiting for transfers between devices: 56.4 us -> none  [the longest x1 34.7 us: routed_experts(): arrived = lax.all_gather(arrived.reshape(slots, own), TP)]
    reduce_scatter x1 -> x0, waiting for transfers between devices: 33.3 us -> none  [routed_experts(): share = lax.psum_scatter(part, TP, scatter_dimension=0, tiled=True)]
    all_gather x2, blocking collectives: 20.6 us -> 41.4 us  [the longest x1 24.3 us: stick_mixer(): q = lax.all_gather(queries, 'z')]
    pallas_call x1, Pallas kernels: 4.44 us -> 23.3 us  [stick_mixer(): pl.pallas_call(functools.partial(block_kernel, depth, width, len_, hd), o...]
    all_to_all x1 -> x3, waiting for transfers between devices: 8.64 us -> 22.7 us  [the longest x1 15.9 us: stick_mixer(): sums = lax.all_to_all(sums, 'z', 0, 0, tiled=True)]
    all_to_all x1 -> x3, starting transfers between devices: 8.8 us -> 16.1 us  [the longest x1 6.95 us: routed_experts(): partial = lax.all_to_all(partial, 'y', 0, 0, tiled=True)]
    all_to_all x2 -> x1, blocking collectives: 32.8 us -> 40 us  [routed_experts(): lax.all_to_all(outgoing.reshape(experts, cap, half), EP, 0, 0, tiled=True)]
    dot_general x2 -> x0, matrix products: 7.08 us -> none  [the longest x1 4.5 us: routed_experts(): jnp.einsum('sf,fjc->jsc', hidden, down_w.reshape(-1, groups, own), prefer...]
  transfers between devices with their start and end apart: 4 -> 5, of which waited for: 4 -> 4; matrix products, arithmetic and copies ran while one was open for 5% -> 1% of each run, Pallas kernels for 4% -> 13%
where the time goes in v2:
time: 197 us; the launch traced here: 196 us
  blocking collectives  106 us (54%)
  Pallas kernels  31.7 us (16%)
  waiting for transfers between devices  27.2 us (14%)
  starting transfers between devices  23 us (12%)
  local copies, waits for them, and re-layouts  4.97 us (3%)
    all_to_all x1, blocking collectives, routed_experts(): lax.all_to_all(outgoing.reshape(experts, cap, half), EP, 0, 0, tiled=True)  40 us
    all_gather x1, blocking collectives, stick_mixer(): q = lax.all_gather(queries, 'z')  24.3 us
    all_gather x1, blocking collectives, routed_experts(): return lax.all_gather(mixed, TP, axis=1, tiled=True)  24.2 us
    pallas_call x1, Pallas kernels, stick_mixer(): pl.pallas_call(functools.partial(block_kernel, depth, width, len_, hd), o...  23.3 us
    all_gather x1, blocking collectives, stick_mixer(): kvo = lax.all_gather(kvo, 'x')  17.1 us
    all_to_all x1, waiting for transfers between devices, stick_mixer(): sums = lax.all_to_all(sums, 'z', 0, 0, tiled=True)  15.9 us
    ppermute x2, starting transfers between devices, swap(): return lax.ppermute(x, 'core', [(0, 1), (1, 0)])  7 us
    all_to_all x1, starting transfers between devices, routed_experts(): partial = lax.all_to_all(partial, 'y', 0, 0, tiled=True)  6.95 us
  transfers between devices with their start and end apart: 5, of which 4 were waited for; matrix products, arithmetic and copies ran while one was open for 1% of the time, Pallas kernels for 13%

profile of v2, /device:TPU:1, one launch (start us, length us, event | category | flops | bytes accessed | tf_op | source)
XLA Modules:
  0.0 195.5 jit_solution(706934393236208057)
XLA Ops:
  0.6 1.4 copy.15.ids_ref
  2.0 1.4 copy.16.wts_ref
  3.4 0.0 copy-start.2
  3.4 3.0 %dispatch.1 = (bf16[512,1024]{1,0:T(8,128)(2,1)}, bf16[128,512]{1,0:T(8,128)(2,1)}, bf16[128,512]{1,0:T(8,128)(2,1)}) custom-call(s32[1]{0:T(128)} %bitcast.4.at_ref, bf16[128,2048]{1,0:T(8,128)(2,1)} %rows_ref.1, f32[1,2048]{1,0:T(1,128)} %bitcast.40, s32[128,2]{1,0:T(8,128)} %copy.15.ids_ref, f32[128,2]{1,0:T(8,128)} %copy.16.wts_ref), custom_call_target="tpu_custom_call" | custom-call | tf_op jit(solution)/shard_map/dispatch/pallas_call | solution.py:224
  6.5 0.0 copy-start
  6.5 0.0 copy-start.1
  6.5 40.0 %all_to_all.20 = bf16[32,16,1024]{2,1,0:T(8,128)(2,1)S(1)} all-to-all(bf16[32,16,1024]{2,1,0:T(8,128)(2,1)} %bitcast.39), channel_id=1, replica_groups=mesh['z'=8,'x'=4,'y'=8,'core'=2] {'z','x'}, dimensions={0} | all-to-all | bytes 2097152 | tf_op jit(solution)/shard_map/all_to_all | solution.py:235
  46.5 4.7 %collective-permute-start = (bf16[512,1024]{1,0:T(8,128)(2,1)S(1)}, bf16[512,1024]{1,0:T(8,128)(2,1)S(1)}, u32[]{:S(2)}, u32[]{:S(2)}) collective-permute-start(bf16[512,1024]{1,0:T(8,128)(2,1)S(1)} %bitcast.30), channel_id=1, source_target_pairs={{0,1},{1,0},{2,3},{3,2},{4,5},{5,4},{6,7},{7,6},{8,9},{9,8},{10,11... | collective-permute-start | bytes 3145736 | tf_op jit(solution)/shard_map/ppermute | solution.py:213
  51.2 2.3 %collective-permute-done.other_ref = bf16[512,1024]{1,0:T(8,128)(2,1)S(1)} collective-permute-done((bf16[512,1024]{1,0:T(8,128)(2,1)S(1)}, bf16[512,1024]{1,0:T(8,128)(2,1)S(1)}, u32[]{:S(2)}, u32[]{:S(2)}) %collective-permute-start) | collective-permute-done | bytes 1048608 | tf_op jit(solution)/shard_map/ppermute | solution.py:213
  53.5 0.0 copy-done.2
  53.5 0.0 copy-done
  53.5 0.0 copy-done.1
  53.5 2.9 %experts.1 = (bf16[512,1024]{1,0:T(8,128)(2,1)S(1)}, bf16[512,1024]{1,0:T(8,128)(2,1)S(1)}) custom-call(s32[1]{0:T(128)} %bitcast.4.at_ref, bf16[512,1024]{1,0:T(8,128)(2,1)S(1)} %bitcast.31, bf16[512,1024]{1,0:T(8,128)(2,1)S(1)} %collective-permute-done.other_ref, bf16[224,2048]{1,0:T(8,128)(2,1)S(1)} %bitcast.34, bf16[224,2048]{1,0:T(8,128)(2,1)S(1)} %bitcast.35, ...), custom_call_target="tpu_custom_call" | custom-call | flops 1409286144 | bytes 6946816 | tf_op jit(solution)/shard_map/experts/pallas_call | solution.py:238
  56.5 2.3 %collective-permute-start.1 = (bf16[512,1024]{1,0:T(8,128)(2,1)S(1)}, bf16[512,1024]{1,0:T(8,128)(2,1)S(1)}, u32[]{:S(2)}, u32[]{:S(2)}) collective-permute-start(bf16[512,1024]{1,0:T(8,128)(2,1)S(1)} %get-tuple-element.10), channel_id=1, source_target_pairs={{0,1},{1,0},{2,3},{3,2},{4,5},{5,4},{6,7},{7,6},{8,9},{9,8},{10,11... | collective-permute-start | bytes 3145736 | tf_op jit(solution)/shard_map/ppermute | solution.py:213
  58.7 2.3 %collective-permute-done.1 = bf16[512,1024]{1,0:T(8,128)(2,1)S(1)} collective-permute-done((bf16[512,1024]{1,0:T(8,128)(2,1)S(1)}, bf16[512,1024]{1,0:T(8,128)(2,1)S(1)}, u32[]{:S(2)}, u32[]{:S(2)}) %collective-permute-start.1) | collective-permute-done | bytes 1048608 | tf_op jit(solution)/shard_map/ppermute | solution.py:213
  61.0 1.4 add_convert_fusion
  62.4 0.0 copy-start.9
  62.4 0.0 copy-start.7
  62.4 0.0 copy-start.8
  62.4 5.4 %all-to-all-start.2 = ((bf16[32,16,1024]{2,1,0:T(8,128)(2,1)}), bf16[32,16,1024]{2,1,0:T(8,128)(2,1)S(1)}, u32[]{:S(2)}, u32[]{:S(2)}) async-start(bf16[32,16,1024]{2,1,0:T(8,128)(2,1)} %bitcast.13), calls=%async_computation.2 | async-start | bytes 2097152 | tf_op jit(solution)/shard_map/all_to_all | solution.py:253
  67.8 0.0 copy-start.6
  67.9 0.0 copy-done.9
  67.9 0.1 pad_add_fusion.at_ref
  68.0 0.0 copy-done.7
  68.0 0.0 copy-done.8
  68.0 17.1 %all-gather.1 = bf16[3136,128]{1,0:T(8,128)(2,1)S(1)} all-gather(bf16[784,128]{1,0:T(8,128)(2,1)S(1)} %fusion.3), channel_id=3, replica_groups=mesh['z'=8,'x'=4,'y'=8,'core'=2] {'x'}, dimensions={0}, use_global_device_ids=true | all-gather | bytes 1003520 | tf_op jit(solution)/shard_map/all_gather | solution.py:129
  85.1 0.0 copy-done.6
  85.1 24.3 %all-gather = bf16[3072,128]{1,0:T(8,128)(2,1)S(1)} all-gather(bf16[384,128]{1,0:T(8,128)(2,1)S(1)} %copy-done.6), channel_id=2, replica_groups=mesh['z'=8,'x'=4,'y'=8,'core'=2] {'z'}, dimensions={0}, use_global_device_ids=true | all-gather | bytes 884736 | tf_op jit(solution)/shard_map/all_gather | solution.py:130
  109.4 23.3 %stick_blocks.1 = bf16[8,400,128]{2,1,0:T(8,128)(2,1)} custom-call(s32[2]{0:T(128)S(1)} %pad_add_fusion.at_ref, bf16[8,384,128]{2,1,0:T(8,128)(2,1)S(1)} %bitcast.33, bf16[4,784,128]{2,1,0:T(8,128)(2,1)S(1)} %bitcast.32), custom_call_target="tpu_custom_call" | custom-call | flops 6039797760 | bytes 2375680 | tf_op jit(solution)/shard_map/stick_blocks/pallas_call | solution.py:131
  132.7 0.0 copy-start.4
  132.7 0.0 all-to-all-done.2
  132.7 3.7 %all-to-all-start = ((bf16[8,400,128]{2,1,0:T(8,128)(2,1)}), bf16[8,400,128]{2,1,0:T(8,128)(2,1)S(1)}, u32[]{:S(2)}, u32[]{:S(2)}) async-start(bf16[8,400,128]{2,1,0:T(8,128)(2,1)} %stick_blocks.1), calls=%async_computation | async-start | bytes 1638400 | tf_op jit(solution)/shard_map/all_to_all | solution.py:150
  136.4 0.0 copy-start.5
  136.4 0.0 copy-done.4
  136.4 0.3 fusion.4
  136.7 0.6 copy-done.5
  137.3 0.3 fusion.1
  137.6 0.8 copy.20
  138.4 15.9 %all-to-all-done.in_ref = bf16[8,400,128]{2,1,0:T(8,128)(2,1)S(1)} async-done(((bf16[8,400,128]{2,1,0:T(8,128)(2,1)}), bf16[8,400,128]{2,1,0:T(8,128)(2,1)S(1)}, u32[]{:S(2)}, u32[]{:S(2)}) %all-to-all-start) | async-done | bytes 819232 | tf_op jit(solution)/shard_map/all_to_all | solution.py:150
  154.2 0.0 copy-start.3
  154.2 6.9 %all-to-all-start.3 = ((bf16[8,128,128]{2,1,0:T(8,128)(2,1)}), bf16[8,128,128]{2,1,0:T(8,128)(2,1)S(1)}, u32[]{:S(2)}, u32[]{:S(2)}) async-start(bf16[8,128,128]{2,1,0:T(8,128)(2,1)} %bitcast.29), calls=%async_computation.3 | async-start | bytes 524288 | tf_op jit(solution)/shard_map/all_to_all | solution.py:257
  161.2 0.0 copy-done.3
  161.2 2.5 %stick_join.1 = bf16[384,128]{1,0:T(8,128)(2,1)} custom-call(bf16[8,400,128]{2,1,0:T(8,128)(2,1)} %copy-done.3), custom_call_target="tpu_custom_call" | custom-call | flops 786432 | bytes 786432 | tf_op jit(solution)/shard_map/stick_join/pallas_call | solution.py:151
  163.7 6.9 %all-to-all-done.3 = bf16[8,128,128]{2,1,0:T(8,128)(2,1)S(1)} async-done(((bf16[8,128,128]{2,1,0:T(8,128)(2,1)}), bf16[8,128,128]{2,1,0:T(8,128)(2,1)S(1)}, u32[]{:S(2)}, u32[]{:S(2)}) %all-to-all-start.3) | async-done | bytes 262176 | tf_op jit(solution)/shard_map/all_to_all | solution.py:257
  170.6 24.2 %all_gather.19 = bf16[128,2048]{1,0:T(8,128)(2,1)S(1)} all-gather(bf16[128,128]{1,0:T(8,128)(2,1)S(1)} %reduce_sum.12), channel_id=1, replica_groups=mesh['z'=8,'x'=4,'y'=8,'core'=2] {'y','core'}, dimensions={1}, use_global_device_ids=true | all-gather | bytes 557056 | tf_op jit(solution)/shard_map/all_gather | solution.py:259
  194.7 0.8 copy.22
  (3 shorter events, 0.1 us)
Async XLA Ops:
  3.4 50.1 %copy-start.2 = (bf16[1,224,2048]{2,1,0:T(8,128)(2,1)S(1)}, bf16[1,224,2048]{2,1,0:T(8,128)(2,1)}, u32[]{:S(2)}) copy-start(bf16[1,224,2048]{2,1,0:T(8,128)(2,1)} %param.19) | copy-start | bytes 2752516
  6.5 47.0 %copy-start = (bf16[1,2048,224]{1,2,0:T(8,128)(2,1)S(1)}, bf16[1,2048,224]{1,2,0:T(8,128)(2,1)}, u32[]{:S(2)}) copy-start(bf16[1,2048,224]{1,2,0:T(8,128)(2,1)} %param.17) | copy-start | bytes 2752516
  6.5 47.0 %copy-start.1 = (bf16[1,2048,224]{1,2,0:T(8,128)(2,1)S(1)}, bf16[1,2048,224]{1,2,0:T(8,128)(2,1)}, u32[]{:S(2)}) copy-start(bf16[1,2048,224]{1,2,0:T(8,128)(2,1)} %param.18) | copy-start | bytes 2752516
  46.5 7.0 %collective-permute-start = (bf16[512,1024]{1,0:T(8,128)(2,1)S(1)}, bf16[512,1024]{1,0:T(8,128)(2,1)S(1)}, u32[]{:S(2)}, u32[]{:S(2)}) collective-permute-start(bf16[512,1024]{1,0:T(8,128)(2,1)S(1)} %bitcast.30), channel_id=1, source_target_pairs={{0,1},{1,0},{2,3},{3,2},{4,5},{5,4},{6,7},{7,6},{8,9},{9,8},{10,11... | collective-permute-start | bytes 3145736 | tf_op jit(solution)/shard_map/ppermute | solution.py:213
  56.5 4.6 %collective-permute-start.1 = (bf16[512,1024]{1,0:T(8,128)(2,1)S(1)}, bf16[512,1024]{1,0:T(8,128)(2,1)S(1)}, u32[]{:S(2)}, u32[]{:S(2)}) collective-permute-start(bf16[512,1024]{1,0:T(8,128)(2,1)S(1)} %get-tuple-element.10), channel_id=1, source_target_pairs={{0,1},{1,0},{2,3},{3,2},{4,5},{5,4},{6,7},{7,6},{8,9},{9,8},{10,11... | collective-permute-start | bytes 3145736 | tf_op jit(solution)/shard_map/ppermute | solution.py:213
  62.4 5.5 %copy-start.9 = (bf16[384,1]{0,1:T(2,128)(2,1)S(1)}, bf16[384,1]{0,1:T(2,128)(2,1)}, u32[]{:S(2)}) copy-start(bf16[384,1]{0,1:T(2,128)(2,1)} %param.14) | copy-start | bytes 2308
  62.4 5.6 %copy-start.7 = (bf16[384,128]{1,0:T(8,128)(2,1)S(1)}, bf16[384,128]{1,0:T(8,128)(2,1)}, u32[]{:S(2)}) copy-start(bf16[384,128]{1,0:T(8,128)(2,1)} %param.13) | copy-start | bytes 294916
  62.4 5.6 %copy-start.8 = (bf16[384,128]{1,0:T(8,128)(2,1)S(1)}, bf16[384,128]{1,0:T(8,128)(2,1)}, u32[]{:S(2)}) copy-start(bf16[384,128]{1,0:T(8,128)(2,1)} %param.12) | copy-start | bytes 294916
  62.4 70.3 %all-to-all-start.2 = ((bf16[32,16,1024]{2,1,0:T(8,128)(2,1)}), bf16[32,16,1024]{2,1,0:T(8,128)(2,1)S(1)}, u32[]{:S(2)}, u32[]{:S(2)}) async-start(bf16[32,16,1024]{2,1,0:T(8,128)(2,1)} %bitcast.13), calls=%async_computation.2 | async-start | bytes 2097152 | tf_op jit(solution)/shard_map/all_to_all | solution.py:253
  67.8 17.3 %copy-start.6 = (bf16[384,128]{1,0:T(8,128)(2,1)S(1)}, bf16[384,128]{1,0:T(8,128)(2,1)}, u32[]{:S(2)}) copy-start(bf16[384,128]{1,0:T(8,128)(2,1)} %param.11) | copy-start | bytes 294916
  132.7 3.7 %copy-start.4 = (bf16[128,512]{1,0:T(8,128)(2,1)S(1)}, bf16[128,512]{1,0:T(8,128)(2,1)}, u32[]{:S(2)}) copy-start(bf16[128,512]{1,0:T(8,128)(2,1)} %get-tuple-element.11) | copy-start | bytes 393220
  132.7 21.5 %all-to-all-start = ((bf16[8,400,128]{2,1,0:T(8,128)(2,1)}), bf16[8,400,128]{2,1,0:T(8,128)(2,1)S(1)}, u32[]{:S(2)}, u32[]{:S(2)}) async-start(bf16[8,400,128]{2,1,0:T(8,128)(2,1)} %stick_blocks.1), calls=%async_computation | async-start | bytes 1638400 | tf_op jit(solution)/shard_map/all_to_all | solution.py:150
  136.4 0.9 copy-start.5
  154.2 7.0 %copy-start.3 = (bf16[8,400,128]{2,1,0:T(8,128)(2,1)}, bf16[8,400,128]{2,1,0:T(8,128)(2,1)S(1)}, u32[]{:S(2)}) copy-start(bf16[8,400,128]{2,1,0:T(8,128)(2,1)S(1)} %all-to-all-done.in_ref) | copy-start | bytes 2457604
  154.2 16.3 %all-to-all-start.3 = ((bf16[8,128,128]{2,1,0:T(8,128)(2,1)}), bf16[8,128,128]{2,1,0:T(8,128)(2,1)S(1)}, u32[]{:S(2)}, u32[]{:S(2)}) async-start(bf16[8,128,128]{2,1,0:T(8,128)(2,1)} %bitcast.29), calls=%async_computation.3 | async-start | bytes 524288 | tf_op jit(solution)/shard_map/all_to_all | solution.py:257

commit v3 on v2

v3 whole, which is shorter than its diff:
```python
import functools

import jax
import jax.numpy as jnp
from jax import lax
from jax.experimental import pallas as pl
from jax.experimental.pallas import tpu as pltpu
from jax.sharding import Mesh
from jax.sharding import PartitionSpec as P


EPSILON = 1e-06
LOG2E = 1.4426950408889634
F32 = jnp.float32
BF16 = jnp.bfloat16
EXTRA1 = 0
EXTRA2 = 0
Z, X, Y, CORE = 8, 4, 8, 2
EP = ("z", "x")
TP = ("y", "core")
LANES = 128


def dot(a, b, dims=((1,), (0,))):
    return lax.dot_general(a, b, (dims, ((), ())), preferred_element_type=F32)


def block_kernel(depth, width, len_, hd, at_ref, q_ref, *refs):
    near, (out_ref, kvo_ref, tri_ref, tot_ref, acc_ref, carry_ref) = refs[:width], refs[width:]
    z, x = at_ref[0], at_ref[1]
    for step in range(width):
        kvo_ref[(x + width - step) % width] = near[step][...]
    c = hd**-0.5 * LOG2E
    rows_i = lax.broadcasted_iota(jnp.int32, (len_, len_), 0)
    cols_i = lax.broadcasted_iota(jnp.int32, (len_, len_), 1)
    tri_ref[...] = jnp.where(rows_i > cols_i, -1.0, 0.0).astype(BF16)
    tot_ref[...] = jnp.zeros_like(tot_ref)
    lane = lax.broadcasted_iota(jnp.int32, (len_, LANES), 1)
    n_off = len_ // LANES

    def pair(to, k_at, old, masked):
        q = q_ref[to]
        k = kvo_ref[k_at, pl.ds(0, len_), :]
        v = kvo_ref[k_at, pl.ds(len_, len_), :]
        o = kvo_ref[k_at, pl.ds(2 * len_, 16), :].astype(F32)
        off = jnp.concatenate([o[i : i + 1, :] for i in range(n_off)], axis=1) * LOG2E
        u = dot(q, k, ((1,), (1,))) * c + off
        sp = kept = jnp.maximum(u, 0.0) + jnp.log2(1.0 + jnp.exp2(-jnp.abs(u)))
        if masked:
            strict = cols_i < rows_i
            kept = jnp.where(strict, sp, 0.0)
        w = dot(kept.astype(BF16), tri_ref[...])
        p = jnp.exp2(u - sp + w)
        if masked:
            p = jnp.where(strict, p, 0.0)
        total = jnp.broadcast_to(w[:, 0:1] - kept[:, 0:1], (len_, LANES))
        summed = dot(p.astype(BF16), v)
        if masked:
            acc, carry = summed, total
        else:
            carry = carry_ref[...] * old
            acc = acc_ref[...] * old + jnp.exp2(carry) * summed
            carry = carry + total
        carry_ref[...] = carry
        acc_ref[...] = acc
        out_ref[to, pl.ds(0, len_), :] = acc.astype(BF16)
        tot_ref[...] = jnp.where(lane == to, carry, tot_ref[...])

    pair(z, x, None, True)

    def full(i, done):
        own = i < x
        j = i - x
        fresh = jnp.logical_and(jnp.logical_not(own), j % width == 0)
        pair(
            jnp.where(own, z, z + 1 + j // width),
            jnp.where(own, x - 1 - i, width - 1 - j % width),
            jnp.where(fresh, 0.0, 1.0),
            False,
        )
        return done

    lax.fori_loop(0, x + width * (depth - 1 - z), full, 0)

    def clear(i, done):
        out_ref[i, pl.ds(0, len_), :] = jnp.zeros((len_, hd), BF16)
        return done

    lax.fori_loop(0, z, clear, 0)
    cols = [tot_ref[r * LANES : (r + 1) * LANES, :].T for r in range(n_off)]
    for to in range(depth):
        rest = [col[to : to + 1, :] for col in cols]
        terms = []
        for _ in range(3):
            term = [r.astype(BF16).astype(F32) for r in rest]
            rest = [r - t for r, t in zip(rest, term)]
            terms += term
        terms.append(jnp.zeros((16 - len(terms), LANES), F32))
        out_ref[to, pl.ds(len_, 16), :] = jnp.concatenate(terms, axis=0).astype(BF16)


def join_kernel(depth, len_, in_ref, out_ref, scale_ref):
    n_off = len_ // LANES
    later = [jnp.zeros((1, LANES), F32)] * n_off
    scale_ref[...] = jnp.zeros_like(scale_ref)
    for at in reversed(range(depth)):
        t = in_ref[at, pl.ds(len_, 16), :].astype(F32)
        for r in range(n_off):
            scale_ref[at : at + 1, r * LANES : (r + 1) * LANES] = jnp.exp2(later[r])
            for term in range(3):
                i = term * n_off + r
                later[r] = later[r] + t[i : i + 1, :]
    for r in range(n_off):
        rows = slice(r * LANES, (r + 1) * LANES)
        cols = scale_ref[:, rows].T
        acc = jnp.zeros((LANES, out_ref.shape[1]), F32)
        for at in range(depth):
            acc = acc + in_ref[at, rows, :].astype(F32) * cols[:, at : at + 1]
        out_ref[rows, :] = acc.astype(out_ref.dtype)


def vmem(n):
    return [pl.BlockSpec(memory_space=pltpu.VMEM)] * n


SMEM = pl.BlockSpec(memory_space=pltpu.SMEM)


def dispatch_kernel(cap, at_ref, rows_ref, gain_ref, ids_ref, wts_ref, out_ref, hi_ref, lo_ref):
    tok, slots = rows_ref.shape[0], out_ref.shape[0]
    rows = rows_ref[...].astype(F32)
    rms = lax.rsqrt(jnp.mean(rows * rows, axis=1, keepdims=True) + EPSILON)
    first, second = ids_ref[0:1, :], ids_ref[1:2, :]
    expert = lax.broadcasted_iota(jnp.int32, (LANES, tok), 0)
    chosen = jnp.where((first == expert) | (second == expert), 1.0, 0.0).astype(BF16)
    before = lax.broadcasted_iota(jnp.int32, (tok, tok), 0) < lax.broadcasted_iota(
        jnp.int32, (tok, tok), 1
    )
    rank = dot(chosen, jnp.where(before, 1.0, 0.0).astype(BF16)).astype(BF16)
    spread = (
        lax.broadcasted_iota(jnp.int32, (slots, LANES), 0) // cap
        == lax.broadcasted_iota(jnp.int32, (slots, LANES), 1)
    )
    spread = jnp.where(spread, 1.0, 0.0).astype(BF16)
    slot = lax.broadcasted_iota(jnp.int32, (slots, tok), 0)
    taken = (dot(spread, chosen) > 0.5) & (dot(spread, rank) == (slot % cap).astype(F32))
    pick = jnp.where(taken, 1.0, 0.0).astype(BF16)
    for i in range(out_ref.shape[1] // LANES):
        own = pl.ds(pl.multiple_of((2 * i + at_ref[0]) * LANES, LANES), LANES)
        normed = (rows_ref[:, own].astype(F32) * rms * gain_ref[:, own]).astype(BF16)
        out_ref[:, i * LANES : (i + 1) * LANES] = dot(pick, normed).astype(BF16)
    weight = jnp.where(slot // cap == first, wts_ref[0:1, :], wts_ref[1:2, :])
    weight = jnp.where(taken, weight, 0.0)
    hi = weight.astype(BF16)
    hi_ref[...] = hi
    lo_ref[...] = (weight - hi.astype(F32)).astype(BF16)


def expert_kernel(at_ref, mine_ref, other_ref, gate_ref, up_ref, down_ref, *rest):
    keep_ref, send_ref, all_ref = rest[-3:]
    core = at_ref[0]
    chunks = mine_ref.shape[1] // LANES
    for i in range(chunks):
        here = slice(i * LANES, (i + 1) * LANES)
        all_ref[:, pl.ds(pl.multiple_of((2 * i + core) * LANES, LANES), LANES)] = mine_ref[:, here]
        all_ref[:, pl.ds(pl.multiple_of((2 * i + 1 - core) * LANES, LANES), LANES)] = other_ref[:, here]
    tokens = all_ref[...]
    gate = dot(tokens, gate_ref[...], ((1,), (1,)))
    up = dot(tokens, up_ref[...], ((1,), (1,)))
    hidden = (gate / (1.0 + jnp.exp(-gate)) * up).astype(BF16)
    all_ref[...] = dot(hidden, down_ref[...]).astype(BF16)
    for i in range(chunks):
        keep_ref[i] = all_ref[:, pl.ds(pl.multiple_of((2 * i + core) * LANES, LANES), LANES)]
        send_ref[i] = all_ref[:, pl.ds(pl.multiple_of((2 * i + 1 - core) * LANES, LANES), LANES)]


def sum_kernel(in_ref, *rest):
    out_ref = rest[-1]
    total = in_ref[0].astype(F32)
    for i in range(1, in_ref.shape[0]):
        total = total + in_ref[i].astype(F32)
    out_ref[...] = total.astype(out_ref.dtype)


def combine_kernel(hi_ref, lo_ref, back_ref, out_ref):
    back = back_ref[...]
    out_ref[...] = (
        dot(hi_ref[...], back, ((0,), (0,))) + dot(lo_ref[...], back, ((0,), (0,)))
    ).astype(BF16)


def swap(x):
    return lax.ppermute(x, "core", [(0, 1), (1, 0)])


ANY = pl.BlockSpec(memory_space=pl.ANY)


def layer(
    queries, keys, values, key_offset, rows, gain, gate_w, up_w, down_w, expert_ids, route_weights
):
    experts = lax.axis_size(EP)
    tok, width = rows.shape
    half = width // lax.axis_size("core")
    hosts = lax.axis_size("y")
    cap = 2 * expert_ids.shape[1] * tok // experts
    slots = experts * cap
    depth, wide = lax.axis_size("z"), lax.axis_size("x")
    len_, hd = queries.shape
    core = jnp.stack([lax.axis_index("core")]).astype(jnp.int32)
    place = jnp.stack([lax.axis_index("z"), lax.axis_index("x")]).astype(jnp.int32)
    outgoing, hi, lo = pl.pallas_call(
        functools.partial(dispatch_kernel, cap),
        out_shape=(
            jax.ShapeDtypeStruct((slots, half), BF16),
            jax.ShapeDtypeStruct((slots, tok), BF16),
            jax.ShapeDtypeStruct((slots, tok), BF16),
        ),
        in_specs=[SMEM] + vmem(4),
        out_specs=tuple(vmem(3)),
        name="dispatch",
    )(core, rows, gain.reshape(1, -1), expert_ids.T, route_weights.T)
    mine = lax.all_to_all(outgoing.reshape(experts, cap, half), EP, 0, 0, tiled=True)
    mine = mine.reshape(slots, half)

    off = jnp.pad(key_offset.reshape(-1, LANES), ((0, 16 - len_ // LANES), (0, 0)))
    kvo = [jnp.concatenate([keys, values, off], axis=0)]
    for step in range(1, wide):
        kvo.append(lax.ppermute(kvo[0], "x", [(i, (i + step) % wide) for i in range(wide)]))
    q = lax.all_gather(queries, "z")

    hidden = gate_w.shape[2]
    other = swap(mine)
    keep, send = pl.pallas_call(
        expert_kernel,
        out_shape=(jax.ShapeDtypeStruct((hosts, slots, LANES), BF16),) * 2,
        in_specs=[SMEM] + vmem(5) + [ANY] * EXTRA1,
        out_specs=tuple(vmem(2)),
        scratch_shapes=[pltpu.VMEM((slots, width), BF16)],
        compiler_params=pltpu.CompilerParams(vmem_limit_bytes=32 << 20),
        cost_estimate=pl.CostEstimate(
            flops=6 * slots * width * hidden,
            transcendentals=slots * hidden,
            bytes_accessed=2 * (2 * slots * width + 3 * width * hidden),
        ),
        name="experts",
    )(core, mine, other, gate_w[0].T, up_w[0].T, down_w[0], *([q] * EXTRA1))
    other = swap(send)
    share = (keep.astype(F32) + other.astype(F32)).astype(BF16)
    share = lax.all_to_all(share, "y", 0, 0, tiled=True)

    sums = pl.pallas_call(
        functools.partial(block_kernel, depth, wide, len_, hd),
        out_shape=jax.ShapeDtypeStruct((depth, len_ + 16, hd), BF16),
        in_specs=[SMEM] + vmem(1 + wide),
        out_specs=vmem(1)[0],
        scratch_shapes=[
            pltpu.VMEM((wide, 2 * len_ + 16, hd), BF16),
            pltpu.VMEM((len_, len_), BF16),
            pltpu.VMEM((len_, LANES), F32),
            pltpu.VMEM((len_, hd), F32),
            pltpu.VMEM((len_, LANES), F32),
        ],
        compiler_params=pltpu.CompilerParams(vmem_limit_bytes=32 << 20),
        cost_estimate=pl.CostEstimate(
            flops=depth * wide * len_ * len_ * (4 * hd + 2 * len_),
            transcendentals=3 * depth * wide * len_ * len_,
            bytes_accessed=2 * (2 * depth * len_ * hd + wide * kvo[0].size),
        ),
        name="stick_blocks",
    )(place, q, *kvo)
    arrived = lax.all_to_all(sums, "z", 0, 0, tiled=True)
    attended = pl.pallas_call(
        functools.partial(join_kernel, depth, len_),
        out_shape=jax.ShapeDtypeStruct((len_, hd), BF16),
        in_specs=vmem(1),
        out_specs=vmem(1)[0],
        scratch_shapes=[pltpu.VMEM((LANES, len_), F32)],
        cost_estimate=pl.CostEstimate(
            flops=2 * depth * len_ * hd, transcendentals=depth * len_, bytes_accessed=2 * depth * len_ * hd
        ),
        name="stick_join",
    )(arrived)

    share = pl.pallas_call(
        sum_kernel,
        out_shape=jax.ShapeDtypeStruct((slots, LANES), BF16),
        in_specs=vmem(1) + [ANY] * EXTRA2,
        out_specs=vmem(1)[0],
        name="parts_sum",
    )(share, *([sums] * EXTRA2))
    back = lax.all_to_all(share.reshape(experts, cap, LANES), EP, 0, 0, tiled=True)
    mixed = pl.pallas_call(
        combine_kernel,
        out_shape=jax.ShapeDtypeStruct((tok, LANES), BF16),
        in_specs=vmem(3),
        out_specs=vmem(1)[0],
        name="combine",
    )(hi, lo, back.reshape(slots, LANES))
    mixed = lax.all_gather(mixed, TP, axis=1, tiled=True)
    return (attended, mixed)


def solution(mesh):
    fine = Mesh(mesh.devices.reshape(Z, X, Y, CORE), ("z", "x", "y", "core"))
    return jax.shard_map(
        layer,
        mesh=fine,
        in_specs=(
            P(EP, TP),
            P(EP, TP),
            P(EP, TP),
            P(EP, TP),
            P(EP, None),
            P(),
            P(EP, None, TP),
            P(EP, None, TP),
            P(EP, TP, None),
            P(EP, None),
            P(EP, None),
        ),
        out_specs=(P(EP, TP), P(EP, None)),
        check_vma=False,
    )
```

time: 197 us -> 189 us (0.959)
  blocking collectives: 106 us -> 86.3 us
  starting transfers between devices: 23 us -> 33.8 us
  Pallas kernels: 31.7 us -> 35.5 us
  local copies, waits for them, and re-layouts: 4.97 us -> 2.65 us
    all_gather x3 -> x2, blocking collectives: 65.6 us -> 46.3 us  [the longest x1 24.7 us: layer(): mixed = lax.all_gather(mixed, TP, axis=1, tiled=True)]
    ppermute x0 -> x3, starting transfers between devices: none -> 10.8 us  [layer(): lax.ppermute(kvo[0], 'x', [(i, (i + step) % wide) for i in range(wide)])]
    pallas_call x4 -> x6, Pallas kernels: 31.7 us -> 35.5 us  [the longest x1 23.4 us: layer(): pl.pallas_call(functools.partial(block_kernel, depth, wide, len_, hd), ou...]
    unnamed x23 -> x21, local copies, waits for them, and re-layouts: 4.21 us -> 2.65 us
  transfers between devices with their start and end apart: 5 -> 8, of which waited for: 4 -> 4; matrix products, arithmetic and copies ran while one was open for 1% -> 0% of each run, Pallas kernels for 13% -> 15%
where the time goes in v3:
time: 189 us; the launch traced here: 188 us
  blocking collectives  86.3 us (46%)
  Pallas kernels  35.5 us (19%)
  starting transfers between devices  33.8 us (18%)
  waiting for transfers between devices  27.9 us (15%)
  local copies, waits for them, and re-layouts  2.65 us (1%)
    all_to_all x1, blocking collectives, layer(): lax.all_to_all(outgoing.reshape(experts, cap, half), EP, 0, 0, tiled=True)  40 us
    all_gather x1, blocking collectives, layer(): mixed = lax.all_gather(mixed, TP, axis=1, tiled=True)  24.7 us
    pallas_call x1, Pallas kernels, layer(): pl.pallas_call(functools.partial(block_kernel, depth, wide, len_, hd), ou...  23.4 us
    all_gather x1, blocking collectives, layer(): q = lax.all_gather(queries, 'z')  21.6 us
    all_to_all x1, waiting for transfers between devices, layer(): arrived = lax.all_to_all(sums, 'z', 0, 0, tiled=True)  16.5 us
    ppermute x3, starting transfers between devices, layer(): lax.ppermute(kvo[0], 'x', [(i, (i + step) % wide) for i in range(wide)])  10.8 us
    ppermute x2, starting transfers between devices, swap(): return lax.ppermute(x, 'core', [(0, 1), (1, 0)])  6.99 us
    all_to_all x1, starting transfers between devices, layer(): share = lax.all_to_all(share, 'y', 0, 0, tiled=True)  6.96 us
  transfers between devices with their start and end apart: 8, of which 4 were waited for; matrix products, arithmetic and copies ran while one was open for 0% of the time, Pallas kernels for 15%

profile of v3, /device:TPU:1, one launch (start us, length us, event | category | flops | bytes accessed | tf_op | source)
XLA Modules:
  0.0 188.3 jit_solution(3167991929808905073)
XLA Ops:
  0.6 2.8 %dispatch.1 = (bf16[512,1024]{1,0:T(8,128)(2,1)}, bf16[512,128]{1,0:T(8,128)(2,1)}, bf16[512,128]{1,0:T(8,128)(2,1)}) custom-call(s32[1]{0:T(128)} %bitcast.3.at_ref, bf16[128,2048]{1,0:T(8,128)(2,1)} %rows_ref.1, f32[1,2048]{1,0:T(1,128)} %bitcast.28, s32[2,128]{1,0:T(2,128)} %bitcast.30, f32[2,128]{1,0:T(2,128)} %bitcast.31), custom_call_target="tpu_custom_call" | custom-call | tf_op jit(solution)/shard_map/dispatch/pallas_call | solution.py:212
  3.4 0.0 copy-start
  3.4 0.0 copy-start.1
  3.4 40.0 %all_to_all.20 = bf16[32,16,1024]{2,1,0:T(8,128)(2,1)S(1)} all-to-all(bf16[32,16,1024]{2,1,0:T(8,128)(2,1)} %bitcast.25), channel_id=1, replica_groups=mesh['z'=8,'x'=4,'y'=8,'core'=2] {'z','x'}, dimensions={0} | all-to-all | bytes 2097152 | tf_op jit(solution)/shard_map/all_to_all | solution.py:223
  43.5 4.7 %collective-permute-start.3 = (bf16[512,1024]{1,0:T(8,128)(2,1)S(1)}, bf16[512,1024]{1,0:T(8,128)(2,1)S(1)}, u32[]{:S(2)}, u32[]{:S(2)}) collective-permute-start(bf16[512,1024]{1,0:T(8,128)(2,1)S(1)} %bitcast.19), channel_id=1, source_target_pairs={{0,1},{1,0},{2,3},{3,2},{4,5},{5,4},{6,7},{7,6},{8,9},{9,8},{10,11... | collective-permute-start | bytes 3145736 | tf_op jit(solution)/shard_map/ppermute | solution.py:193
  48.2 2.3 %collective-permute-done.3.other_ref = bf16[512,1024]{1,0:T(8,128)(2,1)S(1)} collective-permute-done((bf16[512,1024]{1,0:T(8,128)(2,1)S(1)}, bf16[512,1024]{1,0:T(8,128)(2,1)S(1)}, u32[]{:S(2)}, u32[]{:S(2)}) %collective-permute-start.3) | collective-permute-done | bytes 1048608 | tf_op jit(solution)/shard_map/ppermute | solution.py:193
  50.4 0.0 copy-done
  50.4 0.0 copy-done.1
  50.4 0.0 copy-start.2
  50.4 1.2 copy-done.2
  51.6 2.9 %experts.1 = (bf16[8,512,128]{2,1,0:T(8,128)(2,1)S(1)}, bf16[8,512,128]{2,1,0:T(8,128)(2,1)S(1)}) custom-call(s32[1]{0:T(128)} %bitcast.3.at_ref, bf16[512,1024]{1,0:T(8,128)(2,1)S(1)} %bitcast.20, bf16[512,1024]{1,0:T(8,128)(2,1)S(1)} %collective-permute-done.3.other_ref, bf16[224,2048]{1,0:T(8,128)(2,1)S(1)} %bitcast.22, bf16[224,2048]{1,0:T(8,128)(2,1)S(1)} %bitcast.23, ...), custom_call_target="tpu_custom_call" | custom-call | flops 1409286144 | bytes 6946816 | tf_op jit(solution)/shard_map/experts/pallas_call | solution.py:234
  54.5 2.3 %collective-permute-start.4 = (bf16[8,512,128]{2,1,0:T(8,128)(2,1)S(1)}, bf16[8,512,128]{2,1,0:T(8,128)(2,1)S(1)}, u32[]{:S(2)}, u32[]{:S(2)}) collective-permute-start(bf16[8,512,128]{2,1,0:T(8,128)(2,1)S(1)} %get-tuple-element.11), channel_id=1, source_target_pairs={{0,1},{1,0},{2,3},{3,2},{4,5},{5,4},{6,7},{7,6},{8,9},{9,8},{10,11... | collective-permute-start | bytes 3145736 | tf_op jit(solution)/shard_map/ppermute | solution.py:193
  56.8 2.3 %collective-permute-done.4 = bf16[8,512,128]{2,1,0:T(8,128)(2,1)S(1)} collective-permute-done((bf16[8,512,128]{2,1,0:T(8,128)(2,1)S(1)}, bf16[8,512,128]{2,1,0:T(8,128)(2,1)S(1)}, u32[]{:S(2)}, u32[]{:S(2)}) %collective-permute-start.4) | collective-permute-done | bytes 1048608 | tf_op jit(solution)/shard_map/ppermute | solution.py:193
  59.1 1.3 add_convert_fusion
  60.4 0.0 copy-start.9
  60.4 0.0 copy-start.7
  60.4 0.0 copy-start.8
  60.4 0.0 copy-start.6
  60.4 7.0 %all-to-all-start.2 = ((bf16[8,512,128]{2,1,0:T(8,128)(2,1)}), bf16[8,512,128]{2,1,0:T(8,128)(2,1)S(1)}, u32[]{:S(2)}, u32[]{:S(2)}) async-start(bf16[8,512,128]{2,1,0:T(8,128)(2,1)} %add_convert_fusion), calls=%async_computation.2 | async-start | bytes 2097152 | tf_op jit(solution)/shard_map/all_to_all | solution.py:250
  67.3 0.0 copy-done.9
  67.4 0.0 copy-done.7
  67.4 0.0 copy-done.8
  67.4 3.4 %collective-permute-start = (bf16[784,128]{1,0:T(8,128)(2,1)S(1)}, bf16[784,128]{1,0:T(8,128)(2,1)S(1)}, u32[]{:S(2)}, u32[]{:S(2)}) collective-permute-start(bf16[784,128]{1,0:T(8,128)(2,1)S(1)} %fusion.1.refs_0_), channel_id=1, source_target_pairs={{0,16},{16,32},{32,48},{48,0},{1,17},{17,33},{33,49},{49,1},{2,18}... | collective-permute-start | bytes 602120 | tf_op jit(solution)/shard_map/ppermute | solution.py:229
  70.8 4.3 %collective-permute-start.1 = (bf16[784,128]{1,0:T(8,128)(2,1)S(1)}, bf16[784,128]{1,0:T(8,128)(2,1)S(1)}, u32[]{:S(2)}, u32[]{:S(2)}) collective-permute-start(bf16[784,128]{1,0:T(8,128)(2,1)S(1)} %fusion.1.refs_0_), channel_id=1, source_target_pairs={{0,32},{16,48},{32,0},{48,16},{1,33},{17,49},{33,1},{49,17},{2,34}... | collective-permute-start | bytes 602120 | tf_op jit(solution)/shard_map/ppermute | solution.py:229
  75.2 3.1 %collective-permute-start.2 = (bf16[784,128]{1,0:T(8,128)(2,1)S(1)}, bf16[784,128]{1,0:T(8,128)(2,1)S(1)}, u32[]{:S(2)}, u32[]{:S(2)}) collective-permute-start(bf16[784,128]{1,0:T(8,128)(2,1)S(1)} %fusion.1.refs_0_), channel_id=1, source_target_pairs={{0,48},{16,0},{32,16},{48,32},{1,49},{17,1},{33,17},{49,33},{2,50}... | collective-permute-start | bytes 602120 | tf_op jit(solution)/shard_map/ppermute | solution.py:229
  78.3 0.0 copy-done.6
  78.3 21.6 %all-gather = bf16[3072,128]{1,0:T(8,128)(2,1)S(1)} all-gather(bf16[384,128]{1,0:T(8,128)(2,1)S(1)} %copy-done.6), channel_id=2, replica_groups=mesh['z'=8,'x'=4,'y'=8,'core'=2] {'z'}, dimensions={0}, use_global_device_ids=true | all-gather | bytes 884736 | tf_op jit(solution)/shard_map/all_gather | solution.py:230
  99.9 0.1 pad_add_fusion.at_ref
  100.0 0.0 collective-permute-done.refs_1_
  100.0 0.0 collective-permute-done.1.refs_2_
  100.0 0.0 collective-permute-done.2.refs_3_
  100.0 23.4 %stick_blocks.1 = bf16[8,400,128]{2,1,0:T(8,128)(2,1)} custom-call(s32[2]{0:T(128)S(1)} %pad_add_fusion.at_ref, bf16[8,384,128]{2,1,0:T(8,128)(2,1)S(1)} %bitcast.21, bf16[784,128]{1,0:T(8,128)(2,1)S(1)} %fusion.1.refs_0_, bf16[784,128]{1,0:T(8,128)(2,1)S(1)} %collective-permute-done.refs_1_, bf16[784,128]{1,0:T(8,128)(2,1)S(1)} %collective-permute-done.1.refs_2_, ...), custom_call_target="tpu_custom_call" | custom-call | flops 6039797760 | bytes 2375680 | tf_op jit(solution)/shard_map/stick_blocks/pallas_call | solution.py:252
  123.4 0.0 all-to-all-done.2.in_ref
  123.4 0.0 copy-start.3
  123.4 3.5 %all-to-all-start = ((bf16[8,400,128]{2,1,0:T(8,128)(2,1)}), bf16[8,400,128]{2,1,0:T(8,128)(2,1)S(1)}, u32[]{:S(2)}, u32[]{:S(2)}) async-start(bf16[8,400,128]{2,1,0:T(8,128)(2,1)} %stick_blocks.1), calls=%async_computation | async-start | bytes 1638400 | tf_op jit(solution)/shard_map/all_to_all | solution.py:272
  127.0 0.0 copy-done.3
  127.0 2.0 %parts_sum.1 = bf16[512,128]{1,0:T(8,128)(2,1)} custom-call(bf16[8,512,128]{2,1,0:T(8,128)(2,1)} %copy-done.3), custom_call_target="tpu_custom_call" | custom-call | tf_op jit(solution)/shard_map/parts_sum/pallas_call | solution.py:285
  129.0 16.5 %all-to-all-done.in_ref = bf16[8,400,128]{2,1,0:T(8,128)(2,1)S(1)} async-done(((bf16[8,400,128]{2,1,0:T(8,128)(2,1)}), bf16[8,400,128]{2,1,0:T(8,128)(2,1)S(1)}, u32[]{:S(2)}, u32[]{:S(2)}) %all-to-all-start) | async-done | bytes 819232 | tf_op jit(solution)/shard_map/all_to_all | solution.py:272
  145.5 0.0 copy-start.4
  145.5 5.5 %all-to-all-start.3 = ((bf16[32,16,128]{2,1,0:T(8,128)(2,1)}), bf16[32,16,128]{2,1,0:T(8,128)(2,1)S(1)}, u32[]{:S(2)}, u32[]{:S(2)}) async-start(bf16[32,16,128]{2,1,0:T(8,128)(2,1)} %bitcast.26), calls=%async_computation.3 | async-start | bytes 262144 | tf_op jit(solution)/shard_map/all_to_all | solution.py:292
  151.0 0.0 copy-done.4
  151.0 2.5 %stick_join.1 = bf16[384,128]{1,0:T(8,128)(2,1)} custom-call(bf16[8,400,128]{2,1,0:T(8,128)(2,1)} %copy-done.4), custom_call_target="tpu_custom_call" | custom-call | flops 786432 | bytes 786432 | tf_op jit(solution)/shard_map/stick_join/pallas_call | solution.py:273
  153.5 6.9 %all-to-all-done.3 = bf16[32,16,128]{2,1,0:T(8,128)(2,1)S(1)} async-done(((bf16[32,16,128]{2,1,0:T(8,128)(2,1)}), bf16[32,16,128]{2,1,0:T(8,128)(2,1)S(1)}, u32[]{:S(2)}, u32[]{:S(2)}) %all-to-all-start.3) | async-done | bytes 131104 | tf_op jit(solution)/shard_map/all_to_all | solution.py:292
  160.3 0.0 copy-start.5
  160.3 0.6 copy-done.5
  161.0 1.9 %combine.1 = bf16[128,128]{1,0:T(8,128)(2,1)} custom-call(bf16[512,128]{1,0:T(8,128)(2,1)} %get-tuple-element.7.hi_ref, bf16[512,128]{1,0:T(8,128)(2,1)} %get-tuple-element.8.lo_ref, bf16[512,128]{1,0:T(8,128)(2,1)} %bitcast.27), custom_call_target="tpu_custom_call" | custom-call | tf_op jit(solution)/shard_map/combine/pallas_call | solution.py:293
  162.9 24.7 %all_gather.11 = bf16[128,2048]{1,0:T(8,128)(2,1)S(1)} all-gather(bf16[128,128]{1,0:T(8,128)(2,1)} %combine.1), channel_id=1, replica_groups=mesh['z'=8,'x'=4,'y'=8,'core'=2] {'y','core'}, dimensions={1}, use_global_device_ids=true | all-gather | bytes 557056 | tf_op jit(solution)/shard_map/all_gather | solution.py:300
  187.6 0.8 copy.14
  (2 shorter events, 0.0 us)
Async XLA Ops:
  3.4 47.0 %copy-start = (bf16[1,2048,224]{1,2,0:T(8,128)(2,1)S(1)}, bf16[1,2048,224]{1,2,0:T(8,128)(2,1)}, u32[]{:S(2)}) copy-start(bf16[1,2048,224]{1,2,0:T(8,128)(2,1)} %param.17) | copy-start | bytes 2752516
  3.4 47.0 %copy-start.1 = (bf16[1,2048,224]{1,2,0:T(8,128)(2,1)S(1)}, bf16[1,2048,224]{1,2,0:T(8,128)(2,1)}, u32[]{:S(2)}) copy-start(bf16[1,2048,224]{1,2,0:T(8,128)(2,1)} %param.18) | copy-start | bytes 2752516
  43.5 7.0 %collective-permute-start.3 = (bf16[512,1024]{1,0:T(8,128)(2,1)S(1)}, bf16[512,1024]{1,0:T(8,128)(2,1)S(1)}, u32[]{:S(2)}, u32[]{:S(2)}) collective-permute-start(bf16[512,1024]{1,0:T(8,128)(2,1)S(1)} %bitcast.19), channel_id=1, source_target_pairs={{0,1},{1,0},{2,3},{3,2},{4,5},{5,4},{6,7},{7,6},{8,9},{9,8},{10,11... | collective-permute-start | bytes 3145736 | tf_op jit(solution)/shard_map/ppermute | solution.py:193
  50.4 1.2 copy-start.2
  54.5 4.6 %collective-permute-start.4 = (bf16[8,512,128]{2,1,0:T(8,128)(2,1)S(1)}, bf16[8,512,128]{2,1,0:T(8,128)(2,1)S(1)}, u32[]{:S(2)}, u32[]{:S(2)}) collective-permute-start(bf16[8,512,128]{2,1,0:T(8,128)(2,1)S(1)} %get-tuple-element.11), channel_id=1, source_target_pairs={{0,1},{1,0},{2,3},{3,2},{4,5},{5,4},{6,7},{7,6},{8,9},{9,8},{10,11... | collective-permute-start | bytes 3145736 | tf_op jit(solution)/shard_map/ppermute | solution.py:193
  60.4 7.0 %copy-start.9 = (bf16[384,1]{0,1:T(2,128)(2,1)S(1)}, bf16[384,1]{0,1:T(2,128)(2,1)}, u32[]{:S(2)}) copy-start(bf16[384,1]{0,1:T(2,128)(2,1)} %param.14) | copy-start | bytes 2308
  60.4 7.0 %copy-start.7 = (bf16[384,128]{1,0:T(8,128)(2,1)S(1)}, bf16[384,128]{1,0:T(8,128)(2,1)}, u32[]{:S(2)}) copy-start(bf16[384,128]{1,0:T(8,128)(2,1)} %param.13) | copy-start | bytes 294916
  60.4 7.0 %copy-start.8 = (bf16[384,128]{1,0:T(8,128)(2,1)S(1)}, bf16[384,128]{1,0:T(8,128)(2,1)}, u32[]{:S(2)}) copy-start(bf16[384,128]{1,0:T(8,128)(2,1)} %param.12) | copy-start | bytes 294916
  60.4 17.9 %copy-start.6 = (bf16[384,128]{1,0:T(8,128)(2,1)S(1)}, bf16[384,128]{1,0:T(8,128)(2,1)}, u32[]{:S(2)}) copy-start(bf16[384,128]{1,0:T(8,128)(2,1)} %param.11) | copy-start | bytes 294916
  60.4 63.0 %all-to-all-start.2 = ((bf16[8,512,128]{2,1,0:T(8,128)(2,1)}), bf16[8,512,128]{2,1,0:T(8,128)(2,1)S(1)}, u32[]{:S(2)}, u32[]{:S(2)}) async-start(bf16[8,512,128]{2,1,0:T(8,128)(2,1)} %add_convert_fusion), calls=%async_computation.2 | async-start | bytes 2097152 | tf_op jit(solution)/shard_map/all_to_all | solution.py:250
  67.4 32.6 %collective-permute-start = (bf16[784,128]{1,0:T(8,128)(2,1)S(1)}, bf16[784,128]{1,0:T(8,128)(2,1)S(1)}, u32[]{:S(2)}, u32[]{:S(2)}) collective-permute-start(bf16[784,128]{1,0:T(8,128)(2,1)S(1)} %fusion.1.refs_0_), channel_id=1, source_target_pairs={{0,16},{16,32},{32,48},{48,0},{1,17},{17,33},{33,49},{49,1},{2,18}... | collective-permute-start | bytes 602120 | tf_op jit(solution)/shard_map/ppermute | solution.py:229
  70.8 29.1 %collective-permute-start.1 = (bf16[784,128]{1,0:T(8,128)(2,1)S(1)}, bf16[784,128]{1,0:T(8,128)(2,1)S(1)}, u32[]{:S(2)}, u32[]{:S(2)}) collective-permute-start(bf16[784,128]{1,0:T(8,128)(2,1)S(1)} %fusion.1.refs_0_), channel_id=1, source_target_pairs={{0,32},{16,48},{32,0},{48,16},{1,33},{17,49},{33,1},{49,17},{2,34}... | collective-permute-start | bytes 602120 | tf_op jit(solution)/shard_map/ppermute | solution.py:229
  75.2 24.8 %collective-permute-start.2 = (bf16[784,128]{1,0:T(8,128)(2,1)S(1)}, bf16[784,128]{1,0:T(8,128)(2,1)S(1)}, u32[]{:S(2)}, u32[]{:S(2)}) collective-permute-start(bf16[784,128]{1,0:T(8,128)(2,1)S(1)} %fusion.1.refs_0_), channel_id=1, source_target_pairs={{0,48},{16,0},{32,16},{48,32},{1,49},{17,1},{33,17},{49,33},{2,50}... | collective-permute-start | bytes 602120 | tf_op jit(solution)/shard_map/ppermute | solution.py:229
  123.4 3.6 %copy-start.3 = (bf16[8,512,128]{2,1,0:T(8,128)(2,1)}, bf16[8,512,128]{2,1,0:T(8,128)(2,1)S(1)}, u32[]{:S(2)}) copy-start(bf16[8,512,128]{2,1,0:T(8,128)(2,1)S(1)} %all-to-all-done.2.in_ref) | copy-start | bytes 3145732
  123.4 22.1 %all-to-all-start = ((bf16[8,400,128]{2,1,0:T(8,128)(2,1)}), bf16[8,400,128]{2,1,0:T(8,128)(2,1)S(1)}, u32[]{:S(2)}, u32[]{:S(2)}) async-start(bf16[8,400,128]{2,1,0:T(8,128)(2,1)} %stick_blocks.1), calls=%async_computation | async-start | bytes 1638400 | tf_op jit(solution)/shard_map/all_to_all | solution.py:272
  145.5 5.5 %copy-start.4 = (bf16[8,400,128]{2,1,0:T(8,128)(2,1)}, bf16[8,400,128]{2,1,0:T(8,128)(2,1)S(1)}, u32[]{:S(2)}) copy-start(bf16[8,400,128]{2,1,0:T(8,128)(2,1)S(1)} %all-to-all-done.in_ref) | copy-start | bytes 2457604
  145.5 14.8 %all-to-all-start.3 = ((bf16[32,16,128]{2,1,0:T(8,128)(2,1)}), bf16[32,16,128]{2,1,0:T(8,128)(2,1)S(1)}, u32[]{:S(2)}, u32[]{:S(2)}) async-start(bf16[32,16,128]{2,1,0:T(8,128)(2,1)} %bitcast.26), calls=%async_computation.3 | async-start | bytes 262144 | tf_op jit(solution)/shard_map/all_to_all | solution.py:292
  160.3 0.6 copy-start.5

commit v4 on v3

--- a/solution.py
+++ b/solution.py
@@ -13,12 +13,11 @@
 LOG2E = 1.4426950408889634
 F32 = jnp.float32
 BF16 = jnp.bfloat16
-EXTRA1 = 0
-EXTRA2 = 0
 Z, X, Y, CORE = 8, 4, 8, 2
 EP = ("z", "x")
 TP = ("y", "core")
 LANES = 128
+TILE = 256
 
 
 def dot(a, b, dims=((1,), (0,))):
@@ -26,61 +25,84 @@
 
 
 def block_kernel(depth, width, len_, hd, at_ref, q_ref, *refs):
-    near, (out_ref, kvo_ref, tri_ref, tot_ref, acc_ref, carry_ref) = refs[:width], refs[width:]
+    near, (out_ref, qq_ref, kk_ref, v_ref, off_ref, tri_ref, tot_ref, acc_ref, carry_ref) = (
+        refs[:width],
+        refs[width:],
+    )
     z, x = at_ref[0], at_ref[1]
+    n_off = len_ // LANES
+    half = width * len_ // 2
     for step in range(width):
-        kvo_ref[(x + width - step) % width] = near[step][...]
-    c = hd**-0.5 * LOG2E
-    rows_i = lax.broadcasted_iota(jnp.int32, (len_, len_), 0)
-    cols_i = lax.broadcasted_iota(jnp.int32, (len_, len_), 1)
-    tri_ref[...] = jnp.where(rows_i > cols_i, -1.0, 0.0).astype(BF16)
+        rows = pl.ds(pl.multiple_of((x + width - step) % width * len_, len_), len_)
+        for twice in range(2):
+            kk_ref[rows, twice * hd : (twice + 1) * hd] = near[step][:len_, :]
+        v_ref[rows, :] = near[step][len_ : 2 * len_, :]
+        o = near[step][2 * len_ :, :].astype(F32) * LOG2E
+        for i in range(n_off):
+            at = pl.ds(pl.multiple_of(((x + width - step) % width * n_off + i) * LANES, LANES), LANES)
+            off_ref[0:1, at] = o[i : i + 1, :]
+
+    def scale(i, done):
+        q = q_ref[i].astype(F32) * (hd**-0.5 * LOG2E)
+        hi = q.astype(BF16)
+        qq_ref[i, :, :hd] = hi
+        qq_ref[i, :, hd:] = (q - hi.astype(F32)).astype(BF16)
+        return done
+
+    lax.fori_loop(z, depth, scale, 0)
+    tri_ref[...] = jnp.where(
+        lax.broadcasted_iota(jnp.int32, (TILE, TILE), 0) > lax.broadcasted_iota(jnp.int32, (TILE, TILE), 1),
+        -1.0,
+        0.0,
+    ).astype(BF16)
     tot_ref[...] = jnp.zeros_like(tot_ref)
     lane = lax.broadcasted_iota(jnp.int32, (len_, LANES), 1)
-    n_off = len_ // LANES
-
-    def pair(to, k_at, old, masked):
-        q = q_ref[to]
-        k = kvo_ref[k_at, pl.ds(0, len_), :]
-        v = kvo_ref[k_at, pl.ds(len_, len_), :]
-        o = kvo_ref[k_at, pl.ds(2 * len_, 16), :].astype(F32)
-        off = jnp.concatenate([o[i : i + 1, :] for i in range(n_off)], axis=1) * LOG2E
-        u = dot(q, k, ((1,), (1,))) * c + off
-        sp = kept = jnp.maximum(u, 0.0) + jnp.log2(1.0 + jnp.exp2(-jnp.abs(u)))
-        if masked:
-            strict = cols_i < rows_i
-            kept = jnp.where(strict, sp, 0.0)
-        w = dot(kept.astype(BF16), tri_ref[...])
-        p = jnp.exp2(u - sp + w)
-        if masked:
-            p = jnp.where(strict, p, 0.0)
-        total = jnp.broadcast_to(w[:, 0:1] - kept[:, 0:1], (len_, LANES))
-        summed = dot(p.astype(BF16), v)
-        if masked:
-            acc, carry = summed, total
-        else:
-            carry = carry_ref[...] * old
-            acc = acc_ref[...] * old + jnp.exp2(carry) * summed
-            carry = carry + total
+
+    def part(to, which, old, masked):
+        start = pl.multiple_of(which * half, half)
+        q = qq_ref[to]
+        carry = 0.0 if masked else carry_ref[...] * old
+        acc = 0.0 if masked else acc_ref[...] * old
+        for tile in reversed(range(half // TILE)):
+            keys = pl.ds(pl.multiple_of(start + tile * TILE, TILE), TILE)
+            u = dot(q, kk_ref[keys, :], ((1,), (1,))) + off_ref[0:1, keys]
+            sp = kept = jnp.maximum(u, 0.0) + jnp.log2(1.0 + jnp.exp2(-jnp.abs(u)))
+            if masked:
+                ahead = lax.broadcasted_iota(jnp.int32, (len_, TILE), 0) - lax.broadcasted_iota(
+                    jnp.int32, (len_, TILE), 1
+                )
+                strict = ahead > start + tile * TILE - x * len_
+                kept = jnp.where(strict, sp, 0.0)
+            w = dot(kept.astype(BF16), tri_ref[...])
+            if isinstance(carry, float):
+                p = jnp.exp2(u - sp + w)
+            else:
+                p = jnp.exp2(u - sp + w + jnp.concatenate([carry] * (TILE // LANES), axis=1))
+            if masked:
+                p = jnp.where(strict, p, 0.0)
+            acc = acc + dot(p.astype(BF16), v_ref[keys, :])
+            carry = carry + jnp.broadcast_to(w[:, 0:1] - kept[:, 0:1], (len_, LANES))
         carry_ref[...] = carry
         acc_ref[...] = acc
         out_ref[to, pl.ds(0, len_), :] = acc.astype(BF16)
         tot_ref[...] = jnp.where(lane == to, carry, tot_ref[...])
 
-    pair(z, x, None, True)
+    own = x * len_ // half
+    part(z, own, None, True)
 
     def full(i, done):
-        own = i < x
-        j = i - x
-        fresh = jnp.logical_and(jnp.logical_not(own), j % width == 0)
-        pair(
-            jnp.where(own, z, z + 1 + j // width),
-            jnp.where(own, x - 1 - i, width - 1 - j % width),
+        j = i - own
+        before = i < own
+        fresh = jnp.logical_and(jnp.logical_not(before), j % 2 == 0)
+        part(
+            jnp.where(before, z, z + 1 + j // 2),
+            jnp.where(before, 0, 1 - j % 2),
             jnp.where(fresh, 0.0, 1.0),
             False,
         )
         return done
 
-    lax.fori_loop(0, x + width * (depth - 1 - z), full, 0)
+    lax.fori_loop(0, own + 2 * (depth - 1 - z), full, 0)
 
     def clear(i, done):
         out_ref[i, pl.ds(0, len_), :] = jnp.zeros((len_, hd), BF16)
@@ -156,8 +178,7 @@
     lo_ref[...] = (weight - hi.astype(F32)).astype(BF16)
 
 
-def expert_kernel(at_ref, mine_ref, other_ref, gate_ref, up_ref, down_ref, *rest):
-    keep_ref, send_ref, all_ref = rest[-3:]
+def expert_kernel(at_ref, mine_ref, other_ref, gate_ref, up_ref, down_ref, keep_ref, send_ref, all_ref):
     core = at_ref[0]
     chunks = mine_ref.shape[1] // LANES
     for i in range(chunks):
@@ -174,8 +195,7 @@
         send_ref[i] = all_ref[:, pl.ds(pl.multiple_of((2 * i + 1 - core) * LANES, LANES), LANES)]
 
 
-def sum_kernel(in_ref, *rest):
-    out_ref = rest[-1]
+def sum_kernel(in_ref, out_ref):
     total = in_ref[0].astype(F32)
     for i in range(1, in_ref.shape[0]):
         total = total + in_ref[i].astype(F32)
@@ -191,9 +211,6 @@
 
 def swap(x):
     return lax.ppermute(x, "core", [(0, 1), (1, 0)])
-
-
-ANY = pl.BlockSpec(memory_space=pl.ANY)
 
 
 def layer(
@@ -234,7 +251,7 @@
     keep, send = pl.pallas_call(
         expert_kernel,
         out_shape=(jax.ShapeDtypeStruct((hosts, slots, LANES), BF16),) * 2,
-        in_specs=[SMEM] + vmem(5) + [ANY] * EXTRA1,
+        in_specs=[SMEM] + vmem(5),
         out_specs=tuple(vmem(2)),
         scratch_shapes=[pltpu.VMEM((slots, width), BF16)],
         compiler_params=pltpu.CompilerParams(vmem_limit_bytes=32 << 20),
@@ -244,7 +261,7 @@
             bytes_accessed=2 * (2 * slots * width + 3 * width * hidden),
         ),
         name="experts",
-    )(core, mine, other, gate_w[0].T, up_w[0].T, down_w[0], *([q] * EXTRA1))
+    )(core, mine, other, gate_w[0].T, up_w[0].T, down_w[0])
     other = swap(send)
     share = (keep.astype(F32) + other.astype(F32)).astype(BF16)
     share = lax.all_to_all(share, "y", 0, 0, tiled=True)
@@ -255,8 +272,11 @@
         in_specs=[SMEM] + vmem(1 + wide),
         out_specs=vmem(1)[0],
         scratch_shapes=[
-            pltpu.VMEM((wide, 2 * len_ + 16, hd), BF16),
-            pltpu.VMEM((len_, len_), BF16),
+            pltpu.VMEM((depth, len_, 2 * hd), BF16),
+            pltpu.VMEM((wide * len_, 2 * hd), BF16),
+            pltpu.VMEM((wide * len_, hd), BF16),
+            pltpu.VMEM((8, wide * len_), F32),
+            pltpu.VMEM((TILE, TILE), BF16),
             pltpu.VMEM((len_, LANES), F32),
             pltpu.VMEM((len_, hd), F32),
             pltpu.VMEM((len_, LANES), F32),
@@ -285,10 +305,10 @@
     share = pl.pallas_call(
         sum_kernel,
         out_shape=jax.ShapeDtypeStruct((slots, LANES), BF16),
-        in_specs=vmem(1) + [ANY] * EXTRA2,
+        in_specs=vmem(1),
         out_specs=vmem(1)[0],
         name="parts_sum",
-    )(share, *([sums] * EXTRA2))
+    )(share)
     back = lax.all_to_all(share.reshape(experts, cap, LANES), EP, 0, 0, tiled=True)
     mixed = pl.pallas_call(
         combine_kernel,

time: 189 us -> 181 us (0.958)
  Pallas kernels: 35.5 us -> 28.7 us
    pallas_call x1, Pallas kernels: 23.4 us -> 16.7 us  [layer(): pl.pallas_call(functools.partial(block_kernel, depth, wide, len_, hd), ou...]
  transfers between devices with their start and end apart: 8 -> 8, of which waited for: 4 -> 4; matrix products, arithmetic and copies ran while one was open for 0% -> 0% of each run, Pallas kernels for 15% -> 12%
where the time goes in v4:
time: 181 us
  blocking collectives  86.7 us (48%)
  starting transfers between devices  32.5 us (18%)
  Pallas kernels  28.7 us (16%)
  waiting for transfers between devices  27.9 us (15%)
  local copies, waits for them, and re-layouts  2.65 us (1%)
    all_to_all x1, blocking collectives, layer(): lax.all_to_all(outgoing.reshape(experts, cap, half), EP, 0, 0, tiled=True)  40 us
    all_gather x1, blocking collectives, layer(): mixed = lax.all_gather(mixed, TP, axis=1, tiled=True)  25.1 us
    all_gather x1, blocking collectives, layer(): q = lax.all_gather(queries, 'z')  21.6 us
    pallas_call x1, Pallas kernels, layer(): pl.pallas_call(functools.partial(block_kernel, depth, wide, len_, hd), ou...  16.7 us
    all_to_all x1, waiting for transfers between devices, layer(): arrived = lax.all_to_all(sums, 'z', 0, 0, tiled=True)  16.5 us
    ppermute x3, starting transfers between devices, layer(): lax.ppermute(kvo[0], 'x', [(i, (i + step) % wide) for i in range(wide)])  10.8 us
    ppermute x2, starting transfers between devices, swap(): return lax.ppermute(x, 'core', [(0, 1), (1, 0)])  6.99 us
    all_to_all x1, starting transfers between devices, layer(): share = lax.all_to_all(share, 'y', 0, 0, tiled=True)  6.96 us
  transfers between devices with their start and end apart: 8, of which 4 were waited for; matrix products, arithmetic and copies ran while one was open for 0% of the time, Pallas kernels for 12%

profile of v4, /device:TPU:1, one launch (start us, length us, event | category | flops | bytes accessed | tf_op | source)
XLA Modules:
  0.0 180.7 jit_solution(19219158559629617)
XLA Ops:
  0.6 2.8 %dispatch.1 = (bf16[512,1024]{1,0:T(8,128)(2,1)}, bf16[512,128]{1,0:T(8,128)(2,1)}, bf16[512,128]{1,0:T(8,128)(2,1)}) custom-call(s32[1]{0:T(128)} %bitcast.3.at_ref, bf16[128,2048]{1,0:T(8,128)(2,1)} %rows_ref.1, f32[1,2048]{1,0:T(1,128)} %bitcast.28, s32[2,128]{1,0:T(2,128)} %bitcast.30, f32[2,128]{1,0:T(2,128)} %bitcast.31), custom_call_target="tpu_custom_call" | custom-call | tf_op jit(solution)/shard_map/dispatch/pallas_call | solution.py:229
  3.4 0.0 copy-start
  3.4 0.0 copy-start.1
  3.4 40.0 %all_to_all.20 = bf16[32,16,1024]{2,1,0:T(8,128)(2,1)S(1)} all-to-all(bf16[32,16,1024]{2,1,0:T(8,128)(2,1)} %bitcast.25), channel_id=1, replica_groups=mesh['z'=8,'x'=4,'y'=8,'core'=2] {'z','x'}, dimensions={0} | all-to-all | bytes 2097152 | tf_op jit(solution)/shard_map/all_to_all | solution.py:240
  43.5 4.7 %collective-permute-start.3 = (bf16[512,1024]{1,0:T(8,128)(2,1)S(1)}, bf16[512,1024]{1,0:T(8,128)(2,1)S(1)}, u32[]{:S(2)}, u32[]{:S(2)}) collective-permute-start(bf16[512,1024]{1,0:T(8,128)(2,1)S(1)} %bitcast.19), channel_id=1, source_target_pairs={{0,1},{1,0},{2,3},{3,2},{4,5},{5,4},{6,7},{7,6},{8,9},{9,8},{10,11... | collective-permute-start | bytes 3145736 | tf_op jit(solution)/shard_map/ppermute | solution.py:213
  48.2 2.3 %collective-permute-done.3.other_ref = bf16[512,1024]{1,0:T(8,128)(2,1)S(1)} collective-permute-done((bf16[512,1024]{1,0:T(8,128)(2,1)S(1)}, bf16[512,1024]{1,0:T(8,128)(2,1)S(1)}, u32[]{:S(2)}, u32[]{:S(2)}) %collective-permute-start.3) | collective-permute-done | bytes 1048608 | tf_op jit(solution)/shard_map/ppermute | solution.py:213
  50.4 0.0 copy-done
  50.4 0.0 copy-done.1
  50.4 0.0 copy-start.2
  50.4 1.2 copy-done.2
  51.6 2.9 %experts.1 = (bf16[8,512,128]{2,1,0:T(8,128)(2,1)S(1)}, bf16[8,512,128]{2,1,0:T(8,128)(2,1)S(1)}) custom-call(s32[1]{0:T(128)} %bitcast.3.at_ref, bf16[512,1024]{1,0:T(8,128)(2,1)S(1)} %bitcast.20, bf16[512,1024]{1,0:T(8,128)(2,1)S(1)} %collective-permute-done.3.other_ref, bf16[224,2048]{1,0:T(8,128)(2,1)S(1)} %bitcast.22, bf16[224,2048]{1,0:T(8,128)(2,1)S(1)} %bitcast.23, ...), custom_call_target="tpu_custom_call" | custom-call | flops 1409286144 | bytes 6946816 | tf_op jit(solution)/shard_map/experts/pallas_call | solution.py:251
  54.5 2.3 %collective-permute-start.4 = (bf16[8,512,128]{2,1,0:T(8,128)(2,1)S(1)}, bf16[8,512,128]{2,1,0:T(8,128)(2,1)S(1)}, u32[]{:S(2)}, u32[]{:S(2)}) collective-permute-start(bf16[8,512,128]{2,1,0:T(8,128)(2,1)S(1)} %get-tuple-element.11), channel_id=1, source_target_pairs={{0,1},{1,0},{2,3},{3,2},{4,5},{5,4},{6,7},{7,6},{8,9},{9,8},{10,11... | collective-permute-start | bytes 3145736 | tf_op jit(solution)/shard_map/ppermute | solution.py:213
  56.8 2.3 %collective-permute-done.4 = bf16[8,512,128]{2,1,0:T(8,128)(2,1)S(1)} collective-permute-done((bf16[8,512,128]{2,1,0:T(8,128)(2,1)S(1)}, bf16[8,512,128]{2,1,0:T(8,128)(2,1)S(1)}, u32[]{:S(2)}, u32[]{:S(2)}) %collective-permute-start.4) | collective-permute-done | bytes 1048608 | tf_op jit(solution)/shard_map/ppermute | solution.py:213
  59.1 1.3 add_convert_fusion
  60.4 0.0 copy-start.9
  60.4 0.0 copy-start.7
  60.4 0.0 copy-start.8
  60.4 0.0 copy-start.6
  60.4 7.0 %all-to-all-start.2 = ((bf16[8,512,128]{2,1,0:T(8,128)(2,1)}), bf16[8,512,128]{2,1,0:T(8,128)(2,1)S(1)}, u32[]{:S(2)}, u32[]{:S(2)}) async-start(bf16[8,512,128]{2,1,0:T(8,128)(2,1)} %add_convert_fusion), calls=%async_computation.2 | async-start | bytes 2097152 | tf_op jit(solution)/shard_map/all_to_all | solution.py:267
  67.3 0.0 copy-done.9
  67.4 0.0 copy-done.7
  67.4 0.0 copy-done.8
  67.4 3.4 %collective-permute-start = (bf16[784,128]{1,0:T(8,128)(2,1)S(1)}, bf16[784,128]{1,0:T(8,128)(2,1)S(1)}, u32[]{:S(2)}, u32[]{:S(2)}) collective-permute-start(bf16[784,128]{1,0:T(8,128)(2,1)S(1)} %fusion.1.refs_0_), channel_id=1, source_target_pairs={{0,16},{16,32},{32,48},{48,0},{1,17},{17,33},{33,49},{49,1},{2,18}... | collective-permute-start | bytes 602120 | tf_op jit(solution)/shard_map/ppermute | solution.py:246
  70.8 4.3 %collective-permute-start.1 = (bf16[784,128]{1,0:T(8,128)(2,1)S(1)}, bf16[784,128]{1,0:T(8,128)(2,1)S(1)}, u32[]{:S(2)}, u32[]{:S(2)}) collective-permute-start(bf16[784,128]{1,0:T(8,128)(2,1)S(1)} %fusion.1.refs_0_), channel_id=1, source_target_pairs={{0,32},{16,48},{32,0},{48,16},{1,33},{17,49},{33,1},{49,17},{2,34}... | collective-permute-start | bytes 602120 | tf_op jit(solution)/shard_map/ppermute | solution.py:246
  75.2 3.1 %collective-permute-start.2 = (bf16[784,128]{1,0:T(8,128)(2,1)S(1)}, bf16[784,128]{1,0:T(8,128)(2,1)S(1)}, u32[]{:S(2)}, u32[]{:S(2)}) collective-permute-start(bf16[784,128]{1,0:T(8,128)(2,1)S(1)} %fusion.1.refs_0_), channel_id=1, source_target_pairs={{0,48},{16,0},{32,16},{48,32},{1,49},{17,1},{33,17},{49,33},{2,50}... | collective-permute-start | bytes 602120 | tf_op jit(solution)/shard_map/ppermute | solution.py:246
  78.3 0.0 copy-done.6
  78.3 21.6 %all-gather = bf16[3072,128]{1,0:T(8,128)(2,1)S(1)} all-gather(bf16[384,128]{1,0:T(8,128)(2,1)S(1)} %copy-done.6), channel_id=2, replica_groups=mesh['z'=8,'x'=4,'y'=8,'core'=2] {'z'}, dimensions={0}, use_global_device_ids=true | all-gather | bytes 884736 | tf_op jit(solution)/shard_map/all_gather | solution.py:247
  99.9 0.1 pad_add_fusion.at_ref
  100.0 0.0 collective-permute-done.refs_1_
  100.0 0.0 collective-permute-done.1.refs_2_
  100.0 0.0 collective-permute-done.2.refs_3_
  100.0 16.7 %stick_blocks.1 = bf16[8,400,128]{2,1,0:T(8,128)(2,1)} custom-call(s32[2]{0:T(128)S(1)} %pad_add_fusion.at_ref, bf16[8,384,128]{2,1,0:T(8,128)(2,1)S(1)} %bitcast.21, bf16[784,128]{1,0:T(8,128)(2,1)S(1)} %fusion.1.refs_0_, bf16[784,128]{1,0:T(8,128)(2,1)S(1)} %collective-permute-done.refs_1_, bf16[784,128]{1,0:T(8,128)(2,1)S(1)} %collective-permute-done.1.refs_2_, ...), custom_call_target="tpu_custom_call" | custom-call | flops 6039797760 | bytes 2375680 | tf_op jit(solution)/shard_map/stick_blocks/pallas_call | solution.py:269
  116.7 0.0 all-to-all-done.2.in_ref
  116.7 0.0 copy-start.3
  116.7 3.5 %all-to-all-start = ((bf16[8,400,128]{2,1,0:T(8,128)(2,1)}), bf16[8,400,128]{2,1,0:T(8,128)(2,1)S(1)}, u32[]{:S(2)}, u32[]{:S(2)}) async-start(bf16[8,400,128]{2,1,0:T(8,128)(2,1)} %stick_blocks.1), calls=%async_computation | async-start | bytes 1638400 | tf_op jit(solution)/shard_map/all_to_all | solution.py:292
  120.2 0.0 copy-done.3
  120.2 2.0 %parts_sum.1 = bf16[512,128]{1,0:T(8,128)(2,1)} custom-call(bf16[8,512,128]{2,1,0:T(8,128)(2,1)} %copy-done.3), custom_call_target="tpu_custom_call" | custom-call | tf_op jit(solution)/shard_map/parts_sum/pallas_call | solution.py:305
  122.2 16.5 %all-to-all-done.in_ref = bf16[8,400,128]{2,1,0:T(8,128)(2,1)S(1)} async-done(((bf16[8,400,128]{2,1,0:T(8,128)(2,1)}), bf16[8,400,128]{2,1,0:T(8,128)(2,1)S(1)}, u32[]{:S(2)}, u32[]{:S(2)}) %all-to-all-start) | async-done | bytes 819232 | tf_op jit(solution)/shard_map/all_to_all | solution.py:292
  138.8 0.0 copy-start.4
  138.8 4.2 %all-to-all-start.3 = ((bf16[32,16,128]{2,1,0:T(8,128)(2,1)}), bf16[32,16,128]{2,1,0:T(8,128)(2,1)S(1)}, u32[]{:S(2)}, u32[]{:S(2)}) async-start(bf16[32,16,128]{2,1,0:T(8,128)(2,1)} %bitcast.26), calls=%async_computation.3 | async-start | bytes 262144 | tf_op jit(solution)/shard_map/all_to_all | solution.py:312
  142.9 0.0 copy-done.4
  142.9 2.5 %stick_join.1 = bf16[384,128]{1,0:T(8,128)(2,1)} custom-call(bf16[8,400,128]{2,1,0:T(8,128)(2,1)} %copy-done.4), custom_call_target="tpu_custom_call" | custom-call | flops 786432 | bytes 786432 | tf_op jit(solution)/shard_map/stick_join/pallas_call | solution.py:293
  145.4 6.9 %all-to-all-done.3 = bf16[32,16,128]{2,1,0:T(8,128)(2,1)S(1)} async-done(((bf16[32,16,128]{2,1,0:T(8,128)(2,1)}), bf16[32,16,128]{2,1,0:T(8,128)(2,1)S(1)}, u32[]{:S(2)}, u32[]{:S(2)}) %all-to-all-start.3) | async-done | bytes 131104 | tf_op jit(solution)/shard_map/all_to_all | solution.py:312
  152.3 0.0 copy-start.5
  152.3 0.6 copy-done.5
  152.9 1.9 %combine.1 = bf16[128,128]{1,0:T(8,128)(2,1)} custom-call(bf16[512,128]{1,0:T(8,128)(2,1)} %get-tuple-element.7.hi_ref, bf16[512,128]{1,0:T(8,128)(2,1)} %get-tuple-element.8.lo_ref, bf16[512,128]{1,0:T(8,128)(2,1)} %bitcast.27), custom_call_target="tpu_custom_call" | custom-call | tf_op jit(solution)/shard_map/combine/pallas_call | solution.py:313
  154.8 25.1 %all_gather.11 = bf16[128,2048]{1,0:T(8,128)(2,1)S(1)} all-gather(bf16[128,128]{1,0:T(8,128)(2,1)} %combine.1), channel_id=1, replica_groups=mesh['z'=8,'x'=4,'y'=8,'core'=2] {'y','core'}, dimensions={1}, use_global_device_ids=true | all-gather | bytes 557056 | tf_op jit(solution)/shard_map/all_gather | solution.py:320
  179.9 0.8 copy.14
  (2 shorter events, 0.0 us)
Async XLA Ops:
  3.4 47.0 %copy-start = (bf16[1,2048,224]{1,2,0:T(8,128)(2,1)S(1)}, bf16[1,2048,224]{1,2,0:T(8,128)(2,1)}, u32[]{:S(2)}) copy-start(bf16[1,2048,224]{1,2,0:T(8,128)(2,1)} %param.17) | copy-start | bytes 2752516
  3.4 47.0 %copy-start.1 = (bf16[1,2048,224]{1,2,0:T(8,128)(2,1)S(1)}, bf16[1,2048,224]{1,2,0:T(8,128)(2,1)}, u32[]{:S(2)}) copy-start(bf16[1,2048,224]{1,2,0:T(8,128)(2,1)} %param.18) | copy-start | bytes 2752516
  43.5 7.0 %collective-permute-start.3 = (bf16[512,1024]{1,0:T(8,128)(2,1)S(1)}, bf16[512,1024]{1,0:T(8,128)(2,1)S(1)}, u32[]{:S(2)}, u32[]{:S(2)}) collective-permute-start(bf16[512,1024]{1,0:T(8,128)(2,1)S(1)} %bitcast.19), channel_id=1, source_target_pairs={{0,1},{1,0},{2,3},{3,2},{4,5},{5,4},{6,7},{7,6},{8,9},{9,8},{10,11... | collective-permute-start | bytes 3145736 | tf_op jit(solution)/shard_map/ppermute | solution.py:213
  50.4 1.2 copy-start.2
  54.5 4.6 %collective-permute-start.4 = (bf16[8,512,128]{2,1,0:T(8,128)(2,1)S(1)}, bf16[8,512,128]{2,1,0:T(8,128)(2,1)S(1)}, u32[]{:S(2)}, u32[]{:S(2)}) collective-permute-start(bf16[8,512,128]{2,1,0:T(8,128)(2,1)S(1)} %get-tuple-element.11), channel_id=1, source_target_pairs={{0,1},{1,0},{2,3},{3,2},{4,5},{5,4},{6,7},{7,6},{8,9},{9,8},{10,11... | collective-permute-start | bytes 3145736 | tf_op jit(solution)/shard_map/ppermute | solution.py:213
  60.4 7.0 %copy-start.9 = (bf16[384,1]{0,1:T(2,128)(2,1)S(1)}, bf16[384,1]{0,1:T(2,128)(2,1)}, u32[]{:S(2)}) copy-start(bf16[384,1]{0,1:T(2,128)(2,1)} %param.14) | copy-start | bytes 2308
  60.4 7.0 %copy-start.7 = (bf16[384,128]{1,0:T(8,128)(2,1)S(1)}, bf16[384,128]{1,0:T(8,128)(2,1)}, u32[]{:S(2)}) copy-start(bf16[384,128]{1,0:T(8,128)(2,1)} %param.13) | copy-start | bytes 294916
  60.4 7.0 %copy-start.8 = (bf16[384,128]{1,0:T(8,128)(2,1)S(1)}, bf16[384,128]{1,0:T(8,128)(2,1)}, u32[]{:S(2)}) copy-start(bf16[384,128]{1,0:T(8,128)(2,1)} %param.12) | copy-start | bytes 294916
  60.4 17.9 %copy-start.6 = (bf16[384,128]{1,0:T(8,128)(2,1)S(1)}, bf16[384,128]{1,0:T(8,128)(2,1)}, u32[]{:S(2)}) copy-start(bf16[384,128]{1,0:T(8,128)(2,1)} %param.11) | copy-start | bytes 294916
  60.4 56.3 %all-to-all-start.2 = ((bf16[8,512,128]{2,1,0:T(8,128)(2,1)}), bf16[8,512,128]{2,1,0:T(8,128)(2,1)S(1)}, u32[]{:S(2)}, u32[]{:S(2)}) async-start(bf16[8,512,128]{2,1,0:T(8,128)(2,1)} %add_convert_fusion), calls=%async_computation.2 | async-start | bytes 2097152 | tf_op jit(solution)/shard_map/all_to_all | solution.py:267
  67.4 32.6 %collective-permute-start = (bf16[784,128]{1,0:T(8,128)(2,1)S(1)}, bf16[784,128]{1,0:T(8,128)(2,1)S(1)}, u32[]{:S(2)}, u32[]{:S(2)}) collective-permute-start(bf16[784,128]{1,0:T(8,128)(2,1)S(1)} %fusion.1.refs_0_), channel_id=1, source_target_pairs={{0,16},{16,32},{32,48},{48,0},{1,17},{17,33},{33,49},{49,1},{2,18}... | collective-permute-start | bytes 602120 | tf_op jit(solution)/shard_map/ppermute | solution.py:246
  70.8 29.1 %collective-permute-start.1 = (bf16[784,128]{1,0:T(8,128)(2,1)S(1)}, bf16[784,128]{1,0:T(8,128)(2,1)S(1)}, u32[]{:S(2)}, u32[]{:S(2)}) collective-permute-start(bf16[784,128]{1,0:T(8,128)(2,1)S(1)} %fusion.1.refs_0_), channel_id=1, source_target_pairs={{0,32},{16,48},{32,0},{48,16},{1,33},{17,49},{33,1},{49,17},{2,34}... | collective-permute-start | bytes 602120 | tf_op jit(solution)/shard_map/ppermute | solution.py:246
  75.2 24.8 %collective-permute-start.2 = (bf16[784,128]{1,0:T(8,128)(2,1)S(1)}, bf16[784,128]{1,0:T(8,128)(2,1)S(1)}, u32[]{:S(2)}, u32[]{:S(2)}) collective-permute-start(bf16[784,128]{1,0:T(8,128)(2,1)S(1)} %fusion.1.refs_0_), channel_id=1, source_target_pairs={{0,48},{16,0},{32,16},{48,32},{1,49},{17,1},{33,17},{49,33},{2,50}... | collective-permute-start | bytes 602120 | tf_op jit(solution)/shard_map/ppermute | solution.py:246
  116.7 3.6 %copy-start.3 = (bf16[8,512,128]{2,1,0:T(8,128)(2,1)}, bf16[8,512,128]{2,1,0:T(8,128)(2,1)S(1)}, u32[]{:S(2)}) copy-start(bf16[8,512,128]{2,1,0:T(8,128)(2,1)S(1)} %all-to-all-done.2.in_ref) | copy-start | bytes 3145732
  116.7 22.1 %all-to-all-start = ((bf16[8,400,128]{2,1,0:T(8,128)(2,1)}), bf16[8,400,128]{2,1,0:T(8,128)(2,1)S(1)}, u32[]{:S(2)}, u32[]{:S(2)}) async-start(bf16[8,400,128]{2,1,0:T(8,128)(2,1)} %stick_blocks.1), calls=%async_computation | async-start | bytes 1638400 | tf_op jit(solution)/shard_map/all_to_all | solution.py:292
  138.8 4.2 %copy-start.4 = (bf16[8,400,128]{2,1,0:T(8,128)(2,1)}, bf16[8,400,128]{2,1,0:T(8,128)(2,1)S(1)}, u32[]{:S(2)}) copy-start(bf16[8,400,128]{2,1,0:T(8,128)(2,1)S(1)} %all-to-all-done.in_ref) | copy-start | bytes 2457604
  138.8 13.5 %all-to-all-start.3 = ((bf16[32,16,128]{2,1,0:T(8,128)(2,1)}), bf16[32,16,128]{2,1,0:T(8,128)(2,1)S(1)}, u32[]{:S(2)}, u32[]{:S(2)}) async-start(bf16[32,16,128]{2,1,0:T(8,128)(2,1)} %bitcast.26), calls=%async_computation.3 | async-start | bytes 262144 | tf_op jit(solution)/shard_map/all_to_all | solution.py:312
  152.3 0.6 copy-start.5

commit v5 on v4

--- a/solution.py
+++ b/solution.py
@@ -13,8 +13,9 @@
 LOG2E = 1.4426950408889634
 F32 = jnp.float32
 BF16 = jnp.bfloat16
-Z, X, Y, CORE = 8, 4, 8, 2
-EP = ("z", "x")
+ZH, ZL, X, Y, CORE = 4, 2, 4, 8, 2
+Z = ("zh", "zl")
+EP = (*Z, "x")
 TP = ("y", "core")
 LANES = 128
 TILE = 256
@@ -43,7 +44,7 @@
             off_ref[0:1, at] = o[i : i + 1, :]
 
     def scale(i, done):
-        q = q_ref[i].astype(F32) * (hd**-0.5 * LOG2E)
+        q = q_ref[i // 2 * 2 + (i + z) % 2].astype(F32) * (hd**-0.5 * LOG2E)
         hi = q.astype(BF16)
         qq_ref[i, :, :hd] = hi
         qq_ref[i, :, hd:] = (q - hi.astype(F32)).astype(BF16)
@@ -191,21 +192,18 @@
     hidden = (gate / (1.0 + jnp.exp(-gate)) * up).astype(BF16)
     all_ref[...] = dot(hidden, down_ref[...]).astype(BF16)
     for i in range(chunks):
-        keep_ref[i] = all_ref[:, pl.ds(pl.multiple_of((2 * i + core) * LANES, LANES), LANES)]
-        send_ref[i] = all_ref[:, pl.ds(pl.multiple_of((2 * i + 1 - core) * LANES, LANES), LANES)]
-
-
-def sum_kernel(in_ref, out_ref):
-    total = in_ref[0].astype(F32)
-    for i in range(1, in_ref.shape[0]):
-        total = total + in_ref[i].astype(F32)
-    out_ref[...] = total.astype(out_ref.dtype)
+        for to_ref, half in ((keep_ref, core), (send_ref, 1 - core)):
+            cols = pl.ds(pl.multiple_of((2 * i + half) * LANES, LANES), LANES)
+            to_ref[:, i] = all_ref[:, cols].reshape(to_ref.shape[0], to_ref.shape[2], LANES)
 
 
 def combine_kernel(hi_ref, lo_ref, back_ref, out_ref):
-    back = back_ref[...]
+    total = back_ref[:, 0].astype(F32)
+    for i in range(1, back_ref.shape[1]):
+        total = total + back_ref[:, i].astype(F32)
+    total = total.astype(BF16).reshape(-1, LANES)
     out_ref[...] = (
-        dot(hi_ref[...], back, ((0,), (0,))) + dot(lo_ref[...], back, ((0,), (0,)))
+        dot(hi_ref[...], total, ((0,), (0,))) + dot(lo_ref[...], total, ((0,), (0,)))
     ).astype(BF16)
 
 
@@ -222,10 +220,10 @@
     hosts = lax.axis_size("y")
     cap = 2 * expert_ids.shape[1] * tok // experts
     slots = experts * cap
-    depth, wide = lax.axis_size("z"), lax.axis_size("x")
+    depth, wide = lax.axis_size(Z), lax.axis_size("x")
     len_, hd = queries.shape
     core = jnp.stack([lax.axis_index("core")]).astype(jnp.int32)
-    place = jnp.stack([lax.axis_index("z"), lax.axis_index("x")]).astype(jnp.int32)
+    place = jnp.stack([lax.axis_index(Z), lax.axis_index("x")]).astype(jnp.int32)
     outgoing, hi, lo = pl.pallas_call(
         functools.partial(dispatch_kernel, cap),
         out_shape=(
@@ -244,13 +242,15 @@
     kvo = [jnp.concatenate([keys, values, off], axis=0)]
     for step in range(1, wide):
         kvo.append(lax.ppermute(kvo[0], "x", [(i, (i + step) % wide) for i in range(wide)]))
-    q = lax.all_gather(queries, "z")
+    q = lax.ppermute(queries, "zl", [(0, 1), (1, 0)])
+    q = jnp.concatenate([queries, q], axis=0)
+    q = lax.all_gather(q, "zh").reshape(depth, len_, hd)
 
     hidden = gate_w.shape[2]
     other = swap(mine)
     keep, send = pl.pallas_call(
         expert_kernel,
-        out_shape=(jax.ShapeDtypeStruct((hosts, slots, LANES), BF16),) * 2,
+        out_shape=(jax.ShapeDtypeStruct((experts, hosts, cap, LANES), BF16),) * 2,
         in_specs=[SMEM] + vmem(5),
         out_specs=tuple(vmem(2)),
         scratch_shapes=[pltpu.VMEM((slots, width), BF16)],
@@ -264,7 +264,7 @@
     )(core, mine, other, gate_w[0].T, up_w[0].T, down_w[0])
     other = swap(send)
     share = (keep.astype(F32) + other.astype(F32)).astype(BF16)
-    share = lax.all_to_all(share, "y", 0, 0, tiled=True)
+    back = lax.all_to_all(share.reshape(-1, cap, LANES), (*EP, "y"), 0, 0, tiled=True)
 
     sums = pl.pallas_call(
         functools.partial(block_kernel, depth, wide, len_, hd),
@@ -289,7 +289,7 @@
         ),
         name="stick_blocks",
     )(place, q, *kvo)
-    arrived = lax.all_to_all(sums, "z", 0, 0, tiled=True)
+    arrived = lax.all_to_all(sums, Z, 0, 0, tiled=True)
     attended = pl.pallas_call(
         functools.partial(join_kernel, depth, len_),
         out_shape=jax.ShapeDtypeStruct((len_, hd), BF16),
@@ -302,27 +302,19 @@
         name="stick_join",
     )(arrived)
 
-    share = pl.pallas_call(
-        sum_kernel,
-        out_shape=jax.ShapeDtypeStruct((slots, LANES), BF16),
-        in_specs=vmem(1),
-        out_specs=vmem(1)[0],
-        name="parts_sum",
-    )(share)
-    back = lax.all_to_all(share.reshape(experts, cap, LANES), EP, 0, 0, tiled=True)
     mixed = pl.pallas_call(
         combine_kernel,
         out_shape=jax.ShapeDtypeStruct((tok, LANES), BF16),
         in_specs=vmem(3),
         out_specs=vmem(1)[0],
         name="combine",
-    )(hi, lo, back.reshape(slots, LANES))
+    )(hi, lo, back.reshape(experts, hosts, cap, LANES))
     mixed = lax.all_gather(mixed, TP, axis=1, tiled=True)
     return (attended, mixed)
 
 
 def solution(mesh):
-    fine = Mesh(mesh.devices.reshape(Z, X, Y, CORE), ("z", "x", "y", "core"))
+    fine = Mesh(mesh.devices.reshape(ZH, ZL, X, Y, CORE), (*Z, "x", *TP))
     return jax.shard_map(
         layer,
         mesh=fine,

time: 181 us -> 179 us (0.989)
  blocking collectives: 86.7 us -> 37.6 us
  starting transfers between devices: 32.5 us -> 60.1 us
  waiting for transfers between devices: 27.9 us -> 46.8 us
    all_to_all x1 -> x0, blocking collectives: 40 us -> none  [layer(): lax.all_to_all(outgoing.reshape(experts, cap, half), EP, 0, 0, tiled=True)]
    all_to_all x3, waiting for transfers between devices: 23.4 us -> 44.5 us  [the longest x1 26.1 us: layer(): lax.all_to_all(share.reshape(-1, cap, LANES), (*EP, 'y'), 0, 0, tiled=True)]
    all_to_all x3, starting transfers between devices: 14.7 us -> 34.4 us  [the longest x1 16.2 us: layer(): lax.all_to_all(share.reshape(-1, cap, LANES), (*EP, 'y'), 0, 0, tiled=True)]
    ppermute x2, starting transfers between devices: 6.99 us -> 12.1 us  [swap(): return lax.ppermute(x, 'core', [(0, 1), (1, 0)])]
    all_gather x1, blocking collectives: 21.6 us -> 16.7 us  [layer(): q = lax.all_gather(q, 'zh').reshape(depth, len_, hd)]
    all_gather x1, blocking collectives: 25.1 us -> 20.8 us  [layer(): mixed = lax.all_gather(mixed, TP, axis=1, tiled=True)]
    ppermute x0 -> x1, starting transfers between devices: none -> 3.09 us  [layer(): q = lax.ppermute(queries, 'zl', [(0, 1), (1, 0)])]
    ppermute x2, waiting for transfers between devices: 4.53 us -> 2.27 us  [swap(): return lax.ppermute(x, 'core', [(0, 1), (1, 0)])]
  transfers between devices with their start and end apart: 8 -> 9, of which waited for: 4 -> 4; matrix products, arithmetic and copies ran while one was open for 0% -> 1% of each run, Pallas kernels for 12% -> 12%
where the time goes in v5:
time: 179 us; the launch traced here: 178 us
  starting transfers between devices  60.1 us (34%)
  waiting for transfers between devices  46.8 us (26%)
  blocking collectives  37.6 us (21%)
  Pallas kernels  27.1 us (15%)
  local copies, waits for them, and re-layouts  4.15 us (2%)
    all_to_all x1, waiting for transfers between devices, layer(): lax.all_to_all(share.reshape(-1, cap, LANES), (*EP, 'y'), 0, 0, tiled=True)  26.1 us
    all_gather x1, blocking collectives, layer(): mixed = lax.all_gather(mixed, TP, axis=1, tiled=True)  20.8 us
    all_gather x1, blocking collectives, layer(): q = lax.all_gather(q, 'zh').reshape(depth, len_, hd)  16.7 us
    pallas_call x1, Pallas kernels, layer(): pl.pallas_call(functools.partial(block_kernel, depth, wide, len_, hd), ou...  16.7 us
    all_to_all x1, starting transfers between devices, layer(): lax.all_to_all(share.reshape(-1, cap, LANES), (*EP, 'y'), 0, 0, tiled=True)  16.2 us
    all_to_all x1, starting transfers between devices, layer(): lax.all_to_all(outgoing.reshape(experts, cap, half), EP, 0, 0, tiled=True)  13.8 us
    all_to_all x1, waiting for transfers between devices, layer(): lax.all_to_all(outgoing.reshape(experts, cap, half), EP, 0, 0, tiled=True)  12.5 us
    ppermute x2, starting transfers between devices, swap(): return lax.ppermute(x, 'core', [(0, 1), (1, 0)])  12.1 us
  transfers between devices with their start and end apart: 9, of which 4 were waited for; matrix products, arithmetic and copies ran while one was open for 1% of the time, Pallas kernels for 12%

profile of v5, /device:TPU:1, one launch (start us, length us, event | category | flops | bytes accessed | tf_op | source)
XLA Modules:
  0.0 178.0 jit_solution(7601108664438094496)
XLA Ops:
  0.6 2.8 %dispatch.1 = (bf16[512,1024]{1,0:T(8,128)(2,1)}, bf16[512,128]{1,0:T(8,128)(2,1)}, bf16[512,128]{1,0:T(8,128)(2,1)}) custom-call(s32[1]{0:T(128)} %bitcast.3.at_ref, bf16[128,2048]{1,0:T(8,128)(2,1)} %rows_ref.1, f32[1,2048]{1,0:T(1,128)} %bitcast.27, s32[2,128]{1,0:T(2,128)} %bitcast.29, f32[2,128]{1,0:T(2,128)} %bitcast.30), custom_call_target="tpu_custom_call" | custom-call | tf_op jit(solution)/shard_map/dispatch/pallas_call | solution.py:227
  3.4 0.0 copy-start.7
  3.4 0.0 copy-start.4
  3.4 0.0 copy-start.5
  3.4 0.0 copy-start.6
  3.4 13.8 %all-to-all-start.1 = ((bf16[32,16,1024]{2,1,0:T(8,128)(2,1)}), bf16[32,16,1024]{2,1,0:T(8,128)(2,1)S(1)}, u32[]{:S(2)}, u32[]{:S(2)}) async-start(bf16[32,16,1024]{2,1,0:T(8,128)(2,1)} %bitcast.26), calls=%async_computation.1 | async-start | bytes 2097152 | tf_op jit(solution)/shard_map/all_to_all | solution.py:238
  17.3 0.0 copy-done.7
  17.3 0.0 copy-done.4
  17.3 0.0 copy-done.5
  17.4 3.1 %collective-permute-start.1 = (bf16[784,128]{1,0:T(8,128)(2,1)S(1)}, bf16[784,128]{1,0:T(8,128)(2,1)S(1)}, u32[]{:S(2)}, u32[]{:S(2)}) collective-permute-start(bf16[784,128]{1,0:T(8,128)(2,1)S(1)} %fusion.1.refs_0_), channel_id=1, source_target_pairs={{0,16},{16,32},{32,48},{48,0},{1,17},{17,33},{33,49},{49,1},{2,18}... | collective-permute-start | bytes 602120 | tf_op jit(solution)/shard_map/ppermute | solution.py:244
  20.5 4.3 %collective-permute-start.2 = (bf16[784,128]{1,0:T(8,128)(2,1)S(1)}, bf16[784,128]{1,0:T(8,128)(2,1)S(1)}, u32[]{:S(2)}, u32[]{:S(2)}) collective-permute-start(bf16[784,128]{1,0:T(8,128)(2,1)S(1)} %fusion.1.refs_0_), channel_id=1, source_target_pairs={{0,32},{16,48},{32,0},{48,16},{1,33},{17,49},{33,1},{49,17},{2,34}... | collective-permute-start | bytes 602120 | tf_op jit(solution)/shard_map/ppermute | solution.py:244
  24.8 3.1 %collective-permute-start.3 = (bf16[784,128]{1,0:T(8,128)(2,1)S(1)}, bf16[784,128]{1,0:T(8,128)(2,1)S(1)}, u32[]{:S(2)}, u32[]{:S(2)}) collective-permute-start(bf16[784,128]{1,0:T(8,128)(2,1)S(1)} %fusion.1.refs_0_), channel_id=1, source_target_pairs={{0,48},{16,0},{32,16},{48,32},{1,49},{17,1},{33,17},{49,33},{2,50}... | collective-permute-start | bytes 602120 | tf_op jit(solution)/shard_map/ppermute | solution.py:244
  27.9 0.0 copy-done.6
  27.9 3.1 %collective-permute-start = (bf16[384,128]{1,0:T(8,128)(2,1)S(1)}, bf16[384,128]{1,0:T(8,128)(2,1)S(1)}, u32[]{:S(2)}, u32[]{:S(2)}) collective-permute-start(bf16[384,128]{1,0:T(8,128)(2,1)S(1)} %copy-done.6), channel_id=1, source_target_pairs={{0,64},{64,0},{1,65},{65,1},{2,66},{66,2},{3,67},{67,3},{4,68},{68... | collective-permute-start | bytes 294920 | tf_op jit(solution)/shard_map/ppermute | solution.py:245
  31.0 12.5 %all-to-all-done.1 = bf16[32,16,1024]{2,1,0:T(8,128)(2,1)S(1)} async-done(((bf16[32,16,1024]{2,1,0:T(8,128)(2,1)}), bf16[32,16,1024]{2,1,0:T(8,128)(2,1)S(1)}, u32[]{:S(2)}, u32[]{:S(2)}) %all-to-all-start.1) | async-done | bytes 1048608 | tf_op jit(solution)/shard_map/all_to_all | solution.py:238
  43.5 6.1 %collective-permute-start.4 = (bf16[512,1024]{1,0:T(8,128)(2,1)S(1)}, bf16[512,1024]{1,0:T(8,128)(2,1)S(1)}, u32[]{:S(2)}, u32[]{:S(2)}) collective-permute-start(bf16[512,1024]{1,0:T(8,128)(2,1)S(1)} %bitcast.19), channel_id=1, source_target_pairs={{0,1},{1,0},{2,3},{3,2},{4,5},{5,4},{6,7},{7,6},{8,9},{9,8},{10,11... | collective-permute-start | bytes 3145736 | tf_op jit(solution)/shard_map/ppermute | solution.py:211
  49.6 0.1 pad_add_fusion.at_ref
  49.7 0.0 collective-permute-done
  49.7 16.7 %all-gather = bf16[3072,128]{1,0:T(8,128)(2,1)S(1)} all-gather(bf16[768,128]{1,0:T(8,128)(2,1)S(1)} %pad_maximum_fusion), channel_id=2, replica_groups=mesh['zh'=4,'zl'=2,'x'=4,'y'=8,'core'=2] {'zh'}, dimensions={0}, use_global_device_ids=true | all-gather | bytes 983040 | tf_op jit(solution)/shard_map/all_gather | solution.py:247
  66.4 0.0 collective-permute-done.1.refs_1_
  66.4 0.0 collective-permute-done.2.refs_2_
  66.4 0.0 collective-permute-done.3.refs_3_
  66.4 16.7 %stick_blocks.1 = bf16[8,400,128]{2,1,0:T(8,128)(2,1)} custom-call(s32[2]{0:T(128)S(1)} %pad_add_fusion.at_ref, bf16[8,384,128]{2,1,0:T(8,128)(2,1)S(1)} %bitcast.21, bf16[784,128]{1,0:T(8,128)(2,1)S(1)} %fusion.1.refs_0_, bf16[784,128]{1,0:T(8,128)(2,1)S(1)} %collective-permute-done.1.refs_1_, bf16[784,128]{1,0:T(8,128)(2,1)S(1)} %collective-permute-done.2.refs_2_, ...), custom_call_target="tpu_custom_call" | custom-call | flops 6039797760 | bytes 2375680 | tf_op jit(solution)/shard_map/stick_blocks/pallas_call | solution.py:269
  83.1 0.0 copy-start
  83.1 4.4 %all-to-all-start = ((bf16[8,400,128]{2,1,0:T(8,128)(2,1)}), bf16[8,400,128]{2,1,0:T(8,128)(2,1)}, u32[]{:S(2)}, u32[]{:S(2)}) async-start(bf16[8,400,128]{2,1,0:T(8,128)(2,1)} %stick_blocks.1), calls=%async_computation | async-start | bytes 1638400 | tf_op jit(solution)/shard_map/all_to_all | solution.py:292
  87.5 0.0 collective-permute-done.4.other_ref
  87.5 0.0 copy-done
  87.5 0.0 copy-start.1
  87.5 1.2 copy-done.1
  88.7 0.0 copy-start.2
  88.7 1.2 copy-done.2
  89.9 2.9 %experts.1 = (bf16[32,8,16,128]{3,2,1,0:T(8,128)(2,1)S(1)}, bf16[32,8,16,128]{3,2,1,0:T(8,128)(2,1)S(1)}) custom-call(s32[1]{0:T(128)} %bitcast.3.at_ref, bf16[512,1024]{1,0:T(8,128)(2,1)S(1)} %bitcast.20, bf16[512,1024]{1,0:T(8,128)(2,1)S(1)} %collective-permute-done.4.other_ref, bf16[224,2048]{1,0:T(8,128)(2,1)S(1)} %bitcast.22, ...), custom_call_target="tpu_custom_call" | custom-call | flops 1409286144 | bytes 6946816 | tf_op jit(solution)/shard_map/experts/pallas_call | solution.py:251
  92.8 6.0 %collective-permute-start.5 = (bf16[32,8,16,128]{3,2,1,0:T(8,128)(2,1)S(1)}, bf16[32,8,16,128]{3,2,1,0:T(8,128)(2,1)S(1)}, u32[]{:S(2)}, u32[]{:S(2)}) collective-permute-start(bf16[32,8,16,128]{3,2,1,0:T(8,128)(2,1)S(1)} %get-tuple-element.11), channel_id=1, source_target_pairs={{0,1},{1,0},{2,3},{3,2},{4,5},{5,4},{6,7},{7,6},{8,9},{9,8},{10,11... | collective-permute-start | bytes 3145736 | tf_op jit(solution)/shard_map/ppermute | solution.py:211
  98.8 2.3 %collective-permute-done.5 = bf16[32,8,16,128]{3,2,1,0:T(8,128)(2,1)S(1)} collective-permute-done((bf16[32,8,16,128]{3,2,1,0:T(8,128)(2,1)S(1)}, bf16[32,8,16,128]{3,2,1,0:T(8,128)(2,1)S(1)}, u32[]{:S(2)}, u32[]{:S(2)}) %collective-permute-start.5) | collective-permute-done | bytes 1048608 | tf_op jit(solution)/shard_map/ppermute | solution.py:211
  101.0 1.4 add_convert_fusion
  102.4 5.9 %all-to-all-done.in_ref = bf16[8,400,128]{2,1,0:T(8,128)(2,1)} async-done(((bf16[8,400,128]{2,1,0:T(8,128)(2,1)}), bf16[8,400,128]{2,1,0:T(8,128)(2,1)}, u32[]{:S(2)}, u32[]{:S(2)}) %all-to-all-start) | async-done | bytes 819232 | tf_op jit(solution)/shard_map/all_to_all | solution.py:292
  108.4 16.2 %all-to-all-start.2 = ((bf16[256,16,128]{2,1,0:T(8,128)(2,1)}), bf16[256,16,128]{2,1,0:T(8,128)(2,1)S(1)}, u32[]{:S(2)}, u32[]{:S(2)}) async-start(bf16[256,16,128]{2,1,0:T(8,128)(2,1)} %bitcast.14), calls=%async_computation.2 | async-start | bytes 2097152 | tf_op jit(solution)/shard_map/all_to_all | solution.py:267
  124.6 2.5 %stick_join.1 = bf16[384,128]{1,0:T(8,128)(2,1)} custom-call(bf16[8,400,128]{2,1,0:T(8,128)(2,1)} %all-to-all-done.in_ref), custom_call_target="tpu_custom_call" | custom-call | flops 786432 | bytes 786432 | tf_op jit(solution)/shard_map/stick_join/pallas_call | solution.py:293
  127.0 26.1 %all-to-all-done.2 = bf16[256,16,128]{2,1,0:T(8,128)(2,1)S(1)} async-done(((bf16[256,16,128]{2,1,0:T(8,128)(2,1)}), bf16[256,16,128]{2,1,0:T(8,128)(2,1)S(1)}, u32[]{:S(2)}, u32[]{:S(2)}) %all-to-all-start.2) | async-done | bytes 1048608 | tf_op jit(solution)/shard_map/all_to_all | solution.py:267
  153.1 0.0 copy-start.3
  153.1 1.0 copy-done.3
  154.1 2.3 %combine.1 = bf16[128,128]{1,0:T(8,128)(2,1)} custom-call(bf16[512,128]{1,0:T(8,128)(2,1)} %get-tuple-element.7.hi_ref, bf16[512,128]{1,0:T(8,128)(2,1)} %get-tuple-element.8.lo_ref, bf16[32,8,16,128]{3,2,1,0:T(8,128)(2,1)} %bitcast.25), custom_call_target="tpu_custom_call" | custom-call | tf_op jit(solution)/shard_map/combine/pallas_call | solution.py:305
  156.4 20.8 %all_gather.11 = bf16[128,2048]{1,0:T(8,128)(2,1)S(1)} all-gather(bf16[128,128]{1,0:T(8,128)(2,1)} %combine.1), channel_id=1, replica_groups=mesh['zh'=4,'zl'=2,'x'=4,'y'=8,'core'=2] {'y','core'}, dimensions={1}, use_global_device_ids=true | all-gather | bytes 557056 | tf_op jit(solution)/shard_map/all_gather | solution.py:312
  177.2 0.8 copy.14
  (3 shorter events, 0.1 us)
Async XLA Ops:
  3.4 13.9 %copy-start.7 = (bf16[384,1]{0,1:T(2,128)(2,1)S(1)}, bf16[384,1]{0,1:T(2,128)(2,1)}, u32[]{:S(2)}) copy-start(bf16[384,1]{0,1:T(2,128)(2,1)} %param.14) | copy-start | bytes 2308
  3.4 13.9 %copy-start.4 = (bf16[384,128]{1,0:T(8,128)(2,1)S(1)}, bf16[384,128]{1,0:T(8,128)(2,1)}, u32[]{:S(2)}) copy-start(bf16[384,128]{1,0:T(8,128)(2,1)} %param.13) | copy-start | bytes 294916
  3.4 13.9 %copy-start.5 = (bf16[384,128]{1,0:T(8,128)(2,1)S(1)}, bf16[384,128]{1,0:T(8,128)(2,1)}, u32[]{:S(2)}) copy-start(bf16[384,128]{1,0:T(8,128)(2,1)} %param.12) | copy-start | bytes 294916
  3.4 24.5 %copy-start.6 = (bf16[384,128]{1,0:T(8,128)(2,1)S(1)}, bf16[384,128]{1,0:T(8,128)(2,1)}, u32[]{:S(2)}) copy-start(bf16[384,128]{1,0:T(8,128)(2,1)} %param.11) | copy-start | bytes 294916
  3.4 40.1 %all-to-all-start.1 = ((bf16[32,16,1024]{2,1,0:T(8,128)(2,1)}), bf16[32,16,1024]{2,1,0:T(8,128)(2,1)S(1)}, u32[]{:S(2)}, u32[]{:S(2)}) async-start(bf16[32,16,1024]{2,1,0:T(8,128)(2,1)} %bitcast.26), calls=%async_computation.1 | async-start | bytes 2097152 | tf_op jit(solution)/shard_map/all_to_all | solution.py:238
  17.4 49.1 %collective-permute-start.1 = (bf16[784,128]{1,0:T(8,128)(2,1)S(1)}, bf16[784,128]{1,0:T(8,128)(2,1)S(1)}, u32[]{:S(2)}, u32[]{:S(2)}) collective-permute-start(bf16[784,128]{1,0:T(8,128)(2,1)S(1)} %fusion.1.refs_0_), channel_id=1, source_target_pairs={{0,16},{16,32},{32,48},{48,0},{1,17},{17,33},{33,49},{49,1},{2,18}... | collective-permute-start | bytes 602120 | tf_op jit(solution)/shard_map/ppermute | solution.py:244
  20.5 45.9 %collective-permute-start.2 = (bf16[784,128]{1,0:T(8,128)(2,1)S(1)}, bf16[784,128]{1,0:T(8,128)(2,1)S(1)}, u32[]{:S(2)}, u32[]{:S(2)}) collective-permute-start(bf16[784,128]{1,0:T(8,128)(2,1)S(1)} %fusion.1.refs_0_), channel_id=1, source_target_pairs={{0,32},{16,48},{32,0},{48,16},{1,33},{17,49},{33,1},{49,17},{2,34}... | collective-permute-start | bytes 602120 | tf_op jit(solution)/shard_map/ppermute | solution.py:244
  24.8 41.6 %collective-permute-start.3 = (bf16[784,128]{1,0:T(8,128)(2,1)S(1)}, bf16[784,128]{1,0:T(8,128)(2,1)S(1)}, u32[]{:S(2)}, u32[]{:S(2)}) collective-permute-start(bf16[784,128]{1,0:T(8,128)(2,1)S(1)} %fusion.1.refs_0_), channel_id=1, source_target_pairs={{0,48},{16,0},{32,16},{48,32},{1,49},{17,1},{33,17},{49,33},{2,50}... | collective-permute-start | bytes 602120 | tf_op jit(solution)/shard_map/ppermute | solution.py:244
  27.9 21.7 %collective-permute-start = (bf16[384,128]{1,0:T(8,128)(2,1)S(1)}, bf16[384,128]{1,0:T(8,128)(2,1)S(1)}, u32[]{:S(2)}, u32[]{:S(2)}) collective-permute-start(bf16[384,128]{1,0:T(8,128)(2,1)S(1)} %copy-done.6), channel_id=1, source_target_pairs={{0,64},{64,0},{1,65},{65,1},{2,66},{66,2},{3,67},{67,3},{4,68},{68... | collective-permute-start | bytes 294920 | tf_op jit(solution)/shard_map/ppermute | solution.py:245
  43.5 44.0 %collective-permute-start.4 = (bf16[512,1024]{1,0:T(8,128)(2,1)S(1)}, bf16[512,1024]{1,0:T(8,128)(2,1)S(1)}, u32[]{:S(2)}, u32[]{:S(2)}) collective-permute-start(bf16[512,1024]{1,0:T(8,128)(2,1)S(1)} %bitcast.19), channel_id=1, source_target_pairs={{0,1},{1,0},{2,3},{3,2},{4,5},{5,4},{6,7},{7,6},{8,9},{9,8},{10,11... | collective-permute-start | bytes 3145736 | tf_op jit(solution)/shard_map/ppermute | solution.py:211
  83.1 4.4 %copy-start = (bf16[1,2048,224]{1,2,0:T(8,128)(2,1)S(1)}, bf16[1,2048,224]{1,2,0:T(8,128)(2,1)}, u32[]{:S(2)}) copy-start(bf16[1,2048,224]{1,2,0:T(8,128)(2,1)} %param.17) | copy-start | bytes 2752516
  83.1 25.2 %all-to-all-start = ((bf16[8,400,128]{2,1,0:T(8,128)(2,1)}), bf16[8,400,128]{2,1,0:T(8,128)(2,1)}, u32[]{:S(2)}, u32[]{:S(2)}) async-start(bf16[8,400,128]{2,1,0:T(8,128)(2,1)} %stick_blocks.1), calls=%async_computation | async-start | bytes 1638400 | tf_op jit(solution)/shard_map/all_to_all | solution.py:292
  87.5 1.2 copy-start.1
  88.7 1.2 copy-start.2
  92.8 8.3 %collective-permute-start.5 = (bf16[32,8,16,128]{3,2,1,0:T(8,128)(2,1)S(1)}, bf16[32,8,16,128]{3,2,1,0:T(8,128)(2,1)S(1)}, u32[]{:S(2)}, u32[]{:S(2)}) collective-permute-start(bf16[32,8,16,128]{3,2,1,0:T(8,128)(2,1)S(1)} %get-tuple-element.11), channel_id=1, source_target_pairs={{0,1},{1,0},{2,3},{3,2},{4,5},{5,4},{6,7},{7,6},{8,9},{9,8},{10,11... | collective-permute-start | bytes 3145736 | tf_op jit(solution)/shard_map/ppermute | solution.py:211
  108.4 44.8 %all-to-all-start.2 = ((bf16[256,16,128]{2,1,0:T(8,128)(2,1)}), bf16[256,16,128]{2,1,0:T(8,128)(2,1)S(1)}, u32[]{:S(2)}, u32[]{:S(2)}) async-start(bf16[256,16,128]{2,1,0:T(8,128)(2,1)} %bitcast.14), calls=%async_computation.2 | async-start | bytes 2097152 | tf_op jit(solution)/shard_map/all_to_all | solution.py:267
  153.1 1.0 copy-start.3

commit v6 on v4

--- a/solution.py
+++ b/solution.py
@@ -13,8 +13,9 @@
 LOG2E = 1.4426950408889634
 F32 = jnp.float32
 BF16 = jnp.bfloat16
-Z, X, Y, CORE = 8, 4, 8, 2
-EP = ("z", "x")
+ZH, ZL, X, Y, CORE = 4, 2, 4, 8, 2
+Z = ("zh", "zl")
+EP = (*Z, "x")
 TP = ("y", "core")
 LANES = 128
 TILE = 256
@@ -43,7 +44,7 @@
             off_ref[0:1, at] = o[i : i + 1, :]
 
     def scale(i, done):
-        q = q_ref[i].astype(F32) * (hd**-0.5 * LOG2E)
+        q = q_ref[i // 2 * 2 + (i + z) % 2].astype(F32) * (hd**-0.5 * LOG2E)
         hi = q.astype(BF16)
         qq_ref[i, :, :hd] = hi
         qq_ref[i, :, hd:] = (q - hi.astype(F32)).astype(BF16)
@@ -58,15 +59,12 @@
     tot_ref[...] = jnp.zeros_like(tot_ref)
     lane = lax.broadcasted_iota(jnp.int32, (len_, LANES), 1)
 
-    def part(to, which, old, masked):
-        start = pl.multiple_of(which * half, half)
+    def part(to, start, tiles, carry, acc, masked):
         q = qq_ref[to]
-        carry = 0.0 if masked else carry_ref[...] * old
-        acc = 0.0 if masked else acc_ref[...] * old
-        for tile in reversed(range(half // TILE)):
+        for tile in reversed(range(tiles)):
             keys = pl.ds(pl.multiple_of(start + tile * TILE, TILE), TILE)
             u = dot(q, kk_ref[keys, :], ((1,), (1,))) + off_ref[0:1, keys]
-            sp = kept = jnp.maximum(u, 0.0) + jnp.log2(1.0 + jnp.exp2(-jnp.abs(u)))
+            sp = kept = jnp.maximum(u, jnp.log2(1.0 + jnp.exp2(jnp.minimum(u, 126.0))))
             if masked:
                 ahead = lax.broadcasted_iota(jnp.int32, (len_, TILE), 0) - lax.broadcasted_iota(
                     jnp.int32, (len_, TILE), 1
@@ -74,35 +72,32 @@
                 strict = ahead > start + tile * TILE - x * len_
                 kept = jnp.where(strict, sp, 0.0)
             w = dot(kept.astype(BF16), tri_ref[...])
-            if isinstance(carry, float):
+            if carry is None:
                 p = jnp.exp2(u - sp + w)
             else:
                 p = jnp.exp2(u - sp + w + jnp.concatenate([carry] * (TILE // LANES), axis=1))
             if masked:
                 p = jnp.where(strict, p, 0.0)
-            acc = acc + dot(p.astype(BF16), v_ref[keys, :])
-            carry = carry + jnp.broadcast_to(w[:, 0:1] - kept[:, 0:1], (len_, LANES))
-        carry_ref[...] = carry
-        acc_ref[...] = acc
+            summed = dot(p.astype(BF16), v_ref[keys, :])
+            total = jnp.broadcast_to(w[:, 0:1] - kept[:, 0:1], (len_, LANES))
+            acc = summed if acc is None else acc + summed
+            carry = total if carry is None else carry + total
         out_ref[to, pl.ds(0, len_), :] = acc.astype(BF16)
         tot_ref[...] = jnp.where(lane == to, carry, tot_ref[...])
+        return carry, acc
 
     own = x * len_ // half
-    part(z, own, None, True)
+    carry_ref[...], acc_ref[...] = part(z, own * half, half // TILE, None, None, True)
+
+    @pl.when(own == 1)
+    def _():
+        part(z, 0, half // TILE, carry_ref[...], acc_ref[...], False)
 
     def full(i, done):
-        j = i - own
-        before = i < own
-        fresh = jnp.logical_and(jnp.logical_not(before), j % 2 == 0)
-        part(
-            jnp.where(before, z, z + 1 + j // 2),
-            jnp.where(before, 0, 1 - j % 2),
-            jnp.where(fresh, 0.0, 1.0),
-            False,
-        )
+        part(i, 0, 2 * half // TILE, None, None, False)
         return done
 
-    lax.fori_loop(0, own + 2 * (depth - 1 - z), full, 0)
+    lax.fori_loop(z + 1, depth, full, 0)
 
     def clear(i, done):
         out_ref[i, pl.ds(0, len_), :] = jnp.zeros((len_, hd), BF16)
@@ -222,10 +217,10 @@
     hosts = lax.axis_size("y")
     cap = 2 * expert_ids.shape[1] * tok // experts
     slots = experts * cap
-    depth, wide = lax.axis_size("z"), lax.axis_size("x")
+    depth, wide = lax.axis_size(Z), lax.axis_size("x")
     len_, hd = queries.shape
     core = jnp.stack([lax.axis_index("core")]).astype(jnp.int32)
-    place = jnp.stack([lax.axis_index("z"), lax.axis_index("x")]).astype(jnp.int32)
+    place = jnp.stack([lax.axis_index(Z), lax.axis_index("x")]).astype(jnp.int32)
     outgoing, hi, lo = pl.pallas_call(
         functools.partial(dispatch_kernel, cap),
         out_shape=(
@@ -244,7 +239,9 @@
     kvo = [jnp.concatenate([keys, values, off], axis=0)]
     for step in range(1, wide):
         kvo.append(lax.ppermute(kvo[0], "x", [(i, (i + step) % wide) for i in range(wide)]))
-    q = lax.all_gather(queries, "z")
+    q = lax.ppermute(queries, "zl", [(0, 1), (1, 0)])
+    q = jnp.concatenate([queries, q], axis=0)
+    q = lax.all_gather(q, "zh").reshape(depth, len_, hd)
 
     hidden = gate_w.shape[2]
     other = swap(mine)
@@ -289,7 +286,7 @@
         ),
         name="stick_blocks",
     )(place, q, *kvo)
-    arrived = lax.all_to_all(sums, "z", 0, 0, tiled=True)
+    arrived = lax.all_to_all(sums, Z, 0, 0, tiled=True)
     attended = pl.pallas_call(
         functools.partial(join_kernel, depth, len_),
         out_shape=jax.ShapeDtypeStruct((len_, hd), BF16),
@@ -322,7 +319,7 @@
 
 
 def solution(mesh):
-    fine = Mesh(mesh.devices.reshape(Z, X, Y, CORE), ("z", "x", "y", "core"))
+    fine = Mesh(mesh.devices.reshape(ZH, ZL, X, Y, CORE), (*Z, "x", *TP))
     return jax.shard_map(
         layer,
         mesh=fine,

time: 181 us -> 181 us (level)
  blocking collectives: 86.7 us -> 77.7 us
  starting transfers between devices: 32.5 us -> 39.3 us
  waiting for transfers between devices: 27.9 us -> 31.5 us
    all_gather x1, blocking collectives: 21.6 us -> 15.3 us  [layer(): q = lax.all_gather(q, 'zh').reshape(depth, len_, hd)]
    all_to_all x1, starting transfers between devices: 4.16 us -> 8.75 us  [layer(): lax.all_to_all(share.reshape(experts, cap, LANES), EP, 0, 0, tiled=True)]
    ppermute x0 -> x1, waiting for transfers between devices: none -> 3.36 us  [layer(): q = lax.ppermute(queries, 'zl', [(0, 1), (1, 0)])]
    all_gather x1, blocking collectives: 25.1 us -> 22.4 us  [layer(): mixed = lax.all_gather(mixed, TP, axis=1, tiled=True)]
    ppermute x0 -> x1, starting transfers between devices: none -> 2.21 us  [layer(): q = lax.ppermute(queries, 'zl', [(0, 1), (1, 0)])]
    pallas_call x1, Pallas kernels: 16.7 us -> 14.8 us  [layer(): pl.pallas_call(functools.partial(block_kernel, depth, wide, len_, hd), ou...]
  transfers between devices with their start and end apart: 8 -> 9, of which waited for: 4 -> 5; matrix products, arithmetic and copies ran while one was open for 0% -> 0% of each run, Pallas kernels for 12% -> 11%
where the time goes in v6:
time: 181 us; the launch traced here: 180 us
  blocking collectives  77.7 us (43%)
  starting transfers between devices  39.3 us (22%)
  waiting for transfers between devices  31.5 us (17%)
  Pallas kernels  26.9 us (15%)
  local copies, waits for them, and re-layouts  2.65 us (1%)
    all_to_all x1, blocking collectives, layer(): lax.all_to_all(outgoing.reshape(experts, cap, half), EP, 0, 0, tiled=True)  40 us
    all_gather x1, blocking collectives, layer(): mixed = lax.all_gather(mixed, TP, axis=1, tiled=True)  22.4 us
    all_to_all x1, waiting for transfers between devices, layer(): arrived = lax.all_to_all(sums, Z, 0, 0, tiled=True)  16.7 us
    all_gather x1, blocking collectives, layer(): q = lax.all_gather(q, 'zh').reshape(depth, len_, hd)  15.3 us
    pallas_call x1, Pallas kernels, layer(): pl.pallas_call(functools.partial(block_kernel, depth, wide, len_, hd), ou...  14.8 us
    ppermute x3, starting transfers between devices, layer(): lax.ppermute(kvo[0], 'x', [(i, (i + step) % wide) for i in range(wide)])  10.8 us
    all_to_all x1, starting transfers between devices, layer(): lax.all_to_all(share.reshape(experts, cap, LANES), EP, 0, 0, tiled=True)  8.75 us
    ppermute x2, starting transfers between devices, swap(): return lax.ppermute(x, 'core', [(0, 1), (1, 0)])  6.99 us
  transfers between devices with their start and end apart: 9, of which 5 were waited for; matrix products, arithmetic and copies ran while one was open for 0% of the time, Pallas kernels for 11%

profile of v6, /device:TPU:1, one launch (start us, length us, event | category | flops | bytes accessed | tf_op | source)
XLA Modules:
  0.0 180.2 jit_solution(14156400700159609589)
XLA Ops:
  0.6 2.8 %dispatch.1 = (bf16[512,1024]{1,0:T(8,128)(2,1)}, bf16[512,128]{1,0:T(8,128)(2,1)}, bf16[512,128]{1,0:T(8,128)(2,1)}) custom-call(s32[1]{0:T(128)} %bitcast.3.at_ref, bf16[128,2048]{1,0:T(8,128)(2,1)} %rows_ref.1, f32[1,2048]{1,0:T(1,128)} %bitcast.28, s32[2,128]{1,0:T(2,128)} %bitcast.30, f32[2,128]{1,0:T(2,128)} %bitcast.31), custom_call_target="tpu_custom_call" | custom-call | tf_op jit(solution)/shard_map/dispatch/pallas_call | solution.py:224
  3.4 0.0 copy-start
  3.4 0.0 copy-start.1
  3.4 40.0 %all_to_all.20 = bf16[32,16,1024]{2,1,0:T(8,128)(2,1)S(1)} all-to-all(bf16[32,16,1024]{2,1,0:T(8,128)(2,1)} %bitcast.25), channel_id=1, replica_groups=mesh['zh'=4,'zl'=2,'x'=4,'y'=8,'core'=2] {'zh','zl','x'}, dimensions={0} | all-to-all | bytes 2097152 | tf_op jit(solution)/shard_map/all_to_all | solution.py:235
  43.5 4.7 %collective-permute-start.4 = (bf16[512,1024]{1,0:T(8,128)(2,1)S(1)}, bf16[512,1024]{1,0:T(8,128)(2,1)S(1)}, u32[]{:S(2)}, u32[]{:S(2)}) collective-permute-start(bf16[512,1024]{1,0:T(8,128)(2,1)S(1)} %bitcast.19), channel_id=1, source_target_pairs={{0,1},{1,0},{2,3},{3,2},{4,5},{5,4},{6,7},{7,6},{8,9},{9,8},{10,11... | collective-permute-start | bytes 3145736 | tf_op jit(solution)/shard_map/ppermute | solution.py:208
  48.2 2.3 %collective-permute-done.4.other_ref = bf16[512,1024]{1,0:T(8,128)(2,1)S(1)} collective-permute-done((bf16[512,1024]{1,0:T(8,128)(2,1)S(1)}, bf16[512,1024]{1,0:T(8,128)(2,1)S(1)}, u32[]{:S(2)}, u32[]{:S(2)}) %collective-permute-start.4) | collective-permute-done | bytes 1048608 | tf_op jit(solution)/shard_map/ppermute | solution.py:208
  50.4 0.0 copy-done
  50.4 0.0 copy-done.1
  50.4 0.0 copy-start.2
  50.4 1.2 copy-done.2
  51.6 2.9 %experts.1 = (bf16[8,512,128]{2,1,0:T(8,128)(2,1)S(1)}, bf16[8,512,128]{2,1,0:T(8,128)(2,1)S(1)}) custom-call(s32[1]{0:T(128)} %bitcast.3.at_ref, bf16[512,1024]{1,0:T(8,128)(2,1)S(1)} %bitcast.20, bf16[512,1024]{1,0:T(8,128)(2,1)S(1)} %collective-permute-done.4.other_ref, bf16[224,2048]{1,0:T(8,128)(2,1)S(1)} %bitcast.22, bf16[224,2048]{1,0:T(8,128)(2,1)S(1)} %bitcast.23, ...), custom_call_target="tpu_custom_call" | custom-call | flops 1409286144 | bytes 6946816 | tf_op jit(solution)/shard_map/experts/pallas_call | solution.py:248
  54.5 2.3 %collective-permute-start.5 = (bf16[8,512,128]{2,1,0:T(8,128)(2,1)S(1)}, bf16[8,512,128]{2,1,0:T(8,128)(2,1)S(1)}, u32[]{:S(2)}, u32[]{:S(2)}) collective-permute-start(bf16[8,512,128]{2,1,0:T(8,128)(2,1)S(1)} %get-tuple-element.11), channel_id=1, source_target_pairs={{0,1},{1,0},{2,3},{3,2},{4,5},{5,4},{6,7},{7,6},{8,9},{9,8},{10,11... | collective-permute-start | bytes 3145736 | tf_op jit(solution)/shard_map/ppermute | solution.py:208
  56.8 2.3 %collective-permute-done.5 = bf16[8,512,128]{2,1,0:T(8,128)(2,1)S(1)} collective-permute-done((bf16[8,512,128]{2,1,0:T(8,128)(2,1)S(1)}, bf16[8,512,128]{2,1,0:T(8,128)(2,1)S(1)}, u32[]{:S(2)}, u32[]{:S(2)}) %collective-permute-start.5) | collective-permute-done | bytes 1048608 | tf_op jit(solution)/shard_map/ppermute | solution.py:208
  59.1 1.3 add_convert_fusion
  60.3 0.0 copy-start.9
  60.3 0.0 copy-start.6
  60.4 0.0 copy-start.7
  60.4 0.0 copy-start.8
  60.4 7.0 %all-to-all-start.2 = ((bf16[8,512,128]{2,1,0:T(8,128)(2,1)}), bf16[8,512,128]{2,1,0:T(8,128)(2,1)S(1)}, u32[]{:S(2)}, u32[]{:S(2)}) async-start(bf16[8,512,128]{2,1,0:T(8,128)(2,1)} %add_convert_fusion), calls=%async_computation.2 | async-start | bytes 2097152 | tf_op jit(solution)/shard_map/all_to_all | solution.py:264
  67.3 0.0 copy-done.9
  67.3 0.0 copy-done.6
  67.4 0.0 copy-done.7
  67.4 3.4 %collective-permute-start.1 = (bf16[784,128]{1,0:T(8,128)(2,1)S(1)}, bf16[784,128]{1,0:T(8,128)(2,1)S(1)}, u32[]{:S(2)}, u32[]{:S(2)}) collective-permute-start(bf16[784,128]{1,0:T(8,128)(2,1)S(1)} %fusion.1.refs_0_), channel_id=1, source_target_pairs={{0,16},{16,32},{32,48},{48,0},{1,17},{17,33},{33,49},{49,1},{2,18}... | collective-permute-start | bytes 602120 | tf_op jit(solution)/shard_map/ppermute | solution.py:241
  70.8 4.3 %collective-permute-start.2 = (bf16[784,128]{1,0:T(8,128)(2,1)S(1)}, bf16[784,128]{1,0:T(8,128)(2,1)S(1)}, u32[]{:S(2)}, u32[]{:S(2)}) collective-permute-start(bf16[784,128]{1,0:T(8,128)(2,1)S(1)} %fusion.1.refs_0_), channel_id=1, source_target_pairs={{0,32},{16,48},{32,0},{48,16},{1,33},{17,49},{33,1},{49,17},{2,34}... | collective-permute-start | bytes 602120 | tf_op jit(solution)/shard_map/ppermute | solution.py:241
  75.2 3.1 %collective-permute-start.3 = (bf16[784,128]{1,0:T(8,128)(2,1)S(1)}, bf16[784,128]{1,0:T(8,128)(2,1)S(1)}, u32[]{:S(2)}, u32[]{:S(2)}) collective-permute-start(bf16[784,128]{1,0:T(8,128)(2,1)S(1)} %fusion.1.refs_0_), channel_id=1, source_target_pairs={{0,48},{16,0},{32,16},{48,32},{1,49},{17,1},{33,17},{49,33},{2,50}... | collective-permute-start | bytes 602120 | tf_op jit(solution)/shard_map/ppermute | solution.py:241
  78.2 0.0 copy-done.8
  78.3 2.2 %collective-permute-start = (bf16[384,128]{1,0:T(8,128)(2,1)S(1)}, bf16[384,128]{1,0:T(8,128)(2,1)S(1)}, u32[]{:S(2)}, u32[]{:S(2)}) collective-permute-start(bf16[384,128]{1,0:T(8,128)(2,1)S(1)} %copy-done.8), channel_id=1, source_target_pairs={{0,64},{64,0},{1,65},{65,1},{2,66},{66,2},{3,67},{67,3},{4,68},{68... | collective-permute-start | bytes 294920 | tf_op jit(solution)/shard_map/ppermute | solution.py:242
  80.5 0.1 pad_add_fusion.at_ref
  80.6 3.4 %collective-permute-done = bf16[384,128]{1,0:T(8,128)(2,1)S(1)} collective-permute-done((bf16[384,128]{1,0:T(8,128)(2,1)S(1)}, bf16[384,128]{1,0:T(8,128)(2,1)S(1)}, u32[]{:S(2)}, u32[]{:S(2)}) %collective-permute-start) | collective-permute-done | bytes 98336 | tf_op jit(solution)/shard_map/ppermute | solution.py:242
  83.9 15.3 %all-gather = bf16[3072,128]{1,0:T(8,128)(2,1)S(1)} all-gather(bf16[768,128]{1,0:T(8,128)(2,1)S(1)} %pad_maximum_fusion), channel_id=2, replica_groups=mesh['zh'=4,'zl'=2,'x'=4,'y'=8,'core'=2] {'zh'}, dimensions={0}, use_global_device_ids=true | all-gather | bytes 983040 | tf_op jit(solution)/shard_map/all_gather | solution.py:244
  99.2 0.0 collective-permute-done.1.refs_1_
  99.2 0.0 collective-permute-done.2.refs_2_
  99.2 0.0 collective-permute-done.3.refs_3_
  99.2 14.8 %stick_blocks.1 = bf16[8,400,128]{2,1,0:T(8,128)(2,1)} custom-call(s32[2]{0:T(128)S(1)} %pad_add_fusion.at_ref, bf16[8,384,128]{2,1,0:T(8,128)(2,1)S(1)} %bitcast.21, bf16[784,128]{1,0:T(8,128)(2,1)S(1)} %fusion.1.refs_0_, bf16[784,128]{1,0:T(8,128)(2,1)S(1)} %collective-permute-done.1.refs_1_, bf16[784,128]{1,0:T(8,128)(2,1)S(1)} %collective-permute-done.2.refs_2_, ...), custom_call_target="tpu_custom_call" | custom-call | flops 6039797760 | bytes 2375680 | tf_op jit(solution)/shard_map/stick_blocks/pallas_call | solution.py:266
  114.1 0.0 all-to-all-done.2.in_ref
  114.1 0.0 copy-start.3
  114.1 3.5 %all-to-all-start = ((bf16[8,400,128]{2,1,0:T(8,128)(2,1)}), bf16[8,400,128]{2,1,0:T(8,128)(2,1)S(1)}, u32[]{:S(2)}, u32[]{:S(2)}) async-start(bf16[8,400,128]{2,1,0:T(8,128)(2,1)} %stick_blocks.1), calls=%async_computation | async-start | bytes 1638400 | tf_op jit(solution)/shard_map/all_to_all | solution.py:289
  117.6 0.0 copy-done.3
  117.6 2.0 %parts_sum.1 = bf16[512,128]{1,0:T(8,128)(2,1)} custom-call(bf16[8,512,128]{2,1,0:T(8,128)(2,1)} %copy-done.3), custom_call_target="tpu_custom_call" | custom-call | tf_op jit(solution)/shard_map/parts_sum/pallas_call | solution.py:302
  119.6 16.7 %all-to-all-done.in_ref = bf16[8,400,128]{2,1,0:T(8,128)(2,1)S(1)} async-done(((bf16[8,400,128]{2,1,0:T(8,128)(2,1)}), bf16[8,400,128]{2,1,0:T(8,128)(2,1)S(1)}, u32[]{:S(2)}, u32[]{:S(2)}) %all-to-all-start) | async-done | bytes 819232 | tf_op jit(solution)/shard_map/all_to_all | solution.py:289
  136.3 0.0 copy-start.4
  136.3 8.7 %all-to-all-start.3 = ((bf16[32,16,128]{2,1,0:T(8,128)(2,1)}), bf16[32,16,128]{2,1,0:T(8,128)(2,1)S(1)}, u32[]{:S(2)}, u32[]{:S(2)}) async-start(bf16[32,16,128]{2,1,0:T(8,128)(2,1)} %bitcast.26), calls=%async_computation.3 | async-start | bytes 262144 | tf_op jit(solution)/shard_map/all_to_all | solution.py:309
  145.1 0.0 copy-done.4
  145.1 2.5 %stick_join.1 = bf16[384,128]{1,0:T(8,128)(2,1)} custom-call(bf16[8,400,128]{2,1,0:T(8,128)(2,1)} %copy-done.4), custom_call_target="tpu_custom_call" | custom-call | flops 786432 | bytes 786432 | tf_op jit(solution)/shard_map/stick_join/pallas_call | solution.py:290
  147.5 6.9 %all-to-all-done.3 = bf16[32,16,128]{2,1,0:T(8,128)(2,1)S(1)} async-done(((bf16[32,16,128]{2,1,0:T(8,128)(2,1)}), bf16[32,16,128]{2,1,0:T(8,128)(2,1)S(1)}, u32[]{:S(2)}, u32[]{:S(2)}) %all-to-all-start.3) | async-done | bytes 131104 | tf_op jit(solution)/shard_map/all_to_all | solution.py:309
  154.5 0.0 copy-start.5
  154.5 0.6 copy-done.5
  155.1 1.9 %combine.1 = bf16[128,128]{1,0:T(8,128)(2,1)} custom-call(bf16[512,128]{1,0:T(8,128)(2,1)} %get-tuple-element.7.hi_ref, bf16[512,128]{1,0:T(8,128)(2,1)} %get-tuple-element.8.lo_ref, bf16[512,128]{1,0:T(8,128)(2,1)} %bitcast.27), custom_call_target="tpu_custom_call" | custom-call | tf_op jit(solution)/shard_map/combine/pallas_call | solution.py:310
  157.0 22.4 %all_gather.11 = bf16[128,2048]{1,0:T(8,128)(2,1)S(1)} all-gather(bf16[128,128]{1,0:T(8,128)(2,1)} %combine.1), channel_id=1, replica_groups=mesh['zh'=4,'zl'=2,'x'=4,'y'=8,'core'=2] {'y','core'}, dimensions={1}, use_global_device_ids=true | all-gather | bytes 557056 | tf_op jit(solution)/shard_map/all_gather | solution.py:317
  179.4 0.8 copy.14
  (3 shorter events, 0.1 us)
Async XLA Ops:
  3.4 47.0 %copy-start = (bf16[1,2048,224]{1,2,0:T(8,128)(2,1)S(1)}, bf16[1,2048,224]{1,2,0:T(8,128)(2,1)}, u32[]{:S(2)}) copy-start(bf16[1,2048,224]{1,2,0:T(8,128)(2,1)} %param.17) | copy-start | bytes 2752516
  3.4 47.0 %copy-start.1 = (bf16[1,2048,224]{1,2,0:T(8,128)(2,1)S(1)}, bf16[1,2048,224]{1,2,0:T(8,128)(2,1)}, u32[]{:S(2)}) copy-start(bf16[1,2048,224]{1,2,0:T(8,128)(2,1)} %param.18) | copy-start | bytes 2752516
  43.5 7.0 %collective-permute-start.4 = (bf16[512,1024]{1,0:T(8,128)(2,1)S(1)}, bf16[512,1024]{1,0:T(8,128)(2,1)S(1)}, u32[]{:S(2)}, u32[]{:S(2)}) collective-permute-start(bf16[512,1024]{1,0:T(8,128)(2,1)S(1)} %bitcast.19), channel_id=1, source_target_pairs={{0,1},{1,0},{2,3},{3,2},{4,5},{5,4},{6,7},{7,6},{8,9},{9,8},{10,11... | collective-permute-start | bytes 3145736 | tf_op jit(solution)/shard_map/ppermute | solution.py:208
  50.4 1.2 copy-start.2
  54.5 4.6 %collective-permute-start.5 = (bf16[8,512,128]{2,1,0:T(8,128)(2,1)S(1)}, bf16[8,512,128]{2,1,0:T(8,128)(2,1)S(1)}, u32[]{:S(2)}, u32[]{:S(2)}) collective-permute-start(bf16[8,512,128]{2,1,0:T(8,128)(2,1)S(1)} %get-tuple-element.11), channel_id=1, source_target_pairs={{0,1},{1,0},{2,3},{3,2},{4,5},{5,4},{6,7},{7,6},{8,9},{9,8},{10,11... | collective-permute-start | bytes 3145736 | tf_op jit(solution)/shard_map/ppermute | solution.py:208
  60.3 7.0 %copy-start.9 = (bf16[384,1]{0,1:T(2,128)(2,1)S(1)}, bf16[384,1]{0,1:T(2,128)(2,1)}, u32[]{:S(2)}) copy-start(bf16[384,1]{0,1:T(2,128)(2,1)} %param.14) | copy-start | bytes 2308
  60.3 7.0 %copy-start.6 = (bf16[384,128]{1,0:T(8,128)(2,1)S(1)}, bf16[384,128]{1,0:T(8,128)(2,1)}, u32[]{:S(2)}) copy-start(bf16[384,128]{1,0:T(8,128)(2,1)} %param.13) | copy-start | bytes 294916
  60.4 7.0 %copy-start.7 = (bf16[384,128]{1,0:T(8,128)(2,1)S(1)}, bf16[384,128]{1,0:T(8,128)(2,1)}, u32[]{:S(2)}) copy-start(bf16[384,128]{1,0:T(8,128)(2,1)} %param.12) | copy-start | bytes 294916
  60.4 17.9 %copy-start.8 = (bf16[384,128]{1,0:T(8,128)(2,1)S(1)}, bf16[384,128]{1,0:T(8,128)(2,1)}, u32[]{:S(2)}) copy-start(bf16[384,128]{1,0:T(8,128)(2,1)} %param.11) | copy-start | bytes 294916
  60.4 53.7 %all-to-all-start.2 = ((bf16[8,512,128]{2,1,0:T(8,128)(2,1)}), bf16[8,512,128]{2,1,0:T(8,128)(2,1)S(1)}, u32[]{:S(2)}, u32[]{:S(2)}) async-start(bf16[8,512,128]{2,1,0:T(8,128)(2,1)} %add_convert_fusion), calls=%async_computation.2 | async-start | bytes 2097152 | tf_op jit(solution)/shard_map/all_to_all | solution.py:264
  67.4 31.8 %collective-permute-start.1 = (bf16[784,128]{1,0:T(8,128)(2,1)S(1)}, bf16[784,128]{1,0:T(8,128)(2,1)S(1)}, u32[]{:S(2)}, u32[]{:S(2)}) collective-permute-start(bf16[784,128]{1,0:T(8,128)(2,1)S(1)} %fusion.1.refs_0_), channel_id=1, source_target_pairs={{0,16},{16,32},{32,48},{48,0},{1,17},{17,33},{33,49},{49,1},{2,18}... | collective-permute-start | bytes 602120 | tf_op jit(solution)/shard_map/ppermute | solution.py:241
  70.8 28.4 %collective-permute-start.2 = (bf16[784,128]{1,0:T(8,128)(2,1)S(1)}, bf16[784,128]{1,0:T(8,128)(2,1)S(1)}, u32[]{:S(2)}, u32[]{:S(2)}) collective-permute-start(bf16[784,128]{1,0:T(8,128)(2,1)S(1)} %fusion.1.refs_0_), channel_id=1, source_target_pairs={{0,32},{16,48},{32,0},{48,16},{1,33},{17,49},{33,1},{49,17},{2,34}... | collective-permute-start | bytes 602120 | tf_op jit(solution)/shard_map/ppermute | solution.py:241
  75.2 24.1 %collective-permute-start.3 = (bf16[784,128]{1,0:T(8,128)(2,1)S(1)}, bf16[784,128]{1,0:T(8,128)(2,1)S(1)}, u32[]{:S(2)}, u32[]{:S(2)}) collective-permute-start(bf16[784,128]{1,0:T(8,128)(2,1)S(1)} %fusion.1.refs_0_), channel_id=1, source_target_pairs={{0,48},{16,0},{32,16},{48,32},{1,49},{17,1},{33,17},{49,33},{2,50}... | collective-permute-start | bytes 602120 | tf_op jit(solution)/shard_map/ppermute | solution.py:241
  78.3 5.7 %collective-permute-start = (bf16[384,128]{1,0:T(8,128)(2,1)S(1)}, bf16[384,128]{1,0:T(8,128)(2,1)S(1)}, u32[]{:S(2)}, u32[]{:S(2)}) collective-permute-start(bf16[384,128]{1,0:T(8,128)(2,1)S(1)} %copy-done.8), channel_id=1, source_target_pairs={{0,64},{64,0},{1,65},{65,1},{2,66},{66,2},{3,67},{67,3},{4,68},{68... | collective-permute-start | bytes 294920 | tf_op jit(solution)/shard_map/ppermute | solution.py:242
  114.1 3.6 %copy-start.3 = (bf16[8,512,128]{2,1,0:T(8,128)(2,1)}, bf16[8,512,128]{2,1,0:T(8,128)(2,1)S(1)}, u32[]{:S(2)}) copy-start(bf16[8,512,128]{2,1,0:T(8,128)(2,1)S(1)} %all-to-all-done.2.in_ref) | copy-start | bytes 3145732
  114.1 22.3 %all-to-all-start = ((bf16[8,400,128]{2,1,0:T(8,128)(2,1)}), bf16[8,400,128]{2,1,0:T(8,128)(2,1)S(1)}, u32[]{:S(2)}, u32[]{:S(2)}) async-start(bf16[8,400,128]{2,1,0:T(8,128)(2,1)} %stick_blocks.1), calls=%async_computation | async-start | bytes 1638400 | tf_op jit(solution)/shard_map/all_to_all | solution.py:289
  136.3 8.8 %copy-start.4 = (bf16[8,400,128]{2,1,0:T(8,128)(2,1)}, bf16[8,400,128]{2,1,0:T(8,128)(2,1)S(1)}, u32[]{:S(2)}) copy-start(bf16[8,400,128]{2,1,0:T(8,128)(2,1)S(1)} %all-to-all-done.in_ref) | copy-start | bytes 2457604
  136.3 18.1 %all-to-all-start.3 = ((bf16[32,16,128]{2,1,0:T(8,128)(2,1)}), bf16[32,16,128]{2,1,0:T(8,128)(2,1)S(1)}, u32[]{:S(2)}, u32[]{:S(2)}) async-start(bf16[32,16,128]{2,1,0:T(8,128)(2,1)} %bitcast.26), calls=%async_computation.3 | async-start | bytes 262144 | tf_op jit(solution)/shard_map/all_to_all | solution.py:309
  154.5 0.6 copy-start.5
